TPU v7x, 512 devices: a whole 4x4x16 slice. The times are simulated.
512 devices in a mesh: sp: 128 (over z, x, core), tp: 4 (over y).
Axes of the slice: x: 4, y: 4, z: 16, core: 2. Of those that a mesh axis runs over, the one named last changes fastest.
Arguments:
- tokens: bfloat16 [32768, 2048], P('sp', 'tp'), may hold values from -6 to 6
- segments: int32 [32768], P('sp'), may hold values from 0 to 63, never falling along the last dimension, each value on 1 to 1024 neighbouring positions
- in_gain: float32 [2, 2048], replicated, may hold values from 0.1 to 1.9
- w_value: bfloat16 [2, 2048, 1024], P(None, 'sp', 'tp'), may hold values from -0.125 to 0.125
- w_gate: bfloat16 [2, 2048, 1024], P(None, 'sp', 'tp'), may hold values from -0.125 to 0.125
- conv_taps: float32 [2, 129, 1024], P(None, None, 'tp'), may hold values from -4 to 4, as said below
- norm_gain: float32 [2, 1024], P(None, 'tp'), may hold values from 0.1 to 1.9
- w_out: bfloat16 [2, 1024, 2048], P(None, 'tp', 'sp'), may hold values from -0.1875 to 0.1875
Outputs:
- mixed: bfloat16 [32768, 2048], P('sp', 'tp')
Inputs may be any that keep to these rules, and one draw needn't show every extreme that they name: `segments`: document numbers never fall along the sequence; each document has 1 to 1024 positions, one has exactly 1024. `conv_taps`: real-valued taps.
All inputs are finite; a program needn't handle non-finite values.
Results may differ from a plain program's by a relative error of at most 0.014.
Values may be sent and summed in bfloat16 or wider, within the bound.
No kernel may reach another device: no remote copies, remote signals or barrier semaphores. Data moves between devices by JAX's collectives and lax.ppermute only.
A program may use at most 64 MiB of HBM per device.

v0:
```python
import jax
import jax.numpy as jnp
from jax import lax
from jax.sharding import PartitionSpec as P

CF = 1024
KW = 129
LAYERS = 2


EPSILON = 0.01


def turned_gather(arrays, axis, dims):
    turned = [jnp.moveaxis(a, dim, 0) for a, dim in zip(arrays, dims)]
    widths = [t[0].size for t in turned]
    both = jnp.concatenate([t.reshape(-1, w) for t, w in zip(turned, widths)], axis=1)
    result = lax.all_gather(both, axis, axis=0, tiled=True)
    pieces = jnp.split(result, [sum(widths[:k]) for k in range(1, len(widths))], axis=1)
    return tuple(
        (
            jnp.moveaxis(b.reshape(-1, *t.shape[1:]), 0, dim)
            for b, t, dim in zip(pieces, turned, dims)
        )
    )


def copy_for_each(x, axis):
    length = lax.axis_size(axis)
    return lax.all_to_all(jnp.broadcast_to(x[None], (length, *x.shape)), axis, 0, 0, tiled=True)


def laid_out(pieces, dim):
    dims = list(pieces.shape[1:])
    dims[dim] *= pieces.shape[0]
    return jnp.moveaxis(pieces, 0, dim).reshape(dims)


def gather_directly(x, axis, dim):
    pieces = copy_for_each(x, axis)
    return laid_out(pieces, dim)


def padded_2(x, sides, width):
    for axis, dim in sides:
        size, length = (lax.axis_size(axis), x.shape[dim])
        up = [(i, (i + 1) % size) for i in range(size - 1)]
        down = [(j, i) for i, j in up]
        last = lax.slice_in_dim(x, length - width, length, axis=dim)
        initial = lax.slice_in_dim(x, 0, width, axis=dim)
        before = lax.ppermute(last, axis, up)
        after = lax.ppermute(initial, axis, down)
        x = jnp.concatenate([before, x, after], axis=dim)
    return x


def taken_together(x, axis):
    everything = copy_for_each(x, axis)
    return jnp.sum(everything, axis=0)


def together(arrays, axis):
    flat, at, done = (jnp.concatenate([a.reshape(-1) for a in arrays]), 0, [])
    subtotal = taken_together(flat, axis)
    for a in arrays:
        done.append(subtotal[at : at + a.size].reshape(a.shape))
        at += a.size
    return tuple(done)


def in_blocks(x, dim, length):
    dims = x.shape
    pieces = x.reshape(*dims[:dim], length, dims[dim] // length, *dims[dim + 1 :])
    return jnp.moveaxis(pieces, dim, 0)


def sum_at_owner(x, axis, dim):
    length = lax.axis_size(axis)
    pieces = lax.all_to_all(in_blocks(x, dim, length), axis, 0, 0, tiled=True)
    return jnp.sum(pieces.astype(jnp.float32), axis=0)


def rms_rows(stream, gain):
    wide_vals = stream.astype(jnp.float32)
    scale = lax.rsqrt(jnp.mean(wide_vals * wide_vals, axis=-1, keepdims=True) + EPSILON)
    return (wide_vals * scale * gain).astype(jnp.bfloat16)


def per_device(tokens, segments, in_gain, w_value, w_gate, conv_taps, norm_gain, w_out):
    fringe = (KW - 1) // 2
    tok_rows = tokens.shape[0]
    chan_width = w_value.shape[2]
    whole_value, whole_gate, whole_out = turned_gather((w_value, w_gate, w_out), "sp", (1, 1, 2))
    stream = tokens
    for layer_idx in range(LAYERS):
        gathered = gather_directly(stream, "tp", 1)
        normed = rms_rows(gathered, in_gain[layer_idx])
        value_pre = jnp.dot(normed, whole_value[layer_idx], preferred_element_type=jnp.float32)
        gate_pre = jnp.dot(normed, whole_gate[layer_idx], preferred_element_type=jnp.float32)
        gated = (value_pre * jax.nn.sigmoid(gate_pre)).astype(jnp.bfloat16)
        padded, seg_wide = (
            padded_2(gated, (("sp", 0),), fringe),
            padded_2(segments, (("sp", 0),), fringe),
        )
        padded_wide = padded.astype(jnp.float32)
        tap_table = conv_taps[layer_idx]
        conv = jnp.zeros((tok_rows, chan_width), jnp.float32)
        for shift_idx in range(KW):
            same_doc = seg_wide[shift_idx : shift_idx + tok_rows] == segments
            conv = conv + jnp.where(
                same_doc[:, None],
                padded_wide[shift_idx : shift_idx + tok_rows] * tap_table[shift_idx],
                jnp.float32(0.0),
            )
        chan_sums, squares = together((jnp.sum(conv, axis=1), jnp.sum(conv * conv, axis=1)), "tp")
        row_mean = (chan_sums / CF)[:, None]
        row_var = jnp.maximum((squares / CF)[:, None] - row_mean * row_mean, 0.0)
        centred = conv - row_mean
        activated = jax.nn.silu(
            centred * lax.rsqrt(row_var + EPSILON) * norm_gain[layer_idx]
        ).astype(jnp.bfloat16)
        partials = jnp.dot(activated, whole_out[layer_idx], preferred_element_type=jnp.float32)
        summed = sum_at_owner(partials.astype(jnp.bfloat16), "tp", 1)
        stream = (stream.astype(jnp.float32) + summed).astype(jnp.bfloat16)
    return stream


def solution(mesh):
    in_specs = (
        P("sp", "tp"),
        P("sp"),
        P(),
        P(None, "sp", "tp"),
        P(None, "sp", "tp"),
        P(None, None, "tp"),
        P(None, "tp"),
        P(None, "tp", "sp"),
    )
    out_specs = P("sp", "tp")
    return jax.shard_map(
        per_device, mesh=mesh, in_specs=in_specs, out_specs=out_specs, check_vma=False
    )
```

profile of v0, /device:TPU:6, one launch (start us, length us, event | category | flops | bytes accessed | tf_op | source)
XLA Modules:
  0.0 294.6 jit_solution(12067083075690503724)
XLA Ops:
  11.6 4.5 %all-to-all-start = ((bf16[4,256,512]{1,2,0:T(8,128)(2,1)}), bf16[4,256,512]{1,2,0:T(8,128)(2,1)S(1)}, u32[]{:S(2)}, u32[]{:S(2)}) async-start(bf16[4,256,512]{1,2,0:T(8,128)(2,1)} %broadcast_in_dim.1581), calls=%async_computation | async-start | bytes 2097152 | tf_op jit(solution)/shard_map/all_to_all | solution.py:30
  16.1 1.9 collective-permute-start.3
  18.1 2.4 collective-permute-start
  31.8 125.4 %all-gather.2.cloned.1.call-done = bf16[2048,1536]{1,0:T(8,128)(2,1)} async-done(((bf16[16,1536]{1,0:T(8,128)(2,1)}), bf16[2048,1536]{1,0:T(8,128)(2,1)}) %all-gather.2.cloned.1.call-update) | async-done | bytes 6291472 | tf_op jit(solution)/shard_map/all_gather | solution.py:18
  157.2 4.7 %fusion.544 = (bf16[2048,512]{1,0:T(8,128)(2,1)S(1)}, bf16[2048,512]{1,0:T(8,128)(2,1)}, bf16[2048,512]{1,0:T(8,128)(2,1)S(1)}) fusion(bf16[2048,1536]{1,0:T(8,128)(2,1)} %all-gather.2.cloned.1.call-done), kind=kLoop, calls=%fused_computation.970 | loop fusion | bytes 12582912 | tf_op jit(solution)/shard_map/split | solution.py:19
  163.5 2.8 collective-permute-start.2
  166.3 1.9 collective-permute-start.1
  168.4 3.1 %collective-permute-done.1 = bf16[64,256]{1,0:T(8,128)(2,1)S(1)} collective-permute-done((bf16[64,256]{1,0:T(8,128)(2,1)S(1)}, bf16[64,256]{1,0:T(8,128)(2,1)S(1)}, u32[]{:S(2)}, u32[]{:S(2)}) %collective-permute-start.1) | collective-permute-done | bytes 32800 | tf_op jit(solution)/shard_map/ppermute | solution.py:51
  172.0 2.5 fusion.494
  175.0 9.2 %fusion.541 = (f32[256]{0:T(256)S(1)}, f32[256]{0:T(256)S(1)}, f32[256,256]{1,0:T(8,128)S(1)}) fusion(f32[256]{0:T(256)} %bitcast.354, f32[384,256]{1,0:T(8,128)S(1)} %maximum_convert_fusion, pred[256]{0:T(512)(128)(4,1)} %get-tuple-element.404, f32[256]{0:T(256)} %bitcast.355, pred[256]{0:T(512)(128)(4,1)} %get-tuple-element.405, f32[256]{0:T(256)} %bitcast.356, ...), kind=kLoop, calls=%fused_computation.969 | loop fusion | flops 21757440 | bytes 29502720 | tf_op jit(solution)/shard_map/reduce_sum | solution.py:115
  184.8 4.3 %all-to-all-start.1 = ((f32[4,1,512]{2,1,0:T(1,128)}), f32[4,1,512]{2,1,0:T(1,128)S(1)}, u32[]{:S(2)}, u32[]{:S(2)}) async-start(f32[4,1,512]{2,1,0:T(1,128)} %broadcast_in_dim.1710), calls=%async_computation.1 | async-start | bytes 16384 | tf_op jit(solution)/shard_map/all_to_all | solution.py:30
  190.5 4.0 %copy.49 = bf16[2048,512]{0,1:T(8,128)(2,1)} copy(bf16[2048,512]{1,0:T(8,128)(2,1)} %get-tuple-element.14) | data formatting | bytes 4194304 | tf_op jit(solution)/shard_map/reshape | solution.py:22
  197.4 4.8 %all-to-all-start.2 = ((bf16[4,256,512]{2,1,0:T(8,128)(2,1)}), bf16[4,256,512]{2,1,0:T(8,128)(2,1)S(1)}, u32[]{:S(2)}, u32[]{:S(2)}) async-start(bf16[4,256,512]{2,1,0:T(8,128)(2,1)} %bitcast.332), calls=%async_computation.2 | async-start | bytes 2097152 | tf_op jit(solution)/shard_map/all_to_all | solution.py:79
  203.7 14.1 %all-to-all-done.2 = bf16[4,256,512]{2,1,0:T(8,128)(2,1)S(1)} async-done(((bf16[4,256,512]{2,1,0:T(8,128)(2,1)}), bf16[4,256,512]{2,1,0:T(8,128)(2,1)S(1)}, u32[]{:S(2)}, u32[]{:S(2)}) %all-to-all-start.2) | async-done | bytes 1048608 | tf_op jit(solution)/shard_map/all_to_all | solution.py:79
  220.1 3.7 %all-to-all-start.3 = ((bf16[4,256,512]{1,2,0:T(8,128)(2,1)}), bf16[4,256,512]{1,2,0:T(8,128)(2,1)S(1)}, u32[]{:S(2)}, u32[]{:S(2)}) async-start(bf16[4,256,512]{1,2,0:T(8,128)(2,1)} %broadcast_in_dim.1711), calls=%async_computation.3 | async-start | bytes 2097152 | tf_op jit(solution)/shard_map/all_to_all | solution.py:30
  230.0 8.4 %all-to-all-done.3 = bf16[4,256,512]{1,2,0:T(8,128)(2,1)S(1)} async-done(((bf16[4,256,512]{1,2,0:T(8,128)(2,1)}), bf16[4,256,512]{1,2,0:T(8,128)(2,1)S(1)}, u32[]{:S(2)}, u32[]{:S(2)}) %all-to-all-start.3) | async-done | bytes 1048608 | tf_op jit(solution)/shard_map/all_to_all | solution.py:30
  240.8 1.9 collective-permute-start.5
  242.7 2.4 collective-permute-start.4
  246.0 1.9 collective-permute-done.4
  248.4 2.6 fusion.238
  251.4 9.2 %fusion.540 = (f32[256]{0:T(256)S(1)}, f32[256]{0:T(256)S(1)}, f32[256,256]{1,0:T(8,128)S(1)}) fusion(f32[256]{0:T(256)} %bitcast.350, f32[384,256]{1,0:T(8,128)S(1)} %maximum_convert_fusion.1, pred[256]{0:T(512)(128)(4,1)} %get-tuple-element.404, f32[256]{0:T(256)} %bitcast.353, pred[256]{0:T(512)(128)(4,1)} %get-tuple-element.405, f32[256]{0:T(256)} %bitcast.351, ...), kind=kLoop, calls=%fused_computation.968 | loop fusion | flops 21757440 | bytes 29502720 | tf_op jit(solution)/shard_map/reduce_sum | solution.py:115
  260.7 7.7 %all_to_all.32 = f32[4,1,512]{2,1,0:T(1,128)S(1)} all-to-all(f32[4,1,512]{2,1,0:T(1,128)S(1)} %broadcast_in_dim.1712), channel_id=1, replica_groups=mesh['sp'=128,'tp'=4] {'tp'}, dimensions={0} | all-to-all | bytes 16384 | tf_op jit(solution)/shard_map/all_to_all | solution.py:30
  268.4 1.7 convolution_convert_fusion
  270.2 16.7 %all_to_all.33 = bf16[4,256,512]{2,1,0:T(8,128)(2,1)S(1)} all-to-all(bf16[4,256,512]{2,1,0:T(8,128)(2,1)S(1)} %bitcast.333), channel_id=1, replica_groups=mesh['sp'=128,'tp'=4] {'tp'}, dimensions={0} | all-to-all | bytes 2097152 | tf_op jit(solution)/shard_map/all_to_all | solution.py:79
  (268 shorter events, 37.8 us)
Async XLA Ops:
  6.5 9.5 %copy-start.3 = (s32[256]{0:T(256)S(1)}, s32[256]{0:T(256)}, u32[]{:S(2)}) copy-start(s32[256]{0:T(256)} %param.9) | copy-start | bytes 3076
  6.5 150.7 %all-gather.2.cloned.1.call-start = ((), (), s32[]{:S(2)}) async-start(), calls=%async_computation.6 | async-start | bytes 6340608 | tf_op jit(solution)/shard_map/all_gather | solution.py:18
  6.5 14.0 %copy-start.4 = (f32[2,2048]{1,0:T(2,128)S(1)}, f32[2,2048]{1,0:T(2,128)}, u32[]{:S(2)}) copy-start(f32[2,2048]{1,0:T(2,128)} %param.10) | copy-start | bytes 49156
  7.3 13.3 %copy-start.2 = (f32[2,129,256]{2,0,1:T(2,128)S(1)}, f32[2,129,256]{2,0,1:T(2,128)}, u32[]{:S(2)}) copy-start(f32[2,129,256]{2,0,1:T(2,128)} %param.13) | copy-start | bytes 792580
  11.6 19.6 %all-to-all-start = ((bf16[4,256,512]{1,2,0:T(8,128)(2,1)}), bf16[4,256,512]{1,2,0:T(8,128)(2,1)S(1)}, u32[]{:S(2)}, u32[]{:S(2)}) async-start(bf16[4,256,512]{1,2,0:T(8,128)(2,1)} %broadcast_in_dim.1581), calls=%async_computation | async-start | bytes 2097152 | tf_op jit(solution)/shard_map/all_to_all | solution.py:30
  16.1 9.7 %collective-permute-start.3 = (s32[64]{0:T(128)S(1)}, s32[64]{0:T(128)S(1)}, u32[]{:S(2)}, u32[]{:S(2)}) collective-permute-start(s32[64]{0:T(128)S(1)} %get-tuple-element.413), channel_id=1, source_target_pairs={{4,0},{8,4},{12,8},{16,12},{20,16},{24,20},{28,24},{32,28},{36,32}... | collective-permute-start | bytes 776 | tf_op jit(solution)/shard_map/ppermute | solution.py:52
  18.1 10.7 %collective-permute-start = (s32[64]{0:T(128)S(1)}, s32[64]{0:T(128)S(1)}, u32[]{:S(2)}, u32[]{:S(2)}) collective-permute-start(s32[64]{0:T(128)S(1)} %get-tuple-element.412), channel_id=1, source_target_pairs={{0,4},{4,8},{8,12},{12,16},{16,20},{20,24},{24,28},{28,32},{32,36}... | collective-permute-start | bytes 776 | tf_op jit(solution)/shard_map/ppermute | solution.py:51
  163.5 4.9 %collective-permute-start.2 = (bf16[64,256]{1,0:T(8,128)(2,1)S(1)}, bf16[64,256]{1,0:T(8,128)(2,1)S(1)}, u32[]{:S(2)}, u32[]{:S(2)}) collective-permute-start(bf16[64,256]{1,0:T(8,128)(2,1)S(1)} %get-tuple-element.277), channel_id=1, source_target_pairs={{4,0},{8,4},{12,8},{16,12},{20,16},{24,20},{28,24},{32,28},{36,32}... | collective-permute-start | bytes 98312 | tf_op jit(solution)/shard_map/ppermute | solution.py:52
  166.3 5.2 %collective-permute-start.1 = (bf16[64,256]{1,0:T(8,128)(2,1)S(1)}, bf16[64,256]{1,0:T(8,128)(2,1)S(1)}, u32[]{:S(2)}, u32[]{:S(2)}) collective-permute-start(bf16[64,256]{1,0:T(8,128)(2,1)S(1)} %get-tuple-element.276), channel_id=1, source_target_pairs={{0,4},{4,8},{8,12},{12,16},{16,20},{20,24},{24,28},{28,32},{32,36}... | collective-permute-start | bytes 98312 | tf_op jit(solution)/shard_map/ppermute | solution.py:51
  168.3 6.2 %copy-start.85 = (pred[256]{0:T(512)(128)(4,1)}, pred[256]{0:T(512)(128)(4,1)S(1)}, u32[]{:S(2)}) copy-start(pred[256]{0:T(512)(128)(4,1)S(1)} %get-tuple-element.332) | copy-start | bytes 772
  168.3 6.2 %copy-start.86 = (pred[256]{0:T(512)(128)(4,1)}, pred[256]{0:T(512)(128)(4,1)S(1)}, u32[]{:S(2)}) copy-start(pred[256]{0:T(512)(128)(4,1)S(1)} %get-tuple-element.333) | copy-start | bytes 772
  168.4 6.2 %copy-start.87 = (pred[256]{0:T(512)(128)(4,1)}, pred[256]{0:T(512)(128)(4,1)S(1)}, u32[]{:S(2)}) copy-start(pred[256]{0:T(512)(128)(4,1)S(1)} %get-tuple-element.334) | copy-start | bytes 772
  168.4 6.2 %copy-start.88 = (pred[256]{0:T(512)(128)(4,1)}, pred[256]{0:T(512)(128)(4,1)S(1)}, u32[]{:S(2)}) copy-start(pred[256]{0:T(512)(128)(4,1)S(1)} %get-tuple-element.335) | copy-start | bytes 772
  168.4 6.2 %copy-start.89 = (pred[256]{0:T(512)(128)(4,1)}, pred[256]{0:T(512)(128)(4,1)S(1)}, u32[]{:S(2)}) copy-start(pred[256]{0:T(512)(128)(4,1)S(1)} %get-tuple-element.336) | copy-start | bytes 772
  168.4 6.2 %copy-start.90 = (pred[256]{0:T(512)(128)(4,1)}, pred[256]{0:T(512)(128)(4,1)S(1)}, u32[]{:S(2)}) copy-start(pred[256]{0:T(512)(128)(4,1)S(1)} %get-tuple-element.337) | copy-start | bytes 772
  168.4 6.2 %copy-start.91 = (pred[256]{0:T(512)(128)(4,1)}, pred[256]{0:T(512)(128)(4,1)S(1)}, u32[]{:S(2)}) copy-start(pred[256]{0:T(512)(128)(4,1)S(1)} %get-tuple-element.338) | copy-start | bytes 772
  168.4 6.2 %copy-start.92 = (pred[256]{0:T(512)(128)(4,1)}, pred[256]{0:T(512)(128)(4,1)S(1)}, u32[]{:S(2)}) copy-start(pred[256]{0:T(512)(128)(4,1)S(1)} %get-tuple-element.339) | copy-start | bytes 772
  168.4 6.2 %copy-start.93 = (pred[256]{0:T(512)(128)(4,1)}, pred[256]{0:T(512)(128)(4,1)S(1)}, u32[]{:S(2)}) copy-start(pred[256]{0:T(512)(128)(4,1)S(1)} %get-tuple-element.340) | copy-start | bytes 772
  168.4 6.2 %copy-start.94 = (pred[256]{0:T(512)(128)(4,1)}, pred[256]{0:T(512)(128)(4,1)S(1)}, u32[]{:S(2)}) copy-start(pred[256]{0:T(512)(128)(4,1)S(1)} %get-tuple-element.341) | copy-start | bytes 772
  184.8 9.6 %all-to-all-start.1 = ((f32[4,1,512]{2,1,0:T(1,128)}), f32[4,1,512]{2,1,0:T(1,128)S(1)}, u32[]{:S(2)}, u32[]{:S(2)}) async-start(f32[4,1,512]{2,1,0:T(1,128)} %broadcast_in_dim.1710), calls=%async_computation.1 | async-start | bytes 16384 | tf_op jit(solution)/shard_map/all_to_all | solution.py:30
  197.4 20.4 %all-to-all-start.2 = ((bf16[4,256,512]{2,1,0:T(8,128)(2,1)}), bf16[4,256,512]{2,1,0:T(8,128)(2,1)S(1)}, u32[]{:S(2)}, u32[]{:S(2)}) async-start(bf16[4,256,512]{2,1,0:T(8,128)(2,1)} %bitcast.332), calls=%async_computation.2 | async-start | bytes 2097152 | tf_op jit(solution)/shard_map/all_to_all | solution.py:79
  220.1 18.2 %all-to-all-start.3 = ((bf16[4,256,512]{1,2,0:T(8,128)(2,1)}), bf16[4,256,512]{1,2,0:T(8,128)(2,1)S(1)}, u32[]{:S(2)}, u32[]{:S(2)}) async-start(bf16[4,256,512]{1,2,0:T(8,128)(2,1)} %broadcast_in_dim.1711), calls=%async_computation.3 | async-start | bytes 2097152 | tf_op jit(solution)/shard_map/all_to_all | solution.py:30
  240.8 5.2 %collective-permute-start.5 = (bf16[64,256]{1,0:T(8,128)(2,1)S(1)}, bf16[64,256]{1,0:T(8,128)(2,1)S(1)}, u32[]{:S(2)}, u32[]{:S(2)}) collective-permute-start(bf16[64,256]{1,0:T(8,128)(2,1)S(1)} %get-tuple-element.275), channel_id=1, source_target_pairs={{4,0},{8,4},{12,8},{16,12},{20,16},{24,20},{28,24},{32,28},{36,32}... | collective-permute-start | bytes 98312 | tf_op jit(solution)/shard_map/ppermute | solution.py:52
  242.7 5.2 %collective-permute-start.4 = (bf16[64,256]{1,0:T(8,128)(2,1)S(1)}, bf16[64,256]{1,0:T(8,128)(2,1)S(1)}, u32[]{:S(2)}, u32[]{:S(2)}) collective-permute-start(bf16[64,256]{1,0:T(8,128)(2,1)S(1)} %get-tuple-element.274), channel_id=1, source_target_pairs={{0,4},{4,8},{8,12},{12,16},{16,20},{20,24},{24,28},{28,32},{32,36}... | collective-permute-start | bytes 98312 | tf_op jit(solution)/shard_map/ppermute | solution.py:51
  (82 other events, 246.9 us)
Sparse Core Ops, SparseCore 0:
  10.5 146.6 all-gather.1
where the time goes:
time: 298 us; the launch traced here: 295 us
  waiting for transfers between devices  153 us (51%)
  local copies, waits for them, and re-layouts  33.2 us (11%)
  other arithmetic  32.9 us (11%)
  starting transfers between devices  30.6 us (10%)
  blocking collectives  24.3 us (8%)
  between operations  15.2 us (5%)
  matrix products  5.44 us (2%)
    all_gather x1, waiting for transfers between devices, turned_gather(): result = lax.all_gather(both, axis, axis=0, tiled=True)  125 us
    reduce_sum x2, other arithmetic, per_device(): jnp.sum(conv, axis=1)  18.4 us
    all_to_all x1, blocking collectives, sum_at_owner(): pieces = lax.all_to_all(in_blocks(x, dim, length), axis, 0, 0, tiled=True)  16.7 us
    all_to_all x1, waiting for transfers between devices, sum_at_owner(): pieces = lax.all_to_all(in_blocks(x, dim, length), axis, 0, 0, tiled=True)  14.1 us
    slice x14, local copies, waits for them, and re-layouts, per_device(): tap_table[shift_idx]  13.8 us
    all_to_all x3, starting transfers between devices, copy_for_each(): lax.all_to_all(jnp.broadcast_to(x[None], (length, *x.shape)), axis, 0, 0,...  12.4 us
    all_to_all x3, waiting for transfers between devices, copy_for_each(): lax.all_to_all(jnp.broadcast_to(x[None], (length, *x.shape)), axis, 0, 0,...  8.54 us
    all_to_all x1, blocking collectives, copy_for_each(): lax.all_to_all(jnp.broadcast_to(x[None], (length, *x.shape)), axis, 0, 0,...  7.66 us
  transfers between devices with their start and end apart: 11, of which 6 were waited for; matrix products, arithmetic and copies ran while one was open for 9% of the time, Pallas kernels for 0%

commit v1 on v0

v1 whole, which is shorter than its diff:
```python
import functools

import jax
import jax.numpy as jnp
from jax import lax
from jax.experimental import pallas as pl
from jax.experimental.pallas import tpu as pltpu
from jax.sharding import Mesh
from jax.sharding import PartitionSpec as P

D = 2048
CF = 1024
KW = 129
LAYERS = 2
EPSILON = 0.01
R = (KW - 1) // 2
SP = ("z", "x", "c")
NZ, NX, NC, NT = 16, 4, 2, 4
TOK = 256
CH = 256
FD = 512
LANES = 128
TILE = 64

F32 = jnp.float32
BF16 = jnp.bfloat16
LIMIT = pltpu.CompilerParams(vmem_limit_bytes=24 * 1024 * 1024)
VMEM = pl.BlockSpec(memory_space=pltpu.VMEM)
SMEM = pl.BlockSpec(memory_space=pltpu.SMEM)


def assemble(own_ref, other_ref, core, scratch):
    for x in range(NX):
        scratch[:, x, core] = own_ref[x]
        scratch[:, x, 1 - core] = other_ref[x]


def gate_kernel(core_ref, g_ref, gain_ref, own_ref, other_ref, out_ref, w_ref):
    assemble(own_ref, other_ref, core_ref[0], w_ref)
    wide = [g_ref[y].astype(F32) for y in range(NT)]
    square = sum(jnp.sum(v * v, axis=1, keepdims=True) for v in wide)
    scale = lax.rsqrt(square * (1.0 / D) + EPSILON)
    pre = jnp.zeros((TOK, 2 * CH), F32)
    step = NZ // NT
    for y in range(NT):
        normed = (wide[y] * scale * gain_ref[y : y + 1, :]).astype(BF16)
        w = w_ref[y * step : (y + 1) * step].reshape(FD, 2 * CH)
        pre = pre + jnp.dot(normed, w, preferred_element_type=F32)
    out_ref[...] = (pre[:, :CH] * jax.nn.sigmoid(pre[:, CH:])).astype(BF16)


def gate(core, gathered, gain, own, other):
    return pl.pallas_call(
        gate_kernel,
        out_shape=jax.ShapeDtypeStruct((TOK, CH), BF16),
        in_specs=[SMEM, VMEM, VMEM, VMEM, VMEM],
        out_specs=VMEM,
        scratch_shapes=[pltpu.VMEM((NZ, NX, NC, 16, 2 * CH), BF16)],
        name="gate",
        compiler_params=LIMIT,
    )(core, gathered, gain, own, other)


def conv_kernel(before_ref, mid_ref, after_ref, seg_ref, taps_ref, conv_ref, stat_ref, x_ref):
    for h in range(CH // LANES):
        cols = slice(h * LANES, (h + 1) * LANES)
        x_ref[h, 0:R] = before_ref[:, cols].astype(F32)
        x_ref[h, R : R + TOK] = mid_ref[:, cols].astype(F32)
        x_ref[h, R + TOK : R + TOK + R] = after_ref[:, cols].astype(F32)

    def tile(i, carry):
        first = pl.multiple_of(i * TILE, TILE)
        own = seg_ref[pl.ds(first + R, TILE), :]
        acc = [jnp.zeros((TILE, LANES), F32) for _ in range(CH // LANES)]
        for k in range(KW):
            same = seg_ref[pl.ds(first + k, TILE), :] == own
            for h in range(CH // LANES):
                tap = taps_ref[k : k + 1, h * LANES : (h + 1) * LANES]
                window = x_ref[h, pl.ds(first + k, TILE), :]
                acc[h] = acc[h] + jnp.where(same, window * tap, 0.0)
        for h in range(CH // LANES):
            conv_ref[pl.ds(first, TILE), h * LANES : (h + 1) * LANES] = acc[h]
        return carry

    lax.fori_loop(0, TOK // TILE, tile, 0)
    conv = conv_ref[...]
    ones = jnp.ones((8, CH), F32)
    dims = (((1,), (1,)), ((), ()))
    total = lax.dot_general(ones, conv, dims, precision=lax.Precision.HIGHEST, preferred_element_type=F32)
    square = lax.dot_general(ones, conv * conv, dims, precision=lax.Precision.HIGHEST, preferred_element_type=F32)
    stat_ref[0:1, :] = total[0:1, :]
    stat_ref[1:2, :] = square[0:1, :]


def convolve(before, mid, after, seg, taps):
    return pl.pallas_call(
        conv_kernel,
        out_shape=(jax.ShapeDtypeStruct((TOK, CH), F32), jax.ShapeDtypeStruct((2, TOK), F32)),
        in_specs=[VMEM] * 5,
        out_specs=(VMEM, VMEM),
        scratch_shapes=[pltpu.VMEM((CH // LANES, TOK + 2 * R, LANES), F32)],
        name="conv",
        compiler_params=LIMIT,
    )(before, mid, after, seg, taps)


def out_kernel(core_ref, conv_ref, stat_ref, gain_ref, own_ref, other_ref, out_ref, w_ref):
    assemble(own_ref, other_ref, core_ref[0], w_ref)
    stat = stat_ref[...]
    kind = lax.broadcasted_iota(jnp.int32, (2 * NT, CH), 0) % 2
    dims = (((0,), (0,)), ((), ()))

    def spread(which):
        pick = jnp.where(kind == which, 1.0, 0.0).astype(F32)
        return lax.dot_general(stat, pick, dims, precision=lax.Precision.HIGHEST, preferred_element_type=F32)

    mean = spread(0) * (1.0 / CF)
    var = jnp.maximum(spread(1) * (1.0 / CF) - mean * mean, 0.0)
    v = (conv_ref[...] - mean) * lax.rsqrt(var + EPSILON) * gain_ref[...]
    act = jax.nn.silu(v).astype(BF16)
    step = NZ // NT
    for y in range(NT):
        w = w_ref[y * step : (y + 1) * step].reshape(FD, CH)
        part = lax.dot_general(act, w, (((1,), (1,)), ((), ())), preferred_element_type=F32)
        out_ref[y] = part.astype(BF16)


def project(core, conv, stat, gain, own, other):
    return pl.pallas_call(
        out_kernel,
        out_shape=jax.ShapeDtypeStruct((NT, TOK, FD), BF16),
        in_specs=[SMEM, VMEM, VMEM, VMEM, VMEM, VMEM],
        out_specs=VMEM,
        scratch_shapes=[pltpu.VMEM((NZ, NX, NC, 16, CH), BF16)],
        name="project",
        compiler_params=LIMIT,
    )(core, conv, stat, gain, own, other)


def add_kernel(copies, stream_ref, parts_ref, out_ref):
    total = stream_ref[...].astype(F32) + sum(parts_ref[y].astype(F32) for y in range(NT))
    total = total.astype(BF16)
    if copies == 1:
        out_ref[...] = total
    else:
        for y in range(copies):
            out_ref[y] = total


def add_parts(stream, parts, copies):
    shape = (TOK, FD) if copies == 1 else (copies, TOK, FD)
    return pl.pallas_call(
        functools.partial(add_kernel, copies),
        out_shape=jax.ShapeDtypeStruct(shape, BF16),
        in_specs=[VMEM, VMEM],
        out_specs=VMEM,
        name="add_parts",
        compiler_params=LIMIT,
    )(stream, parts)


def copies_of(x, n):
    return jnp.broadcast_to(x[None], (n, *x.shape))


def swap_core(x):
    return lax.ppermute(x, "c", [(0, 1), (1, 0)])


def exchange(x, axis):
    return lax.all_to_all(x, axis, 0, 0, tiled=True)


def shift_ring(x, step):
    return lax.ppermute(x, "x", [(i, (i + step) % NX) for i in range(NX)])


def neighbours(x):
    n = NZ * NX * NC
    up = [(i, i + 1) for i in range(n - 1)]
    down = [(j, i) for i, j in up]
    before = lax.ppermute(x[x.shape[0] - R :], SP, up)
    after = lax.ppermute(x[:R], SP, down)
    return before, after


def after_(x, *others):
    return lax.optimization_barrier((x, *others))[0]


def per_device(tokens, segments, in_gain, w_value, w_gate, conv_taps, norm_gain, w_out):
    core = lax.axis_index("c").astype(jnp.int32).reshape(1)
    gains = in_gain.reshape(LAYERS, NT, FD)

    out_t = jnp.swapaxes(w_out, 1, 2)
    own = jnp.concatenate(
        [w_value[0], w_gate[0], out_t[0], w_value[1], w_gate[1], out_t[1]], axis=1
    )
    gathered = exchange(copies_of(tokens, NT), "tp")
    column = lax.all_gather(own, "z", axis=0, tiled=True)

    def over_x(piece):
        width = piece.shape[1]
        return exchange(copies_of(piece, NX), "x").reshape(NX, NZ, 16, width)

    vg0 = over_x(column[:, : 2 * CH])
    vg0_other = swap_core(vg0)
    out0 = over_x(after_(column[:, 2 * CH : 3 * CH], vg0))
    seg_before, seg_after = neighbours(after_(segments, column))
    seg_wide = jnp.concatenate([seg_before, segments, seg_after])
    seg_lanes = jnp.broadcast_to(seg_wide[:, None], (TOK + 2 * R, LANES))

    stream = tokens
    rest = None
    for layer in range(LAYERS):
        if layer == 0:
            vg, vg_other = vg0, vg0_other
        else:
            vg, vg_other = vg1, vg1_other
        gated = gate(core, gathered, gains[layer], vg, vg_other)
        before, after = neighbours(gated)
        conv, stat = convolve(before, gated, after, seg_lanes, conv_taps[layer])
        if layer == 0:
            out, out_other = out0, swap_core(out0)
        else:
            out, out_other = out1, out1_other
        stats = lax.all_gather(stat, "tp", axis=0, tiled=True)
        parts = project(core, conv, stats, norm_gain[layer].reshape(1, CH), out, out_other)
        received = exchange(parts, "tp")
        if layer == 0:
            rest = over_x(after_(column[:, 3 * CH :], out0))
            rest_other = swap_core(rest)
            vg1, out1 = rest[..., : 2 * CH], rest[..., 2 * CH :]
            vg1_other, out1_other = rest_other[..., : 2 * CH], rest_other[..., 2 * CH :]
            spread = add_parts(stream, received, NT)
            stream = spread[0]
            gathered = exchange(spread, "tp")
        else:
            stream = add_parts(stream, received, 1)
    return stream


def solution(mesh):
    fine = Mesh(mesh.devices.reshape(NZ, NX, NC, NT), ("z", "x", "c", "tp"))
    in_specs = (
        P(SP, "tp"),
        P(SP),
        P(),
        P(None, SP, "tp"),
        P(None, SP, "tp"),
        P(None, None, "tp"),
        P(None, "tp"),
        P(None, "tp", SP),
    )
    out_specs = P(SP, "tp")
    return jax.shard_map(
        per_device, mesh=fine, in_specs=in_specs, out_specs=out_specs, check_vma=False
    )
```

time: 298 us -> 217 us (0.73)
  waiting for transfers between devices: 153 us -> 56.8 us
  blocking collectives: 24.3 us -> 71.5 us
  other arithmetic: 32.9 us -> 0.08 us
  Pallas kernels: 0 us -> 24.3 us
  local copies, waits for them, and re-layouts: 33.2 us -> 15 us
  starting transfers between devices: 30.6 us -> 47.2 us
  between operations: 15.2 us -> 0.3 us
  matrix products: 5.44 us -> 0 us
    all_gather x1 -> x0, waiting for transfers between devices: 125 us -> none  [turned_gather(): result = lax.all_gather(both, axis, axis=0, tiled=True)]
    all_gather x0 -> x3, blocking collectives: none -> 61 us  [the longest x1 40.1 us: per_device(): column = lax.all_gather(own, 'z', axis=0, tiled=True)]
    all_to_all x4 -> x6, waiting for transfers between devices: 22.6 us -> 52.9 us  [exchange(): return lax.all_to_all(x, axis, 0, 0, tiled=True)]
    pallas_call x0 -> x8, Pallas kernels: none -> 24.3 us  [the longest x2 14 us: convolve(): pl.pallas_call(conv_kernel, out_shape=(jax.ShapeDtypeStruct((TOK, CH), F3...]
    reduce_sum x8 -> x0, other arithmetic: 19.3 us -> none  [the longest x2 18.4 us: per_device(): jnp.sum(conv, axis=1)]
    all_to_all x2 -> x1, blocking collectives: 24.3 us -> 10.5 us  [exchange(): return lax.all_to_all(x, axis, 0, 0, tiled=True)]
    all_to_all x4 -> x6, starting transfers between devices: 17.2 us -> 26.8 us  [exchange(): return lax.all_to_all(x, axis, 0, 0, tiled=True)]
    slice x19 -> x13, local copies, waits for them, and re-layouts: 15.3 us -> 6.13 us  [the longest x2 2.37 us: per_device(): vg1, out1 = (rest[..., :2 * CH], rest[..., 2 * CH:])]
  transfers between devices with their start and end apart: 11 -> 15, of which waited for: 6 -> 7; matrix products, arithmetic and copies ran while one was open for 9% -> 4% of each run, Pallas kernels for 0% -> 6%
where the time goes in v1:
time: 217 us; the launch traced here: 215 us
  blocking collectives  71.5 us (33%)
  waiting for transfers between devices  56.8 us (26%)
  starting transfers between devices  47.2 us (22%)
  Pallas kernels  24.3 us (11%)
  local copies, waits for them, and re-layouts  15 us (7%)
    all_to_all x6, waiting for transfers between devices, exchange(): return lax.all_to_all(x, axis, 0, 0, tiled=True)  52.9 us
    all_gather x1, blocking collectives, per_device(): column = lax.all_gather(own, 'z', axis=0, tiled=True)  40.1 us
    all_to_all x6, starting transfers between devices, exchange(): return lax.all_to_all(x, axis, 0, 0, tiled=True)  26.8 us
    all_gather x2, blocking collectives, per_device(): stats = lax.all_gather(stat, 'tp', axis=0, tiled=True)  20.9 us
    pallas_call x2, Pallas kernels, convolve(): pl.pallas_call(conv_kernel, out_shape=(jax.ShapeDtypeStruct((TOK, CH), F3...  14 us
    all_to_all x1, blocking collectives, exchange(): return lax.all_to_all(x, axis, 0, 0, tiled=True)  10.5 us
    ppermute x3, starting transfers between devices, neighbours(): after = lax.ppermute(x[:R], SP, down)  8.43 us
    ppermute x3, starting transfers between devices, neighbours(): before = lax.ppermute(x[x.shape[0] - R:], SP, up)  6.24 us
  transfers between devices with their start and end apart: 15, of which 7 were waited for; matrix products, arithmetic and copies ran while one was open for 4% of the time, Pallas kernels for 6%

profile of v1, /device:TPU:6, one launch (start us, length us, event | category | flops | bytes accessed | tf_op | source)
XLA Modules:
  0.0 215.1 jit_solution(13371988889338399518)
XLA Ops:
  4.2 40.1 %all_gather.9 = bf16[256,1536]{1,0:T(8,128)(2,1)S(1)} all-gather(bf16[16,1536]{1,0:T(8,128)(2,1)S(1)} %constant_dynamic-update-slice_fusion), channel_id=1, replica_groups=mesh['z'=16,'x'=4,'c'=2,'tp'=4] {'z'}, dimensions={0}, use_global_device_ids=true | all-gather | bytes 835584 | tf_op jit(solution)/shard_map/all_gather | solution.py:200
  45.5 4.9 %all-to-all-start.1 = ((bf16[4,256,512]{2,1,0:T(8,128)(2,1)}), bf16[4,256,512]{2,1,0:T(8,128)(2,1)S(1)}, u32[]{:S(2)}, u32[]{:S(2)}) async-start(bf16[4,256,512]{2,1,0:T(8,128)(2,1)} %broadcast_in_dim.11), calls=%async_computation.1 | async-start | bytes 2097152 | tf_op jit(solution)/shard_map/all_to_all | solution.py:171
  50.4 10.7 %all-to-all-done.1 = bf16[4,256,512]{2,1,0:T(8,128)(2,1)S(1)} async-done(((bf16[4,256,512]{2,1,0:T(8,128)(2,1)}), bf16[4,256,512]{2,1,0:T(8,128)(2,1)S(1)}, u32[]{:S(2)}, u32[]{:S(2)}) %all-to-all-start.1) | async-done | bytes 1048608 | tf_op jit(solution)/shard_map/all_to_all | solution.py:171
  61.2 10.5 %all_to_all.35 = bf16[4,256,256]{2,1,0:T(8,128)(2,1)S(1)} all-to-all(bf16[4,256,256]{2,1,0:T(8,128)(2,1)S(1)} %broadcast_in_dim.13), channel_id=1, replica_groups=mesh['z'=16,'x'=4,'c'=2,'tp'=4] {'x'}, dimensions={0} | all-to-all | bytes 1048576 | tf_op jit(solution)/shard_map/all_to_all | solution.py:171
  72.7 4.5 %all-to-all-start = ((bf16[4,256,512]{2,1,0:T(8,128)(2,1)}), bf16[4,256,512]{2,1,0:T(8,128)(2,1)S(1)}, u32[]{:S(2)}, u32[]{:S(2)}) async-start(bf16[4,256,512]{2,1,0:T(8,128)(2,1)} %broadcast_in_dim.10), calls=%async_computation | async-start | bytes 2097152 | tf_op jit(solution)/shard_map/all_to_all | solution.py:171
  80.1 7.9 %all-to-all-done.g_ref = bf16[4,256,512]{2,1,0:T(8,128)(2,1)S(1)} async-done(((bf16[4,256,512]{2,1,0:T(8,128)(2,1)}), bf16[4,256,512]{2,1,0:T(8,128)(2,1)S(1)}, u32[]{:S(2)}, u32[]{:S(2)}) %all-to-all-start) | async-done | bytes 1048608 | tf_op jit(solution)/shard_map/all_to_all | solution.py:171
  89.3 6.5 %all-to-all-start.5 = ((bf16[4,256,768]{2,1,0:T(8,128)(2,1)}), bf16[4,256,768]{2,1,0:T(8,128)(2,1)}, u32[]{:S(2)}, u32[]{:S(2)}) async-start(bf16[4,256,768]{2,1,0:T(8,128)(2,1)} %broadcast_in_dim.14), calls=%async_computation.5 | async-start | bytes 3145728 | tf_op jit(solution)/shard_map/all_to_all | solution.py:171
  97.9 3.6 %collective-permute-start.4 = (s32[64]{0:T(128)S(1)}, s32[64]{0:T(128)S(1)}, u32[]{:S(2)}, u32[]{:S(2)}) collective-permute-start(s32[64]{0:T(128)S(1)} %get-tuple-element.30), channel_id=1, source_target_pairs={{4,0},{8,4},{12,8},{16,12},{20,16},{24,20},{28,24},{32,28},{36,32}... | collective-permute-start | bytes 776 | tf_op jit(solution)/shard_map/ppermute | solution.py:183
  103.8 2.3 %gate.2.mid_ref = bf16[256,256]{1,0:T(8,128)(2,1)S(1)} custom-call(s32[1]{0:T(128)} %bitcast.core_ref, bf16[4,256,512]{2,1,0:T(8,128)(2,1)S(1)} %all-to-all-done.g_ref, f32[4,512]{1,0:T(4,128)S(1)} %squeeze.33.gain_ref, bf16[4,16,16,512]{3,2,1,0:T(8,128)(2,1)S(1)} %bitcast.32, bf16[4,16,16,512]{3,2,1,0:T(8,128)(2,1)} %collective-permute-done.other_ref), custom_call_target="tpu_custom_call" | custom-call | tf_op jit(solution)/shard_map/gate/pallas_call | solution.py:53
  106.1 2.9 %collective-permute-start.2 = (bf16[64,256]{1,0:T(8,128)(2,1)S(1)}, bf16[64,256]{1,0:T(8,128)(2,1)S(1)}, u32[]{:S(2)}, u32[]{:S(2)}) collective-permute-start(bf16[64,256]{1,0:T(8,128)(2,1)S(1)} %get-tuple-element.25), channel_id=1, source_target_pairs={{4,0},{8,4},{12,8},{16,12},{20,16},{24,20},{28,24},{32,28},{36,32}... | collective-permute-start | bytes 98312 | tf_op jit(solution)/shard_map/ppermute | solution.py:183
  111.0 3.2 %collective-permute-done.1.before_ref = bf16[64,256]{1,0:T(8,128)(2,1)S(1)} collective-permute-done((bf16[64,256]{1,0:T(8,128)(2,1)S(1)}, bf16[64,256]{1,0:T(8,128)(2,1)S(1)}, u32[]{:S(2)}, u32[]{:S(2)}) %collective-permute-start.1) | collective-permute-done | bytes 32800 | tf_op jit(solution)/shard_map/ppermute | solution.py:182
  114.3 7.0 %conv.2 = (f32[256,256]{1,0:T(8,128)S(1)}, f32[2,256]{1,0:T(2,128)S(1)}) custom-call(bf16[64,256]{1,0:T(8,128)(2,1)S(1)} %collective-permute-done.1.before_ref, bf16[256,256]{1,0:T(8,128)(2,1)S(1)} %gate.2.mid_ref, bf16[64,256]{1,0:T(8,128)(2,1)S(1)} %collective-permute-done.2.after_ref, s32[384,128]{1,0:T(8,128)S(1)} %broadcast_in_dim.12.seg_ref, ...), custom_call_target="tpu_custom_call" | custom-call | tf_op jit(solution)/shard_map/conv/pallas_call | solution.py:96
  121.3 10.4 %all-gather = f32[4,2,256]{2,1,0:T(2,128)S(1)} all-gather(f32[1,2,256]{2,1,0:T(2,128)S(1)} %bitcast.38), channel_id=1, replica_groups=mesh['z'=16,'x'=4,'c'=2,'tp'=4] {'tp'}, dimensions={0}, use_global_device_ids=true | all-gather | bytes 10240 | tf_op jit(solution)/shard_map/all_gather | solution.py:227
  131.8 3.0 %project.2 = bf16[4,256,512]{2,1,0:T(8,128)(2,1)} custom-call(s32[1]{0:T(128)} %bitcast.core_ref, f32[256,256]{1,0:T(8,128)S(1)} %get-tuple-element.13.conv_ref, f32[8,256]{1,0:T(8,128)S(1)} %reshape.27.stat_ref, f32[1,256]{1,0:T(1,128)S(1)} %get-tuple-element.28.gain_ref, bf16[4,16,16,256]{3,2,1,0:T(8,128)(2,1)S(1)} %bitcast.34, ...), custom_call_target="tpu_custom_call" | custom-call | tf_op jit(solution)/shard_map/project/pallas_call | solution.py:129
  134.8 3.7 %all-to-all-start.3 = ((bf16[4,256,512]{2,1,0:T(8,128)(2,1)}), bf16[4,256,512]{2,1,0:T(8,128)(2,1)S(1)}, u32[]{:S(2)}, u32[]{:S(2)}) async-start(bf16[4,256,512]{2,1,0:T(8,128)(2,1)} %project.2), calls=%async_computation.3 | async-start | bytes 2097152 | tf_op jit(solution)/shard_map/all_to_all | solution.py:171
  140.4 12.2 %all-to-all-done.3.parts_ref = bf16[4,256,512]{2,1,0:T(8,128)(2,1)S(1)} async-done(((bf16[4,256,512]{2,1,0:T(8,128)(2,1)}), bf16[4,256,512]{2,1,0:T(8,128)(2,1)S(1)}, u32[]{:S(2)}, u32[]{:S(2)}) %all-to-all-start.3) | async-done | bytes 1048608 | tf_op jit(solution)/shard_map/all_to_all | solution.py:171
  153.7 3.5 %all-to-all-start.4 = ((bf16[4,256,512]{2,1,0:T(8,128)(2,1)}), bf16[4,256,512]{2,1,0:T(8,128)(2,1)S(1)}, u32[]{:S(2)}, u32[]{:S(2)}) async-start(bf16[4,256,512]{2,1,0:T(8,128)(2,1)} %add_parts.2), calls=%async_computation.4 | async-start | bytes 2097152 | tf_op jit(solution)/shard_map/all_to_all | solution.py:171
  159.9 10.6 %all-to-all-done.4.g_ref = bf16[4,256,512]{2,1,0:T(8,128)(2,1)S(1)} async-done(((bf16[4,256,512]{2,1,0:T(8,128)(2,1)}), bf16[4,256,512]{2,1,0:T(8,128)(2,1)S(1)}, u32[]{:S(2)}, u32[]{:S(2)}) %all-to-all-start.4) | async-done | bytes 1048608 | tf_op jit(solution)/shard_map/all_to_all | solution.py:171
  173.4 2.4 %collective-permute-start.7 = (bf16[64,256]{1,0:T(8,128)(2,1)S(1)}, bf16[64,256]{1,0:T(8,128)(2,1)S(1)}, u32[]{:S(2)}, u32[]{:S(2)}) collective-permute-start(bf16[64,256]{1,0:T(8,128)(2,1)S(1)} %get-tuple-element.24), channel_id=1, source_target_pairs={{0,4},{4,8},{8,12},{12,16},{16,20},{20,24},{24,28},{28,32},{32,36}... | collective-permute-start | bytes 98312 | tf_op jit(solution)/shard_map/ppermute | solution.py:182
  178.7 7.0 %conv.3 = (f32[256,256]{1,0:T(8,128)S(1)}, f32[2,256]{1,0:T(2,128)S(1)}) custom-call(bf16[64,256]{1,0:T(8,128)(2,1)S(1)} %collective-permute-done.7.before_ref, bf16[256,256]{1,0:T(8,128)(2,1)S(1)} %gate.3.mid_ref, bf16[64,256]{1,0:T(8,128)(2,1)S(1)} %collective-permute-done.8.after_ref, s32[384,128]{1,0:T(8,128)S(1)} %broadcast_in_dim.12.seg_ref, ...), custom_call_target="tpu_custom_call" | custom-call | tf_op jit(solution)/shard_map/conv/pallas_call | solution.py:96
  185.7 10.4 %all-gather.1 = f32[4,2,256]{2,1,0:T(2,128)S(1)} all-gather(f32[1,2,256]{2,1,0:T(2,128)S(1)} %bitcast.37), channel_id=1, replica_groups=mesh['z'=16,'x'=4,'c'=2,'tp'=4] {'tp'}, dimensions={0}, use_global_device_ids=true | all-gather | bytes 10240 | tf_op jit(solution)/shard_map/all_gather | solution.py:227
  196.1 2.0 project.3
  198.2 3.7 %all-to-all-start.6 = ((bf16[4,256,512]{2,1,0:T(8,128)(2,1)}), bf16[4,256,512]{2,1,0:T(8,128)(2,1)S(1)}, u32[]{:S(2)}, u32[]{:S(2)}) async-start(bf16[4,256,512]{2,1,0:T(8,128)(2,1)} %project.3), calls=%async_computation.6 | async-start | bytes 2097152 | tf_op jit(solution)/shard_map/all_to_all | solution.py:171
  202.8 11.4 %all-to-all-done.6.parts_ref = bf16[4,256,512]{2,1,0:T(8,128)(2,1)S(1)} async-done(((bf16[4,256,512]{2,1,0:T(8,128)(2,1)}), bf16[4,256,512]{2,1,0:T(8,128)(2,1)S(1)}, u32[]{:S(2)}, u32[]{:S(2)}) %all-to-all-start.6) | async-done | bytes 1048608 | tf_op jit(solution)/shard_map/all_to_all | solution.py:171
  (62 shorter events, 30.2 us)
Async XLA Ops:
  44.3 28.4 %copy-start.1 = (bf16[256,1536]{1,0:T(8,128)(2,1)}, bf16[256,1536]{1,0:T(8,128)(2,1)S(1)}, u32[]{:S(2)}) copy-start(bf16[256,1536]{1,0:T(8,128)(2,1)S(1)} %all_gather.9) | copy-start | bytes 2359300
  45.5 26.2 %copy-start = (bf16[256,512]{1,0:T(8,128)(2,1)S(1)}, bf16[256,512]{1,0:T(8,128)(2,1)}, u32[]{:S(2)}) copy-start(bf16[256,512]{1,0:T(8,128)(2,1)} %stream_ref.1) | copy-start | bytes 786436
  45.5 15.6 %all-to-all-start.1 = ((bf16[4,256,512]{2,1,0:T(8,128)(2,1)}), bf16[4,256,512]{2,1,0:T(8,128)(2,1)S(1)}, u32[]{:S(2)}, u32[]{:S(2)}) async-start(bf16[4,256,512]{2,1,0:T(8,128)(2,1)} %broadcast_in_dim.11), calls=%async_computation.1 | async-start | bytes 2097152 | tf_op jit(solution)/shard_map/all_to_all | solution.py:171
  72.7 15.4 %all-to-all-start = ((bf16[4,256,512]{2,1,0:T(8,128)(2,1)}), bf16[4,256,512]{2,1,0:T(8,128)(2,1)S(1)}, u32[]{:S(2)}, u32[]{:S(2)}) async-start(bf16[4,256,512]{2,1,0:T(8,128)(2,1)} %broadcast_in_dim.10), calls=%async_computation | async-start | bytes 2097152 | tf_op jit(solution)/shard_map/all_to_all | solution.py:171
  77.2 26.6 %collective-permute-start = (bf16[4,16,16,512]{3,2,1,0:T(8,128)(2,1)S(1)}, bf16[4,16,16,512]{3,2,1,0:T(8,128)(2,1)}, u32[]{:S(2)}, u32[]{:S(2)}) collective-permute-start(bf16[4,16,16,512]{3,2,1,0:T(8,128)(2,1)S(1)} %bitcast.31), channel_id=1, source_target_pairs={{0,4},{4,0},{1,5},{5,1},{2,6},{6,2},{3,7},{7,3},{8,12},{12,8},{9,1... | collective-permute-start | bytes 3145736 | tf_op jit(solution)/shard_map/ppermute | solution.py:167
  89.3 6.5 %copy-start.4 = (s32[256]{0:T(256)S(1)}, s32[256]{0:T(256)}, u32[]{:S(2)}) copy-start(s32[256]{0:T(256)} %param.9) | copy-start | bytes 3076
  89.3 12.2 %copy-start.3 = (f32[2,2048]{1,0:T(2,128)S(1)}, f32[2,2048]{1,0:T(2,128)}, u32[]{:S(2)}) copy-start(f32[2,2048]{1,0:T(2,128)} %param.10) | copy-start | bytes 49156
  89.3 12.3 %copy-start.2 = (f32[2,129,256]{2,0,1:T(2,128)S(1)}, f32[2,129,256]{2,0,1:T(2,128)}, u32[]{:S(2)}) copy-start(f32[2,129,256]{2,0,1:T(2,128)} %param.13) | copy-start | bytes 792580
  89.3 14.4 %copy-start.5 = (f32[2,256]{1,0:T(2,128)S(1)}, f32[2,256]{1,0:T(2,128)}, u32[]{:S(2)}) copy-start(f32[2,256]{1,0:T(2,128)} %param.14) | copy-start | bytes 6148
  89.3 45.4 %all-to-all-start.5 = ((bf16[4,256,768]{2,1,0:T(8,128)(2,1)}), bf16[4,256,768]{2,1,0:T(8,128)(2,1)}, u32[]{:S(2)}, u32[]{:S(2)}) async-start(bf16[4,256,768]{2,1,0:T(8,128)(2,1)} %broadcast_in_dim.14), calls=%async_computation.5 | async-start | bytes 3145728 | tf_op jit(solution)/shard_map/all_to_all | solution.py:171
  95.9 14.9 %collective-permute-start.3 = (s32[64]{0:T(128)S(1)}, s32[64]{0:T(128)S(1)}, u32[]{:S(2)}, u32[]{:S(2)}) collective-permute-start(s32[64]{0:T(128)S(1)} %get-tuple-element.29), channel_id=1, source_target_pairs={{0,4},{4,8},{8,12},{12,16},{16,20},{20,24},{24,28},{28,32},{32,36}... | collective-permute-start | bytes 776 | tf_op jit(solution)/shard_map/ppermute | solution.py:182
  97.9 13.0 %collective-permute-start.4 = (s32[64]{0:T(128)S(1)}, s32[64]{0:T(128)S(1)}, u32[]{:S(2)}, u32[]{:S(2)}) collective-permute-start(s32[64]{0:T(128)S(1)} %get-tuple-element.30), channel_id=1, source_target_pairs={{4,0},{8,4},{12,8},{16,12},{20,16},{24,20},{28,24},{32,28},{36,32}... | collective-permute-start | bytes 776 | tf_op jit(solution)/shard_map/ppermute | solution.py:183
  101.8 29.9 %collective-permute-start.5 = (bf16[4,16,16,256]{3,2,1,0:T(8,128)(2,1)S(1)}, bf16[4,16,16,256]{3,2,1,0:T(8,128)(2,1)}, u32[]{:S(2)}, u32[]{:S(2)}) collective-permute-start(bf16[4,16,16,256]{3,2,1,0:T(8,128)(2,1)S(1)} %bitcast.33), channel_id=1, source_target_pairs={{0,4},{4,0},{1,5},{5,1},{2,6},{6,2},{3,7},{7,3},{8,12},{12,8},{9,1... | collective-permute-start | bytes 1572872 | tf_op jit(solution)/shard_map/ppermute | solution.py:167
  106.1 4.9 %collective-permute-start.2 = (bf16[64,256]{1,0:T(8,128)(2,1)S(1)}, bf16[64,256]{1,0:T(8,128)(2,1)S(1)}, u32[]{:S(2)}, u32[]{:S(2)}) collective-permute-start(bf16[64,256]{1,0:T(8,128)(2,1)S(1)} %get-tuple-element.25), channel_id=1, source_target_pairs={{4,0},{8,4},{12,8},{16,12},{20,16},{24,20},{28,24},{32,28},{36,32}... | collective-permute-start | bytes 98312 | tf_op jit(solution)/shard_map/ppermute | solution.py:183
  108.9 5.2 %collective-permute-start.1 = (bf16[64,256]{1,0:T(8,128)(2,1)S(1)}, bf16[64,256]{1,0:T(8,128)(2,1)S(1)}, u32[]{:S(2)}, u32[]{:S(2)}) collective-permute-start(bf16[64,256]{1,0:T(8,128)(2,1)S(1)} %get-tuple-element.26), channel_id=1, source_target_pairs={{0,4},{4,8},{8,12},{12,16},{16,20},{20,24},{24,28},{28,32},{32,36}... | collective-permute-start | bytes 98312 | tf_op jit(solution)/shard_map/ppermute | solution.py:182
  134.8 17.8 %all-to-all-start.3 = ((bf16[4,256,512]{2,1,0:T(8,128)(2,1)}), bf16[4,256,512]{2,1,0:T(8,128)(2,1)S(1)}, u32[]{:S(2)}, u32[]{:S(2)}) async-start(bf16[4,256,512]{2,1,0:T(8,128)(2,1)} %project.2), calls=%async_computation.3 | async-start | bytes 2097152 | tf_op jit(solution)/shard_map/all_to_all | solution.py:171
  138.5 20.1 %collective-permute-start.6 = (bf16[4,16,16,768]{3,2,1,0:T(8,128)(2,1)}, bf16[4,16,16,768]{3,2,1,0:T(8,128)(2,1)}, u32[]{:S(2)}, u32[]{:S(2)}) collective-permute-start(bf16[4,16,16,768]{3,2,1,0:T(8,128)(2,1)} %bitcast.13), channel_id=1, source_target_pairs={{0,4},{4,0},{1,5},{5,1},{2,6},{6,2},{3,7},{7,3},{8,12},{12,8},{9,1... | collective-permute-start | bytes 4718600 | tf_op jit(solution)/shard_map/ppermute | solution.py:167
  153.7 16.7 %all-to-all-start.4 = ((bf16[4,256,512]{2,1,0:T(8,128)(2,1)}), bf16[4,256,512]{2,1,0:T(8,128)(2,1)S(1)}, u32[]{:S(2)}, u32[]{:S(2)}) async-start(bf16[4,256,512]{2,1,0:T(8,128)(2,1)} %add_parts.2), calls=%async_computation.4 | async-start | bytes 2097152 | tf_op jit(solution)/shard_map/all_to_all | solution.py:171
  171.5 6.5 %collective-permute-start.8 = (bf16[64,256]{1,0:T(8,128)(2,1)S(1)}, bf16[64,256]{1,0:T(8,128)(2,1)S(1)}, u32[]{:S(2)}, u32[]{:S(2)}) collective-permute-start(bf16[64,256]{1,0:T(8,128)(2,1)S(1)} %get-tuple-element.23), channel_id=1, source_target_pairs={{4,0},{8,4},{12,8},{16,12},{20,16},{24,20},{28,24},{32,28},{36,32}... | collective-permute-start | bytes 98312 | tf_op jit(solution)/shard_map/ppermute | solution.py:183
  173.4 5.2 %collective-permute-start.7 = (bf16[64,256]{1,0:T(8,128)(2,1)S(1)}, bf16[64,256]{1,0:T(8,128)(2,1)S(1)}, u32[]{:S(2)}, u32[]{:S(2)}) collective-permute-start(bf16[64,256]{1,0:T(8,128)(2,1)S(1)} %get-tuple-element.24), channel_id=1, source_target_pairs={{0,4},{4,8},{8,12},{12,16},{16,20},{20,24},{24,28},{28,32},{32,36}... | collective-permute-start | bytes 98312 | tf_op jit(solution)/shard_map/ppermute | solution.py:182
  198.2 16.1 %all-to-all-start.6 = ((bf16[4,256,512]{2,1,0:T(8,128)(2,1)}), bf16[4,256,512]{2,1,0:T(8,128)(2,1)S(1)}, u32[]{:S(2)}, u32[]{:S(2)}) async-start(bf16[4,256,512]{2,1,0:T(8,128)(2,1)} %project.3), calls=%async_computation.6 | async-start | bytes 2097152 | tf_op jit(solution)/shard_map/all_to_all | solution.py:171

commit v2 on v1

v2 whole, which is shorter than its diff:
```python
import functools

import jax
import jax.numpy as jnp
from jax import lax
from jax.experimental import pallas as pl
from jax.experimental.pallas import tpu as pltpu
from jax.sharding import Mesh
from jax.sharding import PartitionSpec as P


D = 2048
CF = 1024
KW = 129
LAYERS = 2
EPSILON = 0.01
R = (KW - 1) // 2
SP = ("z", "x", "c")
NZ, NX, NC, NT = 16, 4, 2, 4
TOK = 256
CH = 256
FD = 512
LANES = 128
TILE = 64
STEPS = (0, 1, 3, 2)

F32 = jnp.float32
BF16 = jnp.bfloat16
LIMIT = pltpu.CompilerParams(vmem_limit_bytes=16 * 1024 * 1024)
VMEM = pl.BlockSpec(memory_space=pltpu.VMEM)
SMEM = pl.BlockSpec(memory_space=pltpu.SMEM)


def assemble(rotated, at_ref, own_ref, other_ref, cols, scratch):
    core = at_ref[0]
    width = cols.stop - cols.start
    for i in range(NX):
        x = lax.rem(at_ref[2] + (NX - STEPS[i]), NX) if rotated else i
        scratch[:, x, core] = own_ref[i, :, cols].reshape(NZ, 16, width)
        scratch[:, x, 1 - core] = other_ref[i, :, cols].reshape(NZ, 16, width)


def pack_kernel(value_ref, gate_ref, out_ref, packed_ref):
    at = 0
    for layer in range(LAYERS):
        for ref in (value_ref, gate_ref, out_ref):
            packed_ref[:, at : at + CH] = ref[layer]
            at += CH


def pack(value, gate_, out):
    return pl.pallas_call(
        pack_kernel,
        out_shape=jax.ShapeDtypeStruct((16, 6 * CH), BF16),
        in_specs=[VMEM] * 3,
        out_specs=VMEM,
        name="pack",
        compiler_params=LIMIT,
    )(value, gate_, out)


def gate_kernel(layer, at_ref, p0_ref, p1_ref, p2_ref, p3_ref, gain_ref, own_ref, other_ref, out_ref, w_ref):
    assemble(layer > 0, at_ref, own_ref, other_ref, slice(0, 2 * CH), w_ref)
    wide = [ref[...].astype(F32) for ref in (p0_ref, p1_ref, p2_ref, p3_ref)]
    square = sum(jnp.sum(v * v, axis=1, keepdims=True) for v in wide)
    scale = lax.rsqrt(square * (1.0 / D) + EPSILON)
    pre = jnp.zeros((TOK, 2 * CH), F32)
    part = NZ // NT
    for v, step in zip(wide, STEPS):
        y = lax.rem(at_ref[1] + (NT - step), NT)
        gain = gain_ref[layer : layer + 1, pl.ds(pl.multiple_of(y * FD, FD), FD)]
        normed = (v * scale * gain).astype(BF16)
        w = w_ref[pl.ds(y * part, part)].reshape(FD, 2 * CH)
        pre = pre + jnp.dot(normed, w, preferred_element_type=F32)
    out_ref[...] = (pre[:, :CH] * jax.nn.sigmoid(pre[:, CH:])).astype(BF16)


def gate(layer, at, pieces, gain, own, other):
    return pl.pallas_call(
        functools.partial(gate_kernel, layer),
        out_shape=jax.ShapeDtypeStruct((TOK, CH), BF16),
        in_specs=[SMEM] + [VMEM] * 7,
        out_specs=VMEM,
        scratch_shapes=[pltpu.VMEM((NZ, NX, NC, 16, 2 * CH), BF16)],
        name="gate",
        compiler_params=LIMIT,
    )(at, *pieces, gain, own, other)


def conv_kernel(layer, before_ref, mid_ref, after_ref, seg_ref, taps_ref, conv_ref, stat_ref, x_ref):
    for h in range(CH // LANES):
        cols = slice(h * LANES, (h + 1) * LANES)
        x_ref[h, 0:R] = before_ref[:, cols].astype(F32)
        x_ref[h, R : R + TOK] = mid_ref[:, cols].astype(F32)
        x_ref[h, R + TOK : R + TOK + R] = after_ref[:, cols].astype(F32)

    def tile(i, carry):
        first = pl.multiple_of(i * TILE, TILE)
        own = seg_ref[pl.ds(first + R, TILE), :]
        acc = [jnp.zeros((TILE, LANES), F32) for _ in range(CH // LANES)]
        for k in range(KW):
            same = seg_ref[pl.ds(first + k, TILE), :] == own
            for h in range(CH // LANES):
                tap = taps_ref[k, layer : layer + 1, h * LANES : (h + 1) * LANES]
                window = x_ref[h, pl.ds(first + k, TILE), :]
                acc[h] = acc[h] + jnp.where(same, window * tap, 0.0)
        for h in range(CH // LANES):
            conv_ref[pl.ds(first, TILE), h * LANES : (h + 1) * LANES] = acc[h]
        return carry

    lax.fori_loop(0, TOK // TILE, tile, 0)
    conv = conv_ref[...]
    ones = jnp.ones((8, CH), F32)
    dims = (((1,), (1,)), ((), ()))
    total = lax.dot_general(ones, conv, dims, precision=lax.Precision.HIGHEST, preferred_element_type=F32)
    square = lax.dot_general(ones, conv * conv, dims, precision=lax.Precision.HIGHEST, preferred_element_type=F32)
    stat_ref[0:1, :] = total[0:1, :]
    stat_ref[1:2, :] = square[0:1, :]


def convolve(layer, before, mid, after, seg, taps):
    return pl.pallas_call(
        functools.partial(conv_kernel, layer),
        out_shape=(jax.ShapeDtypeStruct((TOK, CH), F32), jax.ShapeDtypeStruct((2, TOK), F32)),
        in_specs=[VMEM] * 5,
        out_specs=(VMEM, VMEM),
        scratch_shapes=[pltpu.VMEM((CH // LANES, TOK + 2 * R, LANES), F32)],
        name="conv",
        compiler_params=LIMIT,
    )(before, mid, after, seg, taps)


def out_kernel(layer, at_ref, conv_ref, stat_ref, gain_ref, own_ref, other_ref, out_ref, w_ref):
    assemble(layer > 0, at_ref, own_ref, other_ref, slice(2 * CH, 3 * CH), w_ref)
    stat = stat_ref[...]
    kind = lax.broadcasted_iota(jnp.int32, (2 * NT, CH), 0) % 2
    dims = (((0,), (0,)), ((), ()))

    def spread(which):
        pick = jnp.where(kind == which, 1.0, 0.0).astype(F32)
        return lax.dot_general(stat, pick, dims, precision=lax.Precision.HIGHEST, preferred_element_type=F32)

    mean = spread(0) * (1.0 / CF)
    var = jnp.maximum(spread(1) * (1.0 / CF) - mean * mean, 0.0)
    v = (conv_ref[...] - mean) * lax.rsqrt(var + EPSILON) * gain_ref[layer : layer + 1, :]
    act = jax.nn.silu(v).astype(BF16)
    step = NZ // NT
    for y in range(NT):
        w = w_ref[y * step : (y + 1) * step].reshape(FD, CH)
        part = lax.dot_general(act, w, (((1,), (1,)), ((), ())), preferred_element_type=F32)
        out_ref[y] = part.astype(BF16)


def project(layer, at, conv, stat, gain, own, other):
    return pl.pallas_call(
        functools.partial(out_kernel, layer),
        out_shape=jax.ShapeDtypeStruct((NT, TOK, FD), BF16),
        in_specs=[SMEM, VMEM, VMEM, VMEM, VMEM, VMEM],
        out_specs=VMEM,
        scratch_shapes=[pltpu.VMEM((NZ, NX, NC, 16, CH), BF16)],
        name="project",
        compiler_params=LIMIT,
    )(at, conv, stat, gain, own, other)


def add_kernel(stream_ref, parts_ref, out_ref):
    total = stream_ref[...].astype(F32) + sum(parts_ref[y].astype(F32) for y in range(NT))
    out_ref[...] = total.astype(BF16)


def add_parts(stream, parts):
    return pl.pallas_call(
        add_kernel,
        out_shape=jax.ShapeDtypeStruct((TOK, FD), BF16),
        in_specs=[VMEM, VMEM],
        out_specs=VMEM,
        name="add_parts",
        compiler_params=LIMIT,
    )(stream, parts)


def copies_of(x, n):
    return jnp.broadcast_to(x[None], (n, *x.shape))


def swap_core(x):
    return lax.ppermute(x, "c", [(0, 1), (1, 0)])


def exchange(x, axis):
    return lax.all_to_all(x, axis, 0, 0, tiled=True)


def ring(x, axis):
    n = lax.axis_size(axis)
    pieces = [x]
    for step in STEPS[1:]:
        pieces.append(lax.ppermute(x, axis, [(i, (i + step) % n) for i in range(n)]))
    return pieces


def neighbours(x):
    n = NZ * NX * NC
    up = [(i, i + 1) for i in range(n - 1)]
    down = [(j, i) for i, j in up]
    before = lax.ppermute(x[x.shape[0] - R :], SP, up)
    after = lax.ppermute(x[:R], SP, down)
    return before, after


def after_(x, *others):
    return lax.optimization_barrier((x, *others))[0]


def program(tokens, segments, in_gain, w_value, w_gate, conv_taps, norm_gain, w_out):
    at = jnp.stack([lax.axis_index(a).astype(jnp.int32) for a in ("c", "tp", "x")])

    out_t = jnp.swapaxes(w_out, 1, 2)
    own = pack(w_value, w_gate, out_t)
    column = lax.all_gather(own, "z", axis=0, tiled=True)
    first = exchange(copies_of(column[:, : 3 * CH], NX), "x")
    tokens_late, segments_late = lax.optimization_barrier((tokens, segments, column))[:2]
    pieces = ring(tokens_late, "tp")
    seg_before, seg_after = neighbours(segments_late)
    first_other = swap_core(first)
    seg_wide = jnp.concatenate([seg_before, segments_late, seg_after])
    seg_lanes = jnp.broadcast_to(seg_wide[:, None], (TOK + 2 * R, LANES))

    stream = tokens
    weights = (first, first_other)
    for layer in range(LAYERS):
        gated = gate(layer, at, pieces, in_gain, *weights)
        before, after = neighbours(gated)
        conv, stat = convolve(layer, before, gated, after, seg_lanes, jnp.swapaxes(conv_taps, 0, 1))
        stats = lax.all_gather(stat, "tp", axis=0, tiled=True)
        parts = project(layer, at, conv, stats, norm_gain, *weights)
        received = exchange(parts, "tp")
        stream = add_parts(stream, received)
        if layer == 0:
            rest = ring(after_(column[:, 3 * CH :], parts), "x")
            pieces = ring(stream, "tp")
            rest = jnp.stack(list(lax.optimization_barrier((*rest, stream))[:NX]))
            weights = (rest, swap_core(rest))
    return stream


def solution(mesh):
    fine = Mesh(mesh.devices.reshape(NZ, NX, NC, NT), ("z", "x", "c", "tp"))
    in_specs = (
        P(SP, "tp"),
        P(SP),
        P(),
        P(None, SP, "tp"),
        P(None, SP, "tp"),
        P(None, None, "tp"),
        P(None, "tp"),
        P(None, "tp", SP),
    )
    out_specs = P(SP, "tp")
    return jax.shard_map(program, mesh=fine, in_specs=in_specs, out_specs=out_specs, check_vma=False)
```

time: 217 us -> 208 us (0.959)
  waiting for transfers between devices: 56.8 us -> 26.2 us
  blocking collectives: 71.5 us -> 93.8 us
  local copies, waits for them, and re-layouts: 15 us -> 6.64 us
  starting transfers between devices: 47.2 us -> 55.2 us
    all_to_all x6 -> x1, waiting for transfers between devices: 52.9 us -> 2.41 us  [exchange(): return lax.all_to_all(x, axis, 0, 0, tiled=True)]
    ppermute x0 -> x9, starting transfers between devices: none -> 33.1 us  [ring(): lax.ppermute(x, axis, [(i, (i + step) % n) for i in range(n)])]
    all_to_all x6 -> x1, starting transfers between devices: 26.8 us -> 3.83 us  [exchange(): return lax.all_to_all(x, axis, 0, 0, tiled=True)]
    all_to_all x1 -> x2, blocking collectives: 10.5 us -> 32.8 us  [exchange(): return lax.all_to_all(x, axis, 0, 0, tiled=True)]
    ppermute x0 -> x9, waiting for transfers between devices: none -> 18.3 us  [ring(): lax.ppermute(x, axis, [(i, (i + step) % n) for i in range(n)])]
    slice x10 -> x1, local copies, waits for them, and re-layouts: 6.05 us -> 0.8 us  [program(): rest = ring(after_(column[:, 3 * CH:], parts), 'x')]
    broadcast_in_dim x4 -> x1, local copies, waits for them, and re-layouts: 3.52 us -> 0.1 us  [copies_of(): return jnp.broadcast_to(x[None], (n, *x.shape))]
    unnamed x21 -> x34, local copies, waits for them, and re-layouts: 3.55 us -> 5.54 us
  transfers between devices with their start and end apart: 15 -> 18, of which waited for: 7 -> 10; matrix products, arithmetic and copies ran while one was open for 4% -> 0% of each run, Pallas kernels for 6% -> 1%
where the time goes in v2:
time: 208 us; the launch traced here: 206 us
  blocking collectives  93.8 us (45%)
  starting transfers between devices  55.2 us (27%)
  waiting for transfers between devices  26.2 us (13%)
  Pallas kernels  23.7 us (11%)
  local copies, waits for them, and re-layouts  6.64 us (3%)
    all_gather x1, blocking collectives, program(): column = lax.all_gather(own, 'z', axis=0, tiled=True)  40.1 us
    ppermute x9, starting transfers between devices, ring(): lax.ppermute(x, axis, [(i, (i + step) % n) for i in range(n)])  33.1 us
    all_to_all x2, blocking collectives, exchange(): return lax.all_to_all(x, axis, 0, 0, tiled=True)  32.8 us
    all_gather x2, blocking collectives, program(): stats = lax.all_gather(stat, 'tp', axis=0, tiled=True)  20.9 us
    ppermute x9, waiting for transfers between devices, ring(): lax.ppermute(x, axis, [(i, (i + step) % n) for i in range(n)])  18.3 us
    pallas_call x2, Pallas kernels, convolve(): pl.pallas_call(functools.partial(conv_kernel, layer), out_shape=(jax.Shap...  15.8 us
    ppermute x3, starting transfers between devices, neighbours(): after = lax.ppermute(x[:R], SP, down)  7.61 us
    ppermute x3, starting transfers between devices, neighbours(): before = lax.ppermute(x[x.shape[0] - R:], SP, up)  6.72 us
  transfers between devices with their start and end apart: 18, of which 10 were waited for; matrix products, arithmetic and copies ran while one was open for 0% of the time, Pallas kernels for 1%

profile of v2, /device:TPU:6, one launch (start us, length us, event | category | flops | bytes accessed | tf_op | source)
XLA Modules:
  0.0 206.2 jit_solution(8575123005382185006)
XLA Ops:
  2.2 40.1 %all_gather.9 = bf16[256,1536]{1,0:T(8,128)(2,1)S(1)} all-gather(bf16[16,1536]{1,0:T(8,128)(2,1)S(1)} %pack.1), channel_id=1, replica_groups=mesh['z'=16,'x'=4,'c'=2,'tp'=4] {'z'}, dimensions={0}, use_global_device_ids=true | all-gather | bytes 835584 | tf_op jit(solution)/shard_map/all_gather | solution.py:220
  43.2 16.3 %all_to_all.15.own_ref = bf16[4,256,768]{2,1,0:T(8,128)(2,1)S(1)} all-to-all(bf16[4,256,768]{2,1,0:T(8,128)(2,1)S(1)} %broadcast_in_dim.4), channel_id=1, replica_groups=mesh['z'=16,'x'=4,'c'=2,'tp'=4] {'x'}, dimensions={0} | all-to-all | bytes 3145728 | tf_op jit(solution)/shard_map/all_to_all | solution.py:191
  61.5 5.1 %collective-permute-start.2 = (bf16[256,512]{1,0:T(8,128)(2,1)S(1)}, bf16[256,512]{1,0:T(8,128)(2,1)}, u32[]{:S(2)}, u32[]{:S(2)}) collective-permute-start(bf16[256,512]{1,0:T(8,128)(2,1)S(1)} %copy-done.5), channel_id=1, source_target_pairs={{0,2},{1,3},{2,0},{3,1},{4,6},{5,7},{6,4},{7,5},{8,10},{9,11},{10,... | collective-permute-start | bytes 786440 | tf_op jit(solution)/shard_map/ppermute | solution.py:198
  66.6 3.0 %collective-permute-start.1 = (bf16[256,512]{1,0:T(8,128)(2,1)S(1)}, bf16[256,512]{1,0:T(8,128)(2,1)}, u32[]{:S(2)}, u32[]{:S(2)}) collective-permute-start(bf16[256,512]{1,0:T(8,128)(2,1)S(1)} %copy-done.5), channel_id=1, source_target_pairs={{0,3},{1,0},{2,1},{3,2},{4,7},{5,4},{6,5},{7,6},{8,11},{9,8},{10,9... | collective-permute-start | bytes 786440 | tf_op jit(solution)/shard_map/ppermute | solution.py:198
  69.6 2.9 %collective-permute-start = (bf16[256,512]{1,0:T(8,128)(2,1)S(1)}, bf16[256,512]{1,0:T(8,128)(2,1)}, u32[]{:S(2)}, u32[]{:S(2)}) collective-permute-start(bf16[256,512]{1,0:T(8,128)(2,1)S(1)} %copy-done.5), channel_id=1, source_target_pairs={{0,1},{1,2},{2,3},{3,0},{4,5},{5,6},{6,7},{7,4},{8,9},{9,10},{10,1... | collective-permute-start | bytes 786440 | tf_op jit(solution)/shard_map/ppermute | solution.py:198
  74.6 3.8 %collective-permute-start.7 = (s32[64]{0:T(128)S(1)}, s32[64]{0:T(128)S(1)}, u32[]{:S(2)}, u32[]{:S(2)}) collective-permute-start(s32[64]{0:T(128)S(1)} %get-tuple-element.34), channel_id=1, source_target_pairs={{4,0},{8,4},{12,8},{16,12},{20,16},{24,20},{28,24},{32,28},{36,32}... | collective-permute-start | bytes 776 | tf_op jit(solution)/shard_map/ppermute | solution.py:207
  85.0 2.4 %collective-permute-start.4 = (bf16[64,256]{1,0:T(8,128)(2,1)S(1)}, bf16[64,256]{1,0:T(8,128)(2,1)S(1)}, u32[]{:S(2)}, u32[]{:S(2)}) collective-permute-start(bf16[64,256]{1,0:T(8,128)(2,1)S(1)} %get-tuple-element.32), channel_id=1, source_target_pairs={{0,4},{4,8},{8,12},{12,16},{16,20},{20,24},{24,28},{28,32},{32,36}... | collective-permute-start | bytes 98312 | tf_op jit(solution)/shard_map/ppermute | solution.py:206
  87.6 2.7 %collective-permute-done.4.before_ref = bf16[64,256]{1,0:T(8,128)(2,1)S(1)} collective-permute-done((bf16[64,256]{1,0:T(8,128)(2,1)S(1)}, bf16[64,256]{1,0:T(8,128)(2,1)S(1)}, u32[]{:S(2)}, u32[]{:S(2)}) %collective-permute-start.4) | collective-permute-done | bytes 32800 | tf_op jit(solution)/shard_map/ppermute | solution.py:206
  90.4 7.9 %conv.2 = (f32[256,256]{1,0:T(8,128)S(1)}, f32[2,256]{1,0:T(2,128)S(1)}) custom-call(bf16[64,256]{1,0:T(8,128)(2,1)S(1)} %collective-permute-done.4.before_ref, bf16[256,256]{1,0:T(8,128)(2,1)S(1)} %gate.2.mid_ref, bf16[64,256]{1,0:T(8,128)(2,1)S(1)} %collective-permute-done.5.after_ref, s32[384,128]{1,0:T(8,128)S(1)} %broadcast_in_dim.5.seg_ref, ...), custom_call_target="tpu_custom_call" | custom-call | tf_op jit(solution)/shard_map/conv/pallas_call | solution.py:122
  99.0 10.4 %all-gather = f32[4,2,256]{2,1,0:T(2,128)S(1)} all-gather(f32[1,2,256]{2,1,0:T(2,128)S(1)} %bitcast.15), channel_id=1, replica_groups=mesh['z'=16,'x'=4,'c'=2,'tp'=4] {'tp'}, dimensions={0}, use_global_device_ids=true | all-gather | bytes 10240 | tf_op jit(solution)/shard_map/all_gather | solution.py:235
  112.0 3.8 %all-to-all-start.1 = ((bf16[4,256,512]{2,1,0:T(8,128)(2,1)}), bf16[4,256,512]{2,1,0:T(8,128)(2,1)S(1)}, u32[]{:S(2)}, u32[]{:S(2)}) async-start(bf16[4,256,512]{2,1,0:T(8,128)(2,1)} %copy-done), calls=%async_computation.1 | async-start | bytes 2097152 | tf_op jit(solution)/shard_map/all_to_all | solution.py:191
  115.8 4.1 %collective-permute-start.13 = (bf16[256,768]{1,0:T(8,128)(2,1)S(1)}, bf16[256,768]{1,0:T(8,128)(2,1)S(1)}, u32[]{:S(2)}, u32[]{:S(2)}) collective-permute-start(bf16[256,768]{1,0:T(8,128)(2,1)S(1)} %copy-done.14), channel_id=1, source_target_pairs={{0,16},{8,24},{16,0},{24,8},{1,17},{9,25},{17,1},{25,9},{2,18},{10... | collective-permute-start | bytes 1179656 | tf_op jit(solution)/shard_map/ppermute | solution.py:198
  121.9 5.1 %collective-permute-start.11 = (bf16[256,768]{1,0:T(8,128)(2,1)S(1)}, bf16[256,768]{1,0:T(8,128)(2,1)S(1)}, u32[]{:S(2)}, u32[]{:S(2)}) collective-permute-start(bf16[256,768]{1,0:T(8,128)(2,1)S(1)} %copy-done.14), channel_id=1, source_target_pairs={{0,8},{8,16},{16,24},{24,0},{1,9},{9,17},{17,25},{25,1},{2,10},{10... | collective-permute-start | bytes 1179656 | tf_op jit(solution)/shard_map/ppermute | solution.py:198
  127.0 2.4 %all-to-all-done.1.parts_ref = bf16[4,256,512]{2,1,0:T(8,128)(2,1)S(1)} async-done(((bf16[4,256,512]{2,1,0:T(8,128)(2,1)}), bf16[4,256,512]{2,1,0:T(8,128)(2,1)S(1)}, u32[]{:S(2)}, u32[]{:S(2)}) %all-to-all-start.1) | async-done | bytes 1048608 | tf_op jit(solution)/shard_map/all_to_all | solution.py:191
  131.2 5.6 %collective-permute-done.12 = bf16[256,768]{1,0:T(8,128)(2,1)S(1)} collective-permute-done((bf16[256,768]{1,0:T(8,128)(2,1)S(1)}, bf16[256,768]{1,0:T(8,128)(2,1)S(1)}, u32[]{:S(2)}, u32[]{:S(2)}) %collective-permute-start.12) | collective-permute-done | bytes 393248 | tf_op jit(solution)/shard_map/ppermute | solution.py:198
  139.1 5.1 %collective-permute-start.10 = (bf16[256,512]{1,0:T(8,128)(2,1)S(1)}, bf16[256,512]{1,0:T(8,128)(2,1)S(1)}, u32[]{:S(2)}, u32[]{:S(2)}) collective-permute-start(bf16[256,512]{1,0:T(8,128)(2,1)S(1)} %add_parts.2.p0_ref.stream_ref), channel_id=1, source_target_pairs={{0,2},{1,3},{2,0},{3,1},{4,6},{5,7},{6,4},{7,5},{8,10},{9,11},{10,... | collective-permute-start | bytes 786440 | tf_op jit(solution)/shard_map/ppermute | solution.py:198
  144.2 3.1 %collective-permute-start.9 = (bf16[256,512]{1,0:T(8,128)(2,1)S(1)}, bf16[256,512]{1,0:T(8,128)(2,1)S(1)}, u32[]{:S(2)}, u32[]{:S(2)}) collective-permute-start(bf16[256,512]{1,0:T(8,128)(2,1)S(1)} %add_parts.2.p0_ref.stream_ref), channel_id=1, source_target_pairs={{0,3},{1,0},{2,1},{3,2},{4,7},{5,4},{6,5},{7,6},{8,11},{9,8},{10,9... | collective-permute-start | bytes 786440 | tf_op jit(solution)/shard_map/ppermute | solution.py:198
  147.3 2.8 %collective-permute-start.8 = (bf16[256,512]{1,0:T(8,128)(2,1)S(1)}, bf16[256,512]{1,0:T(8,128)(2,1)S(1)}, u32[]{:S(2)}, u32[]{:S(2)}) collective-permute-start(bf16[256,512]{1,0:T(8,128)(2,1)S(1)} %add_parts.2.p0_ref.stream_ref), channel_id=1, source_target_pairs={{0,1},{1,2},{2,3},{3,0},{4,5},{5,6},{6,7},{7,4},{8,9},{9,10},{10,1... | collective-permute-start | bytes 786440 | tf_op jit(solution)/shard_map/ppermute | solution.py:198
  151.2 5.9 %collective-permute-done.9.p2_ref = bf16[256,512]{1,0:T(8,128)(2,1)S(1)} collective-permute-done((bf16[256,512]{1,0:T(8,128)(2,1)S(1)}, bf16[256,512]{1,0:T(8,128)(2,1)S(1)}, u32[]{:S(2)}, u32[]{:S(2)}) %collective-permute-start.9) | collective-permute-done | bytes 262176 | tf_op jit(solution)/shard_map/ppermute | solution.py:198
  162.1 2.4 %collective-permute-start.15 = (bf16[64,256]{1,0:T(8,128)(2,1)S(1)}, bf16[64,256]{1,0:T(8,128)(2,1)S(1)}, u32[]{:S(2)}, u32[]{:S(2)}) collective-permute-start(bf16[64,256]{1,0:T(8,128)(2,1)S(1)} %get-tuple-element.30), channel_id=1, source_target_pairs={{0,4},{4,8},{8,12},{12,16},{16,20},{20,24},{24,28},{28,32},{32,36}... | collective-permute-start | bytes 98312 | tf_op jit(solution)/shard_map/ppermute | solution.py:206
  164.5 2.8 %collective-permute-done.15.before_ref = bf16[64,256]{1,0:T(8,128)(2,1)S(1)} collective-permute-done((bf16[64,256]{1,0:T(8,128)(2,1)S(1)}, bf16[64,256]{1,0:T(8,128)(2,1)S(1)}, u32[]{:S(2)}, u32[]{:S(2)}) %collective-permute-start.15) | collective-permute-done | bytes 32800 | tf_op jit(solution)/shard_map/ppermute | solution.py:206
  167.3 7.9 %conv.3 = (f32[256,256]{1,0:T(8,128)S(1)}, f32[2,256]{1,0:T(2,128)S(1)}) custom-call(bf16[64,256]{1,0:T(8,128)(2,1)S(1)} %collective-permute-done.15.before_ref, bf16[256,256]{1,0:T(8,128)(2,1)S(1)} %gate.3.mid_ref, bf16[64,256]{1,0:T(8,128)(2,1)S(1)} %collective-permute-done.16.after_ref, s32[384,128]{1,0:T(8,128)S(1)} %copy-done.2, f32[129,2,256]{2,1,0:T(2,128)S(1)} %bitcast.12), custom_call_target="tpu_custom_call" | custom-call | tf_op jit(solution)/shard_map/conv/pallas_call | solution.py:122
  175.9 10.4 %all-gather.1 = f32[4,2,256]{2,1,0:T(2,128)S(1)} all-gather(f32[1,2,256]{2,1,0:T(2,128)S(1)} %bitcast.14), channel_id=1, replica_groups=mesh['z'=16,'x'=4,'c'=2,'tp'=4] {'tp'}, dimensions={0}, use_global_device_ids=true | all-gather | bytes 10240 | tf_op jit(solution)/shard_map/all_gather | solution.py:235
  188.9 16.5 %all_to_all.16.parts_ref = bf16[4,256,512]{2,1,0:T(8,128)(2,1)S(1)} all-to-all(bf16[4,256,512]{2,1,0:T(8,128)(2,1)S(1)} %project.3), channel_id=1, replica_groups=mesh['z'=16,'x'=4,'c'=2,'tp'=4] {'tp'}, dimensions={0} | all-to-all | bytes 2097152 | tf_op jit(solution)/shard_map/all_to_all | solution.py:191
  (69 shorter events, 33.3 us)
Async XLA Ops:
  43.2 18.3 %copy-start.5 = (bf16[256,512]{1,0:T(8,128)(2,1)S(1)}, bf16[256,512]{1,0:T(8,128)(2,1)}, u32[]{:S(2)}) copy-start(bf16[256,512]{1,0:T(8,128)(2,1)} %stream_ref.1) | copy-start | bytes 786436
  43.2 29.3 %copy-start.15 = (s32[256]{0:T(256)S(1)}, s32[256]{0:T(256)}, u32[]{:S(2)}) copy-start(s32[256]{0:T(256)} %param.9) | copy-start | bytes 3076
  43.2 37.7 %copy-start.9 = (f32[2,2048]{1,0:T(2,128)S(1)}, f32[2,2048]{1,0:T(2,128)}, u32[]{:S(2)}) copy-start(f32[2,2048]{1,0:T(2,128)} %gain_ref.6) | copy-start | bytes 49156
  59.6 21.4 %collective-permute-start.3 = (bf16[4,256,768]{2,1,0:T(8,128)(2,1)S(1)}, bf16[4,256,768]{2,1,0:T(8,128)(2,1)S(1)}, u32[]{:S(2)}, u32[]{:S(2)}) collective-permute-start(bf16[4,256,768]{2,1,0:T(8,128)(2,1)S(1)} %all_to_all.15.own_ref), channel_id=1, source_target_pairs={{0,4},{4,0},{1,5},{5,1},{2,6},{6,2},{3,7},{7,3},{8,12},{12,8},{9,1... | collective-permute-start | bytes 4718600 | tf_op jit(solution)/shard_map/ppermute | solution.py:187
  61.5 13.1 %collective-permute-start.2 = (bf16[256,512]{1,0:T(8,128)(2,1)S(1)}, bf16[256,512]{1,0:T(8,128)(2,1)}, u32[]{:S(2)}, u32[]{:S(2)}) collective-permute-start(bf16[256,512]{1,0:T(8,128)(2,1)S(1)} %copy-done.5), channel_id=1, source_target_pairs={{0,2},{1,3},{2,0},{3,1},{4,6},{5,7},{6,4},{7,5},{8,10},{9,11},{10,... | collective-permute-start | bytes 786440 | tf_op jit(solution)/shard_map/ppermute | solution.py:198
  66.6 13.1 %collective-permute-start.1 = (bf16[256,512]{1,0:T(8,128)(2,1)S(1)}, bf16[256,512]{1,0:T(8,128)(2,1)}, u32[]{:S(2)}, u32[]{:S(2)}) collective-permute-start(bf16[256,512]{1,0:T(8,128)(2,1)S(1)} %copy-done.5), channel_id=1, source_target_pairs={{0,3},{1,0},{2,1},{3,2},{4,7},{5,4},{6,5},{7,6},{8,11},{9,8},{10,9... | collective-permute-start | bytes 786440 | tf_op jit(solution)/shard_map/ppermute | solution.py:198
  69.6 11.4 %collective-permute-start = (bf16[256,512]{1,0:T(8,128)(2,1)S(1)}, bf16[256,512]{1,0:T(8,128)(2,1)}, u32[]{:S(2)}, u32[]{:S(2)}) collective-permute-start(bf16[256,512]{1,0:T(8,128)(2,1)S(1)} %copy-done.5), channel_id=1, source_target_pairs={{0,1},{1,2},{2,3},{3,0},{4,5},{5,6},{6,7},{7,4},{8,9},{9,10},{10,1... | collective-permute-start | bytes 786440 | tf_op jit(solution)/shard_map/ppermute | solution.py:198
  72.5 14.9 %collective-permute-start.6 = (s32[64]{0:T(128)S(1)}, s32[64]{0:T(128)S(1)}, u32[]{:S(2)}, u32[]{:S(2)}) collective-permute-start(s32[64]{0:T(128)S(1)} %get-tuple-element.33), channel_id=1, source_target_pairs={{0,4},{4,8},{8,12},{12,16},{16,20},{20,24},{24,28},{28,32},{32,36}... | collective-permute-start | bytes 776 | tf_op jit(solution)/shard_map/ppermute | solution.py:206
  74.5 34.9 %copy-start.13 = (f32[2,256]{1,0:T(2,128)S(1)}, f32[2,256]{1,0:T(2,128)}, u32[]{:S(2)}) copy-start(f32[2,256]{1,0:T(2,128)} %gain_ref.7) | copy-start | bytes 6148
  74.6 12.9 %collective-permute-start.7 = (s32[64]{0:T(128)S(1)}, s32[64]{0:T(128)S(1)}, u32[]{:S(2)}, u32[]{:S(2)}) collective-permute-start(s32[64]{0:T(128)S(1)} %get-tuple-element.34), channel_id=1, source_target_pairs={{4,0},{8,4},{12,8},{16,12},{20,16},{24,20},{28,24},{32,28},{36,32}... | collective-permute-start | bytes 776 | tf_op jit(solution)/shard_map/ppermute | solution.py:207
  83.1 4.4 %collective-permute-start.5 = (bf16[64,256]{1,0:T(8,128)(2,1)S(1)}, bf16[64,256]{1,0:T(8,128)(2,1)S(1)}, u32[]{:S(2)}, u32[]{:S(2)}) collective-permute-start(bf16[64,256]{1,0:T(8,128)(2,1)S(1)} %get-tuple-element.31), channel_id=1, source_target_pairs={{4,0},{8,4},{12,8},{16,12},{20,16},{24,20},{28,24},{32,28},{36,32}... | collective-permute-start | bytes 98312 | tf_op jit(solution)/shard_map/ppermute | solution.py:207
  85.0 5.2 %collective-permute-start.4 = (bf16[64,256]{1,0:T(8,128)(2,1)S(1)}, bf16[64,256]{1,0:T(8,128)(2,1)S(1)}, u32[]{:S(2)}, u32[]{:S(2)}) collective-permute-start(bf16[64,256]{1,0:T(8,128)(2,1)S(1)} %get-tuple-element.32), channel_id=1, source_target_pairs={{0,4},{4,8},{8,12},{12,16},{16,20},{20,24},{24,28},{28,32},{32,36}... | collective-permute-start | bytes 98312 | tf_op jit(solution)/shard_map/ppermute | solution.py:206
  112.0 17.5 %all-to-all-start.1 = ((bf16[4,256,512]{2,1,0:T(8,128)(2,1)}), bf16[4,256,512]{2,1,0:T(8,128)(2,1)S(1)}, u32[]{:S(2)}, u32[]{:S(2)}) async-start(bf16[4,256,512]{2,1,0:T(8,128)(2,1)} %copy-done), calls=%async_computation.1 | async-start | bytes 2097152 | tf_op jit(solution)/shard_map/all_to_all | solution.py:191
  115.8 15.4 %collective-permute-start.13 = (bf16[256,768]{1,0:T(8,128)(2,1)S(1)}, bf16[256,768]{1,0:T(8,128)(2,1)S(1)}, u32[]{:S(2)}, u32[]{:S(2)}) collective-permute-start(bf16[256,768]{1,0:T(8,128)(2,1)S(1)} %copy-done.14), channel_id=1, source_target_pairs={{0,16},{8,24},{16,0},{24,8},{1,17},{9,25},{17,1},{25,9},{2,18},{10... | collective-permute-start | bytes 1179656 | tf_op jit(solution)/shard_map/ppermute | solution.py:198
  120.0 16.8 %collective-permute-start.12 = (bf16[256,768]{1,0:T(8,128)(2,1)S(1)}, bf16[256,768]{1,0:T(8,128)(2,1)S(1)}, u32[]{:S(2)}, u32[]{:S(2)}) collective-permute-start(bf16[256,768]{1,0:T(8,128)(2,1)S(1)} %copy-done.14), channel_id=1, source_target_pairs={{0,24},{8,0},{16,8},{24,16},{1,25},{9,1},{17,9},{25,17},{2,26},{10... | collective-permute-start | bytes 1179656 | tf_op jit(solution)/shard_map/ppermute | solution.py:198
  121.9 14.9 %collective-permute-start.11 = (bf16[256,768]{1,0:T(8,128)(2,1)S(1)}, bf16[256,768]{1,0:T(8,128)(2,1)S(1)}, u32[]{:S(2)}, u32[]{:S(2)}) collective-permute-start(bf16[256,768]{1,0:T(8,128)(2,1)S(1)} %copy-done.14), channel_id=1, source_target_pairs={{0,8},{8,16},{16,24},{24,0},{1,9},{9,17},{17,25},{25,1},{2,10},{10... | collective-permute-start | bytes 1179656 | tf_op jit(solution)/shard_map/ppermute | solution.py:198
  137.0 30.3 %copy-start.2 = (s32[384,128]{1,0:T(8,128)S(1)}, s32[384,128]{1,0:T(8,128)}, u32[]{:S(2)}) copy-start(s32[384,128]{1,0:T(8,128)} %copy-done.1) | copy-start | bytes 589828
  137.0 30.3 %copy-start.4 = (f32[2,129,256]{2,0,1:T(2,128)S(1)}, f32[2,129,256]{2,0,1:T(2,128)}, u32[]{:S(2)}) copy-start(f32[2,129,256]{2,0,1:T(2,128)} %param.13) | copy-start | bytes 792580
  137.0 21.5 %collective-permute-start.14 = (bf16[4,256,768]{2,1,0:T(8,128)(2,1)S(1)}, bf16[4,256,768]{2,1,0:T(8,128)(2,1)S(1)}, u32[]{:S(2)}, u32[]{:S(2)}) collective-permute-start(bf16[4,256,768]{2,1,0:T(8,128)(2,1)S(1)} %pad_maximum_fusion.own_ref), channel_id=1, source_target_pairs={{0,4},{4,0},{1,5},{5,1},{2,6},{6,2},{3,7},{7,3},{8,12},{12,8},{9,1... | collective-permute-start | bytes 4718600 | tf_op jit(solution)/shard_map/ppermute | solution.py:187
  139.1 12.1 %collective-permute-start.10 = (bf16[256,512]{1,0:T(8,128)(2,1)S(1)}, bf16[256,512]{1,0:T(8,128)(2,1)S(1)}, u32[]{:S(2)}, u32[]{:S(2)}) collective-permute-start(bf16[256,512]{1,0:T(8,128)(2,1)S(1)} %add_parts.2.p0_ref.stream_ref), channel_id=1, source_target_pairs={{0,2},{1,3},{2,0},{3,1},{4,6},{5,7},{6,4},{7,5},{8,10},{9,11},{10,... | collective-permute-start | bytes 786440 | tf_op jit(solution)/shard_map/ppermute | solution.py:198
  144.2 12.9 %collective-permute-start.9 = (bf16[256,512]{1,0:T(8,128)(2,1)S(1)}, bf16[256,512]{1,0:T(8,128)(2,1)S(1)}, u32[]{:S(2)}, u32[]{:S(2)}) collective-permute-start(bf16[256,512]{1,0:T(8,128)(2,1)S(1)} %add_parts.2.p0_ref.stream_ref), channel_id=1, source_target_pairs={{0,3},{1,0},{2,1},{3,2},{4,7},{5,4},{6,5},{7,6},{8,11},{9,8},{10,9... | collective-permute-start | bytes 786440 | tf_op jit(solution)/shard_map/ppermute | solution.py:198
  147.3 11.3 %collective-permute-start.8 = (bf16[256,512]{1,0:T(8,128)(2,1)S(1)}, bf16[256,512]{1,0:T(8,128)(2,1)S(1)}, u32[]{:S(2)}, u32[]{:S(2)}) collective-permute-start(bf16[256,512]{1,0:T(8,128)(2,1)S(1)} %add_parts.2.p0_ref.stream_ref), channel_id=1, source_target_pairs={{0,1},{1,2},{2,3},{3,0},{4,5},{5,6},{6,7},{7,4},{8,9},{9,10},{10,1... | collective-permute-start | bytes 786440 | tf_op jit(solution)/shard_map/ppermute | solution.py:198
  160.1 4.3 %collective-permute-start.16 = (bf16[64,256]{1,0:T(8,128)(2,1)S(1)}, bf16[64,256]{1,0:T(8,128)(2,1)S(1)}, u32[]{:S(2)}, u32[]{:S(2)}) collective-permute-start(bf16[64,256]{1,0:T(8,128)(2,1)S(1)} %get-tuple-element.29), channel_id=1, source_target_pairs={{4,0},{8,4},{12,8},{16,12},{20,16},{24,20},{28,24},{32,28},{36,32}... | collective-permute-start | bytes 98312 | tf_op jit(solution)/shard_map/ppermute | solution.py:207
  162.1 5.2 %collective-permute-start.15 = (bf16[64,256]{1,0:T(8,128)(2,1)S(1)}, bf16[64,256]{1,0:T(8,128)(2,1)S(1)}, u32[]{:S(2)}, u32[]{:S(2)}) collective-permute-start(bf16[64,256]{1,0:T(8,128)(2,1)S(1)} %get-tuple-element.30), channel_id=1, source_target_pairs={{0,4},{4,8},{8,12},{12,16},{16,20},{20,24},{24,28},{28,32},{32,36}... | collective-permute-start | bytes 98312 | tf_op jit(solution)/shard_map/ppermute | solution.py:206
  (10 other events, 42.6 us)

commit v3 on v2

v3 whole, which is shorter than its diff:
```python
import functools

import jax
import jax.numpy as jnp
from jax import lax
from jax.experimental import pallas as pl
from jax.experimental.pallas import tpu as pltpu
from jax.sharding import Mesh
from jax.sharding import PartitionSpec as P


D = 2048
CF = 1024
KW = 129
LAYERS = 2
EPSILON = 0.01
R = (KW - 1) // 2
SP = ("z", "x", "c")
NZ, NX, NC, NT = 16, 4, 2, 4
TOK = 256
CH = 256
FD = 512
LANES = 128
TILE = 64
STEPS = (0, 2, 1, 3)

F32 = jnp.float32
BF16 = jnp.bfloat16
LIMIT = pltpu.CompilerParams(vmem_limit_bytes=16 * 1024 * 1024)
VMEM = pl.BlockSpec(memory_space=pltpu.VMEM)
HBM = pl.BlockSpec(memory_space=pltpu.HBM)
SMEM = pl.BlockSpec(memory_space=pltpu.SMEM)


def assemble(at_ref, own_ref, other_ref, gate_ref, out_ref):
    core = at_ref[0]
    for i in range(NX):
        x = lax.rem(at_ref[2] + (NX - STEPS[i]), NX)
        for part, ref in ((core, own_ref), (1 - core, other_ref)):
            gate_ref[:, x, part] = ref[i, :, : 2 * CH].reshape(NZ, 16, 2 * CH)
            out_ref[:, x, part] = ref[i, :, 2 * CH :].reshape(NZ, 16, CH)


def pack_kernel(value_ref, gate_ref, out_ref, packed_ref, sems):
    copies = []
    for layer in range(LAYERS):
        for i, ref in enumerate((value_ref, gate_ref, out_ref)):
            n = 3 * layer + i
            target = packed_ref.at[:, n * CH : (n + 1) * CH]
            copies.append(pltpu.make_async_copy(ref.at[layer], target, sems.at[n]))
            copies[-1].start()
    for copy in copies:
        copy.wait()


def pack(value, gate_, out):
    return pl.pallas_call(
        pack_kernel,
        out_shape=jax.ShapeDtypeStruct((16, 6 * CH), BF16),
        in_specs=[HBM] * 3,
        out_specs=VMEM,
        scratch_shapes=[pltpu.SemaphoreType.DMA((6,))],
        name="pack",
    )(value, gate_, out)


def split_kernel(column_ref, first_ref, rest_ref):
    first_ref[...] = column_ref[:, : 3 * CH]
    rest_ref[...] = column_ref[:, 3 * CH :]


def split(column):
    return pl.pallas_call(
        split_kernel,
        out_shape=(jax.ShapeDtypeStruct((NZ * 16, 3 * CH), BF16),) * 2,
        in_specs=[VMEM],
        out_specs=(VMEM, VMEM),
        name="split",
        compiler_params=LIMIT,
    )(column)


def gate_kernel(layer, count, at_ref, *refs):
    *piece_refs, gain_ref, own_ref, other_ref, gated_ref, out_ref, w_ref = refs
    if count == 1:
        blocks = [(y, piece_refs[0][y]) for y in range(NT)]
    else:
        blocks = [(lax.rem(at_ref[1] + (NT - s), NT), ref[...]) for s, ref in zip(STEPS, piece_refs)]
    assemble(at_ref, own_ref, other_ref, w_ref, out_ref)
    wide = [block.astype(F32) for _, block in blocks]
    square = sum(jnp.sum(v * v, axis=1, keepdims=True) for v in wide)
    scale = lax.rsqrt(square * (1.0 / D) + EPSILON)
    pre = jnp.zeros((TOK, 2 * CH), F32)
    part = NZ // NT
    for v, (y, _) in zip(wide, blocks):
        start = y * FD if count == 1 else pl.multiple_of(y * FD, FD)
        gain = gain_ref[layer : layer + 1, pl.ds(start, FD)]
        normed = (v * scale * gain).astype(BF16)
        w = w_ref[pl.ds(y * part, part)].reshape(FD, 2 * CH)
        pre = pre + jnp.dot(normed, w, preferred_element_type=F32)
    gated_ref[...] = (pre[:, :CH] * jax.nn.sigmoid(pre[:, CH:])).astype(BF16)


def gate(layer, at, pieces, gain, own, other):
    return pl.pallas_call(
        functools.partial(gate_kernel, layer, len(pieces)),
        out_shape=(
            jax.ShapeDtypeStruct((TOK, CH), BF16),
            jax.ShapeDtypeStruct((NZ, NX, NC, 16, CH), BF16),
        ),
        in_specs=[SMEM] + [VMEM] * (3 + len(pieces)),
        out_specs=(VMEM, VMEM),
        scratch_shapes=[pltpu.VMEM((NZ, NX, NC, 16, 2 * CH), BF16)],
        name="gate",
        compiler_params=LIMIT,
    )(at, *pieces, gain, own, other)


def tap_sums(layer, x_ref, seg_ref, taps_ref, x_first, seg_first):
    own = seg_ref[seg_first + R : seg_first + R + TILE, :]
    acc = [jnp.zeros((TILE, LANES), F32) for _ in range(CH // LANES)]
    for k in range(KW):
        same = seg_ref[seg_first + k : seg_first + k + TILE, :] == own
        for h in range(CH // LANES):
            tap = taps_ref[k, layer : layer + 1, h * LANES : (h + 1) * LANES]
            window = x_ref[h, x_first + k : x_first + k + TILE, :]
            acc[h] = acc[h] + jnp.where(same, window * tap, 0.0)
    return acc


def inner_kernel(layer, mid_ref, seg_ref, taps_ref, conv_ref, x_ref):
    for h in range(CH // LANES):
        x_ref[h] = mid_ref[:, h * LANES : (h + 1) * LANES].astype(F32)
    for first in range(0, TOK - 2 * R, TILE):
        for h, acc in enumerate(tap_sums(layer, x_ref, seg_ref, taps_ref, first, first + R)):
            conv_ref[first : first + TILE, h * LANES : (h + 1) * LANES] = acc


def inner(layer, mid, seg, taps):
    return pl.pallas_call(
        functools.partial(inner_kernel, layer),
        out_shape=jax.ShapeDtypeStruct((TOK - 2 * R, CH), F32),
        in_specs=[VMEM] * 3,
        out_specs=VMEM,
        scratch_shapes=[pltpu.VMEM((CH // LANES, TOK, LANES), F32)],
        name="inner",
        compiler_params=LIMIT,
    )(mid, seg, taps)


def outer_kernel(layer, before_ref, mid_ref, after_ref, seg_ref, taps_ref, inner_ref, conv_ref, stat_ref, x_ref):
    for h in range(CH // LANES):
        cols = slice(h * LANES, (h + 1) * LANES)
        x_ref[h, 0:R] = before_ref[:, cols].astype(F32)
        x_ref[h, R : 3 * R] = mid_ref[: 2 * R, cols].astype(F32)
        x_ref[h, 3 * R : 5 * R] = mid_ref[TOK - 2 * R :, cols].astype(F32)
        x_ref[h, 5 * R :] = after_ref[:, cols].astype(F32)
    conv_ref[R : TOK - R, :] = inner_ref[...]
    for x_first, first in ((0, 0), (3 * R, TOK - R)):
        for h, acc in enumerate(tap_sums(layer, x_ref, seg_ref, taps_ref, x_first, first)):
            conv_ref[first : first + R, h * LANES : (h + 1) * LANES] = acc
    conv = conv_ref[...]
    ones = jnp.ones((8, CH), F32)
    dims = (((1,), (1,)), ((), ()))
    total = lax.dot_general(ones, conv, dims, precision=lax.Precision.HIGHEST, preferred_element_type=F32)
    square = lax.dot_general(ones, conv * conv, dims, precision=lax.Precision.HIGHEST, preferred_element_type=F32)
    for y in range(NT):
        stat_ref[y, 0:1, :] = total[0:1, :]
        stat_ref[y, 1:2, :] = square[0:1, :]


def outer(layer, before, mid, after, seg, taps, inside):
    return pl.pallas_call(
        functools.partial(outer_kernel, layer),
        out_shape=(jax.ShapeDtypeStruct((TOK, CH), F32), jax.ShapeDtypeStruct((NT, 2, TOK), F32)),
        in_specs=[VMEM] * 6,
        out_specs=(VMEM, VMEM),
        scratch_shapes=[pltpu.VMEM((CH // LANES, 6 * R, LANES), F32)],
        name="outer",
        compiler_params=LIMIT,
    )(before, mid, after, seg, taps, inside)


def out_kernel(layer, conv_ref, stat_ref, gain_ref, w_ref, parts_ref):
    stat = stat_ref[...]
    kind = lax.broadcasted_iota(jnp.int32, (2 * NT, CH), 0) % 2
    dims = (((0,), (0,)), ((), ()))

    def spread(which):
        pick = jnp.where(kind == which, 1.0, 0.0).astype(F32)
        return lax.dot_general(stat, pick, dims, precision=lax.Precision.HIGHEST, preferred_element_type=F32)

    mean = spread(0) * (1.0 / CF)
    var = jnp.maximum(spread(1) * (1.0 / CF) - mean * mean, 0.0)
    v = (conv_ref[...] - mean) * lax.rsqrt(var + EPSILON) * gain_ref[layer : layer + 1, :]
    act = jax.nn.silu(v).astype(BF16)
    rows = NZ // NT
    for y in range(NT):
        w = w_ref[y * rows : (y + 1) * rows].reshape(FD, CH)
        part = lax.dot_general(act, w, (((1,), (1,)), ((), ())), preferred_element_type=F32)
        parts_ref[y] = part.astype(BF16)


def project(layer, conv, stat, gain, weight):
    return pl.pallas_call(
        functools.partial(out_kernel, layer),
        out_shape=jax.ShapeDtypeStruct((NT, TOK, FD), BF16),
        in_specs=[VMEM] * 4,
        out_specs=VMEM,
        name="project",
        compiler_params=LIMIT,
    )(conv, stat, gain, weight)


def add_kernel(stream_ref, parts_ref, out_ref):
    total = stream_ref[...].astype(F32) + sum(parts_ref[y].astype(F32) for y in range(NT))
    out_ref[...] = total.astype(BF16)


def add_parts(stream, parts):
    return pl.pallas_call(
        add_kernel,
        out_shape=jax.ShapeDtypeStruct((TOK, FD), BF16),
        in_specs=[VMEM, VMEM],
        out_specs=VMEM,
        name="add_parts",
        compiler_params=LIMIT,
    )(stream, parts)


def copies_of(x, n):
    return jnp.broadcast_to(x[None], (n, *x.shape))


def swap_core(x):
    return lax.ppermute(x, "c", [(0, 1), (1, 0)])


def exchange(x, axis):
    return lax.all_to_all(x, axis, 0, 0, tiled=True)


def ring(pieces, axis):
    n = lax.axis_size(axis)
    came = [pieces[0]]
    for piece, step in zip(pieces[1:], STEPS[1:]):
        came.append(lax.ppermute(piece, axis, [(i, (i + step) % n) for i in range(n)]))
    return came


def neighbours(up, down):
    n = NZ * NX * NC
    ups = [(i, i + 1) for i in range(n - 1)]
    before = lax.ppermute(up, SP, ups)
    after = lax.ppermute(down, SP, [(j, i) for i, j in ups])
    return before, after


def after_(x, *others):
    return lax.optimization_barrier((x, *others))[0]


def program(tokens, segments, in_gain, w_value, w_gate, conv_taps, norm_gain, w_out):
    at = jnp.stack([lax.axis_index(a).astype(jnp.int32) for a in ("c", "tp", "x")])

    out_t = jnp.swapaxes(w_out, 1, 2)
    own = pack(w_value, w_gate, out_t)
    column = lax.all_gather(own, "z", axis=0, tiled=True)
    first_own, rest_own = split(column)
    first = ring([first_own] * NX, "x")
    tokens_late, segments_late = lax.optimization_barrier((tokens, segments, column))[:2]
    pieces = (exchange(copies_of(tokens_late, NT), "tp"),)
    seg_before, seg_after = neighbours(segments_late, segments_late)
    first = jnp.stack(first)
    first_other = swap_core(first)
    seg_wide = jnp.concatenate([seg_before[TOK - R :], segments, seg_after[:R]])
    seg_lanes = jnp.broadcast_to(seg_wide[:, None], (TOK + 2 * R, LANES))
    taps = jnp.swapaxes(conv_taps, 0, 1)

    stream = tokens
    weights = (first, first_other)
    for layer in range(LAYERS):
        gated, out_weight = gate(layer, at, pieces, in_gain, *weights)
        before, after = neighbours(gated[TOK - R :], gated[:R])
        inside = inner(layer, gated, seg_lanes, taps)
        conv, stat = outer(layer, before, gated, after, seg_lanes, taps, inside)
        stats = exchange(stat, "tp").reshape(2 * NT, TOK)
        parts = project(layer, conv, stats, norm_gain, out_weight)
        received = exchange(parts, "tp")
        stream = add_parts(stream, received)
        if layer == 0:
            rest = ring([after_(rest_own, parts)] * NX, "x")
            pieces = ring([stream] * NT, "tp")
            rest = jnp.stack(list(lax.optimization_barrier((*rest, stream))[:NX]))
            weights = (rest, swap_core(rest))
    return stream


def solution(mesh):
    fine = Mesh(mesh.devices.reshape(NZ, NX, NC, NT), ("z", "x", "c", "tp"))
    in_specs = (
        P(SP, "tp"),
        P(SP),
        P(),
        P(None, SP, "tp"),
        P(None, SP, "tp"),
        P(None, None, "tp"),
        P(None, "tp"),
        P(None, "tp", SP),
    )
    out_specs = P(SP, "tp")
    return jax.shard_map(
        program, mesh=fine, in_specs=in_specs, out_specs=out_specs, check_vma=False
    )
```

time: 208 us -> 202 us (0.971)
  blocking collectives: 93.8 us -> 74.6 us
  waiting for transfers between devices: 26.2 us -> 44 us
  Pallas kernels: 23.7 us -> 20.1 us
  local copies, waits for them, and re-layouts: 6.64 us -> 4.09 us
    all_gather x2 -> x0, blocking collectives: 20.9 us -> none  [program(): stats = lax.all_gather(stat, 'tp', axis=0, tiled=True)]
    all_to_all x1 -> x2, waiting for transfers between devices: 2.41 us -> 15.4 us  [exchange(): return lax.all_to_all(x, axis, 0, 0, tiled=True)]
    pallas_call x4 -> x7, Pallas kernels: 19.5 us -> 14.6 us  [the longest x2 6.08 us: outer(): pl.pallas_call(functools.partial(outer_kernel, layer), out_shape=(jax.Sha...]
    ppermute x15, waiting for transfers between devices: 23.8 us -> 28.6 us  [the longest x9 28.1 us: ring(): lax.ppermute(piece, axis, [(i, (i + step) % n) for i in range(n)])]
    all_to_all x1 -> x2, starting transfers between devices: 3.83 us -> 7.98 us  [exchange(): return lax.all_to_all(x, axis, 0, 0, tiled=True)]
    unnamed x34 -> x20, local copies, waits for them, and re-layouts: 5.54 us -> 1.72 us
    ppermute x15, starting transfers between devices: 47.4 us -> 44.5 us  [the longest x9 27.6 us: ring(): lax.ppermute(piece, axis, [(i, (i + step) % n) for i in range(n)])]
    all_to_all x2 -> x3, blocking collectives: 32.8 us -> 34.2 us  [exchange(): return lax.all_to_all(x, axis, 0, 0, tiled=True)]
  transfers between devices with their start and end apart: 18 -> 19, of which waited for: 10 -> 12; matrix products, arithmetic and copies ran while one was open for 0% -> 1% of each run, Pallas kernels for 1% -> 2%
where the time goes in v3:
time: 202 us; the launch traced here: 201 us
  blocking collectives  74.6 us (37%)
  starting transfers between devices  56.5 us (28%)
  waiting for transfers between devices  44 us (22%)
  Pallas kernels  20.1 us (10%)
  local copies, waits for them, and re-layouts  4.09 us (2%)
    all_gather x1, blocking collectives, program(): column = lax.all_gather(own, 'z', axis=0, tiled=True)  40.4 us
    all_to_all x3, blocking collectives, exchange(): return lax.all_to_all(x, axis, 0, 0, tiled=True)  34.2 us
    ppermute x9, waiting for transfers between devices, ring(): lax.ppermute(piece, axis, [(i, (i + step) % n) for i in range(n)])  28.1 us
    ppermute x9, starting transfers between devices, ring(): lax.ppermute(piece, axis, [(i, (i + step) % n) for i in range(n)])  27.6 us
    all_to_all x2, waiting for transfers between devices, exchange(): return lax.all_to_all(x, axis, 0, 0, tiled=True)  15.4 us
    ppermute x3, starting transfers between devices, neighbours(): after = lax.ppermute(down, SP, [(j, i) for i, j in ups])  10.9 us
    all_to_all x2, starting transfers between devices, exchange(): return lax.all_to_all(x, axis, 0, 0, tiled=True)  7.98 us
    ppermute x3, starting transfers between devices, neighbours(): before = lax.ppermute(up, SP, ups)  6.09 us
  transfers between devices with their start and end apart: 19, of which 12 were waited for; matrix products, arithmetic and copies ran while one was open for 1% of the time, Pallas kernels for 2%

profile of v3, /device:TPU:6, one launch (start us, length us, event | category | flops | bytes accessed | tf_op | source)
XLA Modules:
  0.0 201.2 jit_solution(391228491034752625)
XLA Ops:
  1.5 40.4 %all_gather.3.column_ref = bf16[256,1536]{1,0:T(8,128)(2,1)S(1)} all-gather(bf16[16,1536]{1,0:T(8,128)(2,1)} %pack.1), channel_id=1, replica_groups=mesh['z'=16,'x'=4,'c'=2,'tp'=4] {'z'}, dimensions={0}, use_global_device_ids=true | all-gather | bytes 835584 | tf_op jit(solution)/shard_map/all_gather | solution.py:268
  41.9 3.3 %collective-permute-start = (bf16[256,768]{1,0:T(8,128)(2,1)S(1)}, bf16[256,768]{1,0:T(8,128)(2,1)S(1)}, u32[]{:S(2)}, u32[]{:S(2)}) collective-permute-start(bf16[256,768]{1,0:T(8,128)(2,1)S(1)} %get-tuple-element.23), channel_id=1, source_target_pairs={{0,16},{8,24},{16,0},{24,8},{1,17},{9,25},{17,1},{25,9},{2,18},{10... | collective-permute-start | bytes 1179656 | tf_op jit(solution)/shard_map/ppermute | solution.py:247
  45.3 4.0 %collective-permute-start.1 = (bf16[256,768]{1,0:T(8,128)(2,1)S(1)}, bf16[256,768]{1,0:T(8,128)(2,1)S(1)}, u32[]{:S(2)}, u32[]{:S(2)}) collective-permute-start(bf16[256,768]{1,0:T(8,128)(2,1)S(1)} %get-tuple-element.23), channel_id=1, source_target_pairs={{0,8},{8,16},{16,24},{24,0},{1,9},{9,17},{17,25},{25,1},{2,10},{10... | collective-permute-start | bytes 1179656 | tf_op jit(solution)/shard_map/ppermute | solution.py:247
  51.2 3.3 %collective-permute-done = bf16[256,768]{1,0:T(8,128)(2,1)S(1)} collective-permute-done((bf16[256,768]{1,0:T(8,128)(2,1)S(1)}, bf16[256,768]{1,0:T(8,128)(2,1)S(1)}, u32[]{:S(2)}, u32[]{:S(2)}) %collective-permute-start) | collective-permute-done | bytes 393248 | tf_op jit(solution)/shard_map/ppermute | solution.py:247
  55.4 4.7 %collective-permute-done.2 = bf16[256,768]{1,0:T(8,128)(2,1)S(1)} collective-permute-done((bf16[256,768]{1,0:T(8,128)(2,1)S(1)}, bf16[256,768]{1,0:T(8,128)(2,1)S(1)}, u32[]{:S(2)}, u32[]{:S(2)}) %collective-permute-start.2) | collective-permute-done | bytes 393248 | tf_op jit(solution)/shard_map/ppermute | solution.py:247
  63.4 4.5 %all-to-all-start = ((bf16[4,256,512]{2,1,0:T(8,128)(2,1)}), bf16[4,256,512]{2,1,0:T(8,128)(2,1)S(1)}, u32[]{:S(2)}, u32[]{:S(2)}) async-start(bf16[4,256,512]{2,1,0:T(8,128)(2,1)} %broadcast_in_dim.4), calls=%async_computation | async-start | bytes 2097152 | tf_op jit(solution)/shard_map/all_to_all | solution.py:240
  70.0 3.4 %collective-permute-start.7 = (s32[256]{0:T(256)S(1)}, s32[256]{0:T(256)S(1)}, u32[]{:S(2)}, u32[]{:S(2)}) collective-permute-start(s32[256]{0:T(256)S(1)} %copy-done.7), channel_id=1, source_target_pairs={{4,0},{8,4},{12,8},{16,12},{20,16},{24,20},{28,24},{32,28},{36,32}... | collective-permute-start | bytes 3080 | tf_op jit(solution)/shard_map/ppermute | solution.py:255
  75.2 8.4 %all-to-all-done.refs_0_ = bf16[4,256,512]{2,1,0:T(8,128)(2,1)S(1)} async-done(((bf16[4,256,512]{2,1,0:T(8,128)(2,1)}), bf16[4,256,512]{2,1,0:T(8,128)(2,1)S(1)}, u32[]{:S(2)}, u32[]{:S(2)}) %all-to-all-start) | async-done | bytes 1048608 | tf_op jit(solution)/shard_map/all_to_all | solution.py:240
  89.9 3.6 %collective-permute-start.5 = (bf16[64,256]{1,0:T(8,128)(2,1)S(1)}, bf16[64,256]{1,0:T(8,128)(2,1)S(1)}, u32[]{:S(2)}, u32[]{:S(2)}) collective-permute-start(bf16[64,256]{1,0:T(8,128)(2,1)S(1)} %get-tuple-element.41), channel_id=1, source_target_pairs={{4,0},{8,4},{12,8},{16,12},{20,16},{24,20},{28,24},{32,28},{36,32}... | collective-permute-start | bytes 98312 | tf_op jit(solution)/shard_map/ppermute | solution.py:255
  96.0 3.0 %outer.2 = (f32[256,256]{1,0:T(8,128)S(1)}, f32[4,2,256]{2,1,0:T(2,128)S(1)}) custom-call(bf16[64,256]{1,0:T(8,128)(2,1)S(1)} %collective-permute-done.4.before_ref, bf16[256,256]{1,0:T(8,128)(2,1)S(1)} %get-tuple-element.24.mid_ref, bf16[64,256]{1,0:T(8,128)(2,1)S(1)} %collective-permute-done.5.after_ref, s32[384,128]{1,0:T(8,128)S(1)} %broadcast_in_dim.5.seg_ref, ...), custom_call_target="tpu_custom_call" | custom-call | tf_op jit(solution)/shard_map/outer/pallas_call | solution.py:173
  99.0 7.7 %all_to_all.25 = f32[4,2,256]{2,1,0:T(2,128)S(1)} all-to-all(f32[4,2,256]{2,1,0:T(2,128)S(1)} %get-tuple-element.27), channel_id=1, replica_groups=mesh['z'=16,'x'=4,'c'=2,'tp'=4] {'tp'}, dimensions={0} | all-to-all | bytes 16384 | tf_op jit(solution)/shard_map/all_to_all | solution.py:240
  108.7 3.5 %all-to-all-start.2 = ((bf16[4,256,512]{2,1,0:T(8,128)(2,1)}), bf16[4,256,512]{2,1,0:T(8,128)(2,1)S(1)}, u32[]{:S(2)}, u32[]{:S(2)}) async-start(bf16[4,256,512]{2,1,0:T(8,128)(2,1)} %project.2), calls=%async_computation.2 | async-start | bytes 2097152 | tf_op jit(solution)/shard_map/all_to_all | solution.py:240
  114.4 3.1 %collective-permute-start.12 = (bf16[256,768]{1,0:T(8,128)(2,1)S(1)}, bf16[256,768]{1,0:T(8,128)(2,1)S(1)}, u32[]{:S(2)}, u32[]{:S(2)}) collective-permute-start(bf16[256,768]{1,0:T(8,128)(2,1)S(1)} %get-tuple-element.31), channel_id=1, source_target_pairs={{0,8},{8,16},{16,24},{24,0},{1,9},{9,17},{17,25},{25,1},{2,10},{10... | collective-permute-start | bytes 1179656 | tf_op jit(solution)/shard_map/ppermute | solution.py:247
  120.2 7.0 %all-to-all-done.2.parts_ref = bf16[4,256,512]{2,1,0:T(8,128)(2,1)S(1)} async-done(((bf16[4,256,512]{2,1,0:T(8,128)(2,1)}), bf16[4,256,512]{2,1,0:T(8,128)(2,1)S(1)}, u32[]{:S(2)}, u32[]{:S(2)}) %all-to-all-start.2) | async-done | bytes 1048608 | tf_op jit(solution)/shard_map/all_to_all | solution.py:240
  127.6 3.1 %collective-permute-done.12 = bf16[256,768]{1,0:T(8,128)(2,1)S(1)} collective-permute-done((bf16[256,768]{1,0:T(8,128)(2,1)S(1)}, bf16[256,768]{1,0:T(8,128)(2,1)S(1)}, u32[]{:S(2)}, u32[]{:S(2)}) %collective-permute-start.12) | collective-permute-done | bytes 393248 | tf_op jit(solution)/shard_map/ppermute | solution.py:247
  130.7 4.0 %collective-permute-done.13 = bf16[256,768]{1,0:T(8,128)(2,1)} collective-permute-done((bf16[256,768]{1,0:T(8,128)(2,1)S(1)}, bf16[256,768]{1,0:T(8,128)(2,1)}, u32[]{:S(2)}, u32[]{:S(2)}) %collective-permute-start.13) | collective-permute-done | bytes 393248 | tf_op jit(solution)/shard_map/ppermute | solution.py:247
  137.9 4.8 %collective-permute-start.10 = (bf16[256,512]{1,0:T(8,128)(2,1)S(1)}, bf16[256,512]{1,0:T(8,128)(2,1)S(1)}, u32[]{:S(2)}, u32[]{:S(2)}) collective-permute-start(bf16[256,512]{1,0:T(8,128)(2,1)S(1)} %add_parts.2.refs_0_.stream_ref), channel_id=1, source_target_pairs={{0,3},{1,0},{2,1},{3,2},{4,7},{5,4},{6,5},{7,6},{8,11},{9,8},{10,9... | collective-permute-start | bytes 786440 | tf_op jit(solution)/shard_map/ppermute | solution.py:247
  145.5 2.8 %collective-permute-start.9 = (bf16[256,512]{1,0:T(8,128)(2,1)S(1)}, bf16[256,512]{1,0:T(8,128)(2,1)S(1)}, u32[]{:S(2)}, u32[]{:S(2)}) collective-permute-start(bf16[256,512]{1,0:T(8,128)(2,1)S(1)} %add_parts.2.refs_0_.stream_ref), channel_id=1, source_target_pairs={{0,1},{1,2},{2,3},{3,0},{4,5},{5,6},{6,7},{7,4},{8,9},{9,10},{10,1... | collective-permute-start | bytes 786440 | tf_op jit(solution)/shard_map/ppermute | solution.py:247
  148.2 6.2 %collective-permute-done.10.refs_3_ = bf16[256,512]{1,0:T(8,128)(2,1)S(1)} collective-permute-done((bf16[256,512]{1,0:T(8,128)(2,1)S(1)}, bf16[256,512]{1,0:T(8,128)(2,1)S(1)}, u32[]{:S(2)}, u32[]{:S(2)}) %collective-permute-start.10) | collective-permute-done | bytes 262176 | tf_op jit(solution)/shard_map/ppermute | solution.py:247
  155.3 4.8 %collective-permute-done.9.refs_2_ = bf16[256,512]{1,0:T(8,128)(2,1)S(1)} collective-permute-done((bf16[256,512]{1,0:T(8,128)(2,1)S(1)}, bf16[256,512]{1,0:T(8,128)(2,1)S(1)}, u32[]{:S(2)}, u32[]{:S(2)}) %collective-permute-start.9) | collective-permute-done | bytes 262176 | tf_op jit(solution)/shard_map/ppermute | solution.py:247
  163.7 3.8 %collective-permute-start.16 = (bf16[64,256]{1,0:T(8,128)(2,1)S(1)}, bf16[64,256]{1,0:T(8,128)(2,1)S(1)}, u32[]{:S(2)}, u32[]{:S(2)}) collective-permute-start(bf16[64,256]{1,0:T(8,128)(2,1)S(1)} %get-tuple-element.39), channel_id=1, source_target_pairs={{4,0},{8,4},{12,8},{16,12},{20,16},{24,20},{28,24},{32,28},{36,32}... | collective-permute-start | bytes 98312 | tf_op jit(solution)/shard_map/ppermute | solution.py:255
  169.7 3.0 %outer.3 = (f32[256,256]{1,0:T(8,128)S(1)}, f32[4,2,256]{2,1,0:T(2,128)S(1)}) custom-call(bf16[64,256]{1,0:T(8,128)(2,1)S(1)} %collective-permute-done.15.before_ref, bf16[256,256]{1,0:T(8,128)(2,1)S(1)} %get-tuple-element.35.mid_ref, bf16[64,256]{1,0:T(8,128)(2,1)S(1)} %collective-permute-done.16.after_ref, s32[384,128]{1,0:T(8,128)S(1)} %broadcast_in_dim.5.seg_ref, ...), custom_call_target="tpu_custom_call" | custom-call | tf_op jit(solution)/shard_map/outer/pallas_call | solution.py:173
  172.7 7.7 %all_to_all.26 = f32[4,2,256]{2,1,0:T(2,128)S(1)} all-to-all(f32[4,2,256]{2,1,0:T(2,128)S(1)} %get-tuple-element.37), channel_id=1, replica_groups=mesh['z'=16,'x'=4,'c'=2,'tp'=4] {'tp'}, dimensions={0} | all-to-all | bytes 16384 | tf_op jit(solution)/shard_map/all_to_all | solution.py:240
  181.4 18.8 %all_to_all.27.parts_ref = bf16[4,256,512]{2,1,0:T(8,128)(2,1)S(1)} all-to-all(bf16[4,256,512]{2,1,0:T(8,128)(2,1)S(1)} %project.3), channel_id=1, replica_groups=mesh['z'=16,'x'=4,'c'=2,'tp'=4] {'tp'}, dimensions={0} | all-to-all | bytes 2097152 | tf_op jit(solution)/shard_map/all_to_all | solution.py:240
  (62 shorter events, 41.8 us)
Async XLA Ops:
  41.9 12.6 %collective-permute-start = (bf16[256,768]{1,0:T(8,128)(2,1)S(1)}, bf16[256,768]{1,0:T(8,128)(2,1)S(1)}, u32[]{:S(2)}, u32[]{:S(2)}) collective-permute-start(bf16[256,768]{1,0:T(8,128)(2,1)S(1)} %get-tuple-element.23), channel_id=1, source_target_pairs={{0,16},{8,24},{16,0},{24,8},{1,17},{9,25},{17,1},{25,9},{2,18},{10... | collective-permute-start | bytes 1179656 | tf_op jit(solution)/shard_map/ppermute | solution.py:247
  45.3 10.1 %collective-permute-start.1 = (bf16[256,768]{1,0:T(8,128)(2,1)S(1)}, bf16[256,768]{1,0:T(8,128)(2,1)S(1)}, u32[]{:S(2)}, u32[]{:S(2)}) collective-permute-start(bf16[256,768]{1,0:T(8,128)(2,1)S(1)} %get-tuple-element.23), channel_id=1, source_target_pairs={{0,8},{8,16},{16,24},{24,0},{1,9},{9,17},{17,25},{25,1},{2,10},{10... | collective-permute-start | bytes 1179656 | tf_op jit(solution)/shard_map/ppermute | solution.py:247
  49.3 10.9 %collective-permute-start.2 = (bf16[256,768]{1,0:T(8,128)(2,1)S(1)}, bf16[256,768]{1,0:T(8,128)(2,1)S(1)}, u32[]{:S(2)}, u32[]{:S(2)}) collective-permute-start(bf16[256,768]{1,0:T(8,128)(2,1)S(1)} %get-tuple-element.23), channel_id=1, source_target_pairs={{0,24},{8,0},{16,8},{24,16},{1,25},{9,1},{17,9},{25,17},{2,26},{10... | collective-permute-start | bytes 1179656 | tf_op jit(solution)/shard_map/ppermute | solution.py:247
  60.4 23.2 %collective-permute-start.3 = (bf16[4,256,768]{2,1,0:T(8,128)(2,1)S(1)}, bf16[4,256,768]{2,1,0:T(8,128)(2,1)}, u32[]{:S(2)}, u32[]{:S(2)}) collective-permute-start(bf16[4,256,768]{2,1,0:T(8,128)(2,1)S(1)} %pad_maximum_fusion.refs_2_), channel_id=1, source_target_pairs={{0,4},{4,0},{1,5},{5,1},{2,6},{6,2},{3,7},{7,3},{8,12},{12,8},{9,1... | collective-permute-start | bytes 4718600 | tf_op jit(solution)/shard_map/ppermute | solution.py:236
  63.4 20.2 %all-to-all-start = ((bf16[4,256,512]{2,1,0:T(8,128)(2,1)}), bf16[4,256,512]{2,1,0:T(8,128)(2,1)S(1)}, u32[]{:S(2)}, u32[]{:S(2)}) async-start(bf16[4,256,512]{2,1,0:T(8,128)(2,1)} %broadcast_in_dim.4), calls=%async_computation | async-start | bytes 2097152 | tf_op jit(solution)/shard_map/all_to_all | solution.py:240
  67.8 5.7 %collective-permute-start.6 = (s32[256]{0:T(256)S(1)}, s32[256]{0:T(256)S(1)}, u32[]{:S(2)}, u32[]{:S(2)}) collective-permute-start(s32[256]{0:T(256)S(1)} %copy-done.7), channel_id=1, source_target_pairs={{0,4},{4,8},{8,12},{12,16},{16,20},{20,24},{24,28},{28,32},{32,36}... | collective-permute-start | bytes 3080 | tf_op jit(solution)/shard_map/ppermute | solution.py:254
  70.0 4.7 %collective-permute-start.7 = (s32[256]{0:T(256)S(1)}, s32[256]{0:T(256)S(1)}, u32[]{:S(2)}, u32[]{:S(2)}) collective-permute-start(s32[256]{0:T(256)S(1)} %copy-done.7), channel_id=1, source_target_pairs={{4,0},{8,4},{12,8},{16,12},{20,16},{24,20},{28,24},{32,28},{36,32}... | collective-permute-start | bytes 3080 | tf_op jit(solution)/shard_map/ppermute | solution.py:255
  75.2 18.6 %copy-start = (f32[2,129,256]{2,0,1:T(2,128)S(1)}, f32[2,129,256]{2,0,1:T(2,128)}, u32[]{:S(2)}) copy-start(f32[2,129,256]{2,0,1:T(2,128)} %param.13) | copy-start | bytes 792580
  84.3 9.3 %copy-start.9 = (s32[64]{0:T(128)S(1)}, s32[64]{0:T(128)}, u32[]{:S(2)}) copy-start(s32[64]{0:T(128)} %slice.21) | copy-start | bytes 772
  87.8 18.8 %copy-start.6 = (f32[2,256]{1,0:T(2,128)S(1)}, f32[2,256]{1,0:T(2,128)}, u32[]{:S(2)}) copy-start(f32[2,256]{1,0:T(2,128)} %gain_ref.3) | copy-start | bytes 6148
  87.8 18.8 %copy-start.3 = (bf16[16,4,2,16,256]{4,3,2,1,0:T(8,128)(2,1)S(1)}, bf16[16,4,2,16,256]{4,3,2,1,0:T(8,128)(2,1)}, u32[]{:S(2)}) copy-start(bf16[16,4,2,16,256]{4,3,2,1,0:T(8,128)(2,1)} %copy-done.2) | copy-start | bytes 3145732
  87.9 8.1 %collective-permute-start.4 = (bf16[64,256]{1,0:T(8,128)(2,1)S(1)}, bf16[64,256]{1,0:T(8,128)(2,1)S(1)}, u32[]{:S(2)}, u32[]{:S(2)}) collective-permute-start(bf16[64,256]{1,0:T(8,128)(2,1)S(1)} %get-tuple-element.42), channel_id=1, source_target_pairs={{0,4},{4,8},{8,12},{12,16},{16,20},{20,24},{24,28},{28,32},{32,36}... | collective-permute-start | bytes 98312 | tf_op jit(solution)/shard_map/ppermute | solution.py:254
  89.9 6.0 %collective-permute-start.5 = (bf16[64,256]{1,0:T(8,128)(2,1)S(1)}, bf16[64,256]{1,0:T(8,128)(2,1)S(1)}, u32[]{:S(2)}, u32[]{:S(2)}) collective-permute-start(bf16[64,256]{1,0:T(8,128)(2,1)S(1)} %get-tuple-element.41), channel_id=1, source_target_pairs={{4,0},{8,4},{12,8},{16,12},{20,16},{24,20},{28,24},{32,28},{36,32}... | collective-permute-start | bytes 98312 | tf_op jit(solution)/shard_map/ppermute | solution.py:255
  108.7 18.5 %all-to-all-start.2 = ((bf16[4,256,512]{2,1,0:T(8,128)(2,1)}), bf16[4,256,512]{2,1,0:T(8,128)(2,1)S(1)}, u32[]{:S(2)}, u32[]{:S(2)}) async-start(bf16[4,256,512]{2,1,0:T(8,128)(2,1)} %project.2), calls=%async_computation.2 | async-start | bytes 2097152 | tf_op jit(solution)/shard_map/all_to_all | solution.py:240
  112.2 15.4 %collective-permute-start.11 = (bf16[256,768]{1,0:T(8,128)(2,1)S(1)}, bf16[256,768]{1,0:T(8,128)(2,1)S(1)}, u32[]{:S(2)}, u32[]{:S(2)}) collective-permute-start(bf16[256,768]{1,0:T(8,128)(2,1)S(1)} %get-tuple-element.31), channel_id=1, source_target_pairs={{0,16},{8,24},{16,0},{24,8},{1,17},{9,25},{17,1},{25,9},{2,18},{10... | collective-permute-start | bytes 1179656 | tf_op jit(solution)/shard_map/ppermute | solution.py:247
  114.4 16.3 %collective-permute-start.12 = (bf16[256,768]{1,0:T(8,128)(2,1)S(1)}, bf16[256,768]{1,0:T(8,128)(2,1)S(1)}, u32[]{:S(2)}, u32[]{:S(2)}) collective-permute-start(bf16[256,768]{1,0:T(8,128)(2,1)S(1)} %get-tuple-element.31), channel_id=1, source_target_pairs={{0,8},{8,16},{16,24},{24,0},{1,9},{9,17},{17,25},{25,1},{2,10},{10... | collective-permute-start | bytes 1179656 | tf_op jit(solution)/shard_map/ppermute | solution.py:247
  117.5 17.1 %collective-permute-start.13 = (bf16[256,768]{1,0:T(8,128)(2,1)S(1)}, bf16[256,768]{1,0:T(8,128)(2,1)}, u32[]{:S(2)}, u32[]{:S(2)}) collective-permute-start(bf16[256,768]{1,0:T(8,128)(2,1)S(1)} %get-tuple-element.31), channel_id=1, source_target_pairs={{0,24},{8,0},{16,8},{24,16},{1,25},{9,1},{17,9},{25,17},{2,26},{10... | collective-permute-start | bytes 1179656 | tf_op jit(solution)/shard_map/ppermute | solution.py:247
  134.7 25.4 %copy-start.5 = (f32[2,2048]{1,0:T(2,128)S(1)}, f32[2,2048]{1,0:T(2,128)}, u32[]{:S(2)}) copy-start(f32[2,2048]{1,0:T(2,128)} %refs_4_.1) | copy-start | bytes 49156
  135.9 24.2 %collective-permute-start.14 = (bf16[4,256,768]{2,1,0:T(8,128)(2,1)S(1)}, bf16[4,256,768]{2,1,0:T(8,128)(2,1)S(1)}, u32[]{:S(2)}, u32[]{:S(2)}) collective-permute-start(bf16[4,256,768]{2,1,0:T(8,128)(2,1)S(1)} %pad_maximum_fusion.1.refs_5_), channel_id=1, source_target_pairs={{0,4},{4,0},{1,5},{5,1},{2,6},{6,2},{3,7},{7,3},{8,12},{12,8},{9,1... | collective-permute-start | bytes 4718600 | tf_op jit(solution)/shard_map/ppermute | solution.py:236
  137.9 16.6 %collective-permute-start.10 = (bf16[256,512]{1,0:T(8,128)(2,1)S(1)}, bf16[256,512]{1,0:T(8,128)(2,1)S(1)}, u32[]{:S(2)}, u32[]{:S(2)}) collective-permute-start(bf16[256,512]{1,0:T(8,128)(2,1)S(1)} %add_parts.2.refs_0_.stream_ref), channel_id=1, source_target_pairs={{0,3},{1,0},{2,1},{3,2},{4,7},{5,4},{6,5},{7,6},{8,11},{9,8},{10,9... | collective-permute-start | bytes 786440 | tf_op jit(solution)/shard_map/ppermute | solution.py:247
  142.7 12.6 %collective-permute-start.8 = (bf16[256,512]{1,0:T(8,128)(2,1)S(1)}, bf16[256,512]{1,0:T(8,128)(2,1)S(1)}, u32[]{:S(2)}, u32[]{:S(2)}) collective-permute-start(bf16[256,512]{1,0:T(8,128)(2,1)S(1)} %add_parts.2.refs_0_.stream_ref), channel_id=1, source_target_pairs={{0,2},{1,3},{2,0},{3,1},{4,6},{5,7},{6,4},{7,5},{8,10},{9,11},{10,... | collective-permute-start | bytes 786440 | tf_op jit(solution)/shard_map/ppermute | solution.py:247
  145.5 14.6 %collective-permute-start.9 = (bf16[256,512]{1,0:T(8,128)(2,1)S(1)}, bf16[256,512]{1,0:T(8,128)(2,1)S(1)}, u32[]{:S(2)}, u32[]{:S(2)}) collective-permute-start(bf16[256,512]{1,0:T(8,128)(2,1)S(1)} %add_parts.2.refs_0_.stream_ref), channel_id=1, source_target_pairs={{0,1},{1,2},{2,3},{3,0},{4,5},{5,6},{6,7},{7,4},{8,9},{9,10},{10,1... | collective-permute-start | bytes 786440 | tf_op jit(solution)/shard_map/ppermute | solution.py:247
  161.8 7.9 %collective-permute-start.15 = (bf16[64,256]{1,0:T(8,128)(2,1)S(1)}, bf16[64,256]{1,0:T(8,128)(2,1)S(1)}, u32[]{:S(2)}, u32[]{:S(2)}) collective-permute-start(bf16[64,256]{1,0:T(8,128)(2,1)S(1)} %get-tuple-element.40), channel_id=1, source_target_pairs={{0,4},{4,8},{8,12},{12,16},{16,20},{20,24},{24,28},{28,32},{32,36}... | collective-permute-start | bytes 98312 | tf_op jit(solution)/shard_map/ppermute | solution.py:254
  163.7 6.0 %collective-permute-start.16 = (bf16[64,256]{1,0:T(8,128)(2,1)S(1)}, bf16[64,256]{1,0:T(8,128)(2,1)S(1)}, u32[]{:S(2)}, u32[]{:S(2)}) collective-permute-start(bf16[64,256]{1,0:T(8,128)(2,1)S(1)} %get-tuple-element.39), channel_id=1, source_target_pairs={{4,0},{8,4},{12,8},{16,12},{20,16},{24,20},{28,24},{32,28},{36,32}... | collective-permute-start | bytes 98312 | tf_op jit(solution)/shard_map/ppermute | solution.py:255
  (5 other events, 20.6 us)

commit v4 on v3

--- a/solution.py
+++ b/solution.py
@@ -32,10 +32,10 @@
 SMEM = pl.BlockSpec(memory_space=pltpu.SMEM)
 
 
-def assemble(at_ref, own_ref, other_ref, gate_ref, out_ref):
+def assemble(rotated, at_ref, own_ref, other_ref, gate_ref, out_ref):
     core = at_ref[0]
     for i in range(NX):
-        x = lax.rem(at_ref[2] + (NX - STEPS[i]), NX)
+        x = lax.rem(at_ref[2] + (NX - STEPS[i]), NX) if rotated else i
         for part, ref in ((core, own_ref), (1 - core, other_ref)):
             gate_ref[:, x, part] = ref[i, :, : 2 * CH].reshape(NZ, 16, 2 * CH)
             out_ref[:, x, part] = ref[i, :, 2 * CH :].reshape(NZ, 16, CH)
@@ -80,20 +80,17 @@
     )(column)
 
 
-def gate_kernel(layer, count, at_ref, *refs):
+def gate_kernel(layer, at_ref, *refs):
     *piece_refs, gain_ref, own_ref, other_ref, gated_ref, out_ref, w_ref = refs
-    if count == 1:
-        blocks = [(y, piece_refs[0][y]) for y in range(NT)]
-    else:
-        blocks = [(lax.rem(at_ref[1] + (NT - s), NT), ref[...]) for s, ref in zip(STEPS, piece_refs)]
-    assemble(at_ref, own_ref, other_ref, w_ref, out_ref)
+    blocks = [(lax.rem(at_ref[1] + (NT - s), NT), ref[...]) for s, ref in zip(STEPS, piece_refs)]
+    assemble(layer > 0, at_ref, own_ref, other_ref, w_ref, out_ref)
     wide = [block.astype(F32) for _, block in blocks]
     square = sum(jnp.sum(v * v, axis=1, keepdims=True) for v in wide)
     scale = lax.rsqrt(square * (1.0 / D) + EPSILON)
     pre = jnp.zeros((TOK, 2 * CH), F32)
     part = NZ // NT
     for v, (y, _) in zip(wide, blocks):
-        start = y * FD if count == 1 else pl.multiple_of(y * FD, FD)
+        start = pl.multiple_of(y * FD, FD)
         gain = gain_ref[layer : layer + 1, pl.ds(start, FD)]
         normed = (v * scale * gain).astype(BF16)
         w = w_ref[pl.ds(y * part, part)].reshape(FD, 2 * CH)
@@ -103,12 +100,12 @@
 
 def gate(layer, at, pieces, gain, own, other):
     return pl.pallas_call(
-        functools.partial(gate_kernel, layer, len(pieces)),
+        functools.partial(gate_kernel, layer),
         out_shape=(
             jax.ShapeDtypeStruct((TOK, CH), BF16),
             jax.ShapeDtypeStruct((NZ, NX, NC, 16, CH), BF16),
         ),
-        in_specs=[SMEM] + [VMEM] * (3 + len(pieces)),
+        in_specs=[SMEM] + [VMEM] * (3 + NT),
         out_specs=(VMEM, VMEM),
         scratch_shapes=[pltpu.VMEM((NZ, NX, NC, 16, 2 * CH), BF16)],
         name="gate",
@@ -128,62 +125,76 @@
     return acc
 
 
-def inner_kernel(layer, mid_ref, seg_ref, taps_ref, conv_ref, x_ref):
+HALF = TOK - 2 * R
+
+
+def inner_kernel(layer, own_ref, seg_ref, taps_ref, conv_ref, x_ref):
     for h in range(CH // LANES):
-        x_ref[h] = mid_ref[:, h * LANES : (h + 1) * LANES].astype(F32)
-    for first in range(0, TOK - 2 * R, TILE):
-        for h, acc in enumerate(tap_sums(layer, x_ref, seg_ref, taps_ref, first, first + R)):
+        x_ref[h] = own_ref[:, h * LANES : (h + 1) * LANES].astype(F32)
+    for first in range(0, HALF, TILE):
+        for h, acc in enumerate(tap_sums(layer, x_ref, seg_ref, taps_ref, first, first + (0, 2 * R)[layer])):
             conv_ref[first : first + TILE, h * LANES : (h + 1) * LANES] = acc
 
 
-def inner(layer, mid, seg, taps):
+def inner(layer, own, seg, taps):
     return pl.pallas_call(
         functools.partial(inner_kernel, layer),
-        out_shape=jax.ShapeDtypeStruct((TOK - 2 * R, CH), F32),
+        out_shape=jax.ShapeDtypeStruct((HALF, CH), F32),
         in_specs=[VMEM] * 3,
         out_specs=VMEM,
         scratch_shapes=[pltpu.VMEM((CH // LANES, TOK, LANES), F32)],
         name="inner",
         compiler_params=LIMIT,
-    )(mid, seg, taps)
-
-
-def outer_kernel(layer, before_ref, mid_ref, after_ref, seg_ref, taps_ref, inner_ref, conv_ref, stat_ref, x_ref):
+    )(own, seg, taps)
+
+
+def lane_sums(wide):
+    ones = jnp.ones((8, LANES), BF16)
+    total = jnp.zeros((8, wide.shape[0]), F32)
+    for _ in range(3):
+        part = wide.astype(BF16)
+        wide = wide - part.astype(F32)
+        total = total + lax.dot_general(ones, part, (((1,), (1,)), ((), ())), preferred_element_type=F32)
+    return total[0:1, :]
+
+
+def outer_kernel(layer, own_ref, halo_ref, seg_ref, taps_ref, inner_ref, conv_ref, stat_ref, x_ref):
     for h in range(CH // LANES):
         cols = slice(h * LANES, (h + 1) * LANES)
-        x_ref[h, 0:R] = before_ref[:, cols].astype(F32)
-        x_ref[h, R : 3 * R] = mid_ref[: 2 * R, cols].astype(F32)
-        x_ref[h, 3 * R : 5 * R] = mid_ref[TOK - 2 * R :, cols].astype(F32)
-        x_ref[h, 5 * R :] = after_ref[:, cols].astype(F32)
-    conv_ref[R : TOK - R, :] = inner_ref[...]
-    for x_first, first in ((0, 0), (3 * R, TOK - R)):
-        for h, acc in enumerate(tap_sums(layer, x_ref, seg_ref, taps_ref, x_first, first)):
-            conv_ref[first : first + R, h * LANES : (h + 1) * LANES] = acc
-    conv = conv_ref[...]
-    ones = jnp.ones((8, CH), F32)
-    dims = (((1,), (1,)), ((), ()))
-    total = lax.dot_general(ones, conv, dims, precision=lax.Precision.HIGHEST, preferred_element_type=F32)
-    square = lax.dot_general(ones, conv * conv, dims, precision=lax.Precision.HIGHEST, preferred_element_type=F32)
-    for y in range(NT):
-        stat_ref[y, 0:1, :] = total[0:1, :]
-        stat_ref[y, 1:2, :] = square[0:1, :]
-
-
-def outer(layer, before, mid, after, seg, taps, inside):
+        halo = halo_ref[:, cols].astype(F32)
+        if layer == 0:
+            x_ref[h, :HALF] = own_ref[TOK - HALF :, cols].astype(F32)
+            x_ref[h, HALF:] = halo
+        else:
+            x_ref[h, : 2 * R] = halo
+            x_ref[h, 2 * R :] = own_ref[:HALF, cols].astype(F32)
+    skip, start = ((0, HALF), (2 * R, 0))[layer]
+    conv_ref[skip : skip + HALF, :] = inner_ref[...]
+    for first in range(0, 2 * R, TILE):
+        for h, acc in enumerate(tap_sums(layer, x_ref, seg_ref, taps_ref, first, first + start)):
+            conv_ref[start + first : start + first + TILE, h * LANES : (h + 1) * LANES] = acc
+    low, high = conv_ref[:, :LANES], conv_ref[:, LANES:]
+    for i, wide in enumerate((low + high, low * low + high * high)):
+        row = lane_sums(wide)
+        for y in range(NT):
+            stat_ref[y, i : i + 1, :] = row
+
+
+def outer(layer, own, halo, seg, taps, inside):
     return pl.pallas_call(
         functools.partial(outer_kernel, layer),
         out_shape=(jax.ShapeDtypeStruct((TOK, CH), F32), jax.ShapeDtypeStruct((NT, 2, TOK), F32)),
-        in_specs=[VMEM] * 6,
+        in_specs=[VMEM] * 5,
         out_specs=(VMEM, VMEM),
-        scratch_shapes=[pltpu.VMEM((CH // LANES, 6 * R, LANES), F32)],
+        scratch_shapes=[pltpu.VMEM((CH // LANES, TOK, LANES), F32)],
         name="outer",
         compiler_params=LIMIT,
-    )(before, mid, after, seg, taps, inside)
+    )(own, halo, seg, taps, inside)
 
 
 def out_kernel(layer, conv_ref, stat_ref, gain_ref, w_ref, parts_ref):
     stat = stat_ref[...]
-    kind = lax.broadcasted_iota(jnp.int32, (2 * NT, CH), 0) % 2
+    kind = lax.broadcasted_iota(jnp.int32, (2 * NT, LANES), 0) % 2
     dims = (((0,), (0,)), ((), ()))
 
     def spread(which):
@@ -192,8 +203,13 @@
 
     mean = spread(0) * (1.0 / CF)
     var = jnp.maximum(spread(1) * (1.0 / CF) - mean * mean, 0.0)
-    v = (conv_ref[...] - mean) * lax.rsqrt(var + EPSILON) * gain_ref[layer : layer + 1, :]
-    act = jax.nn.silu(v).astype(BF16)
+    scale = lax.rsqrt(var + EPSILON)
+    act = []
+    for h in range(CH // LANES):
+        cols = slice(h * LANES, (h + 1) * LANES)
+        v = (conv_ref[:, cols] - mean) * scale * gain_ref[layer : layer + 1, cols]
+        act.append(jax.nn.silu(v).astype(BF16))
+    act = jnp.concatenate(act, axis=1)
     rows = NZ // NT
     for y in range(NT):
         w = w_ref[y * rows : (y + 1) * rows].reshape(FD, CH)
@@ -212,20 +228,27 @@
     )(conv, stat, gain, weight)
 
 
-def add_kernel(stream_ref, parts_ref, out_ref):
-    total = stream_ref[...].astype(F32) + sum(parts_ref[y].astype(F32) for y in range(NT))
-    out_ref[...] = total.astype(BF16)
-
-
-def add_parts(stream, parts):
-    return pl.pallas_call(
-        add_kernel,
+def add_kernel(layer, stream_ref, side_ref, parts_ref, out_ref):
+    def part(rows):
+        return sum(parts_ref[y, rows].astype(F32) for y in range(NT))
+
+    if layer == 0:
+        kept, own, side = slice(R, TOK), slice(0, TOK - R), slice(TOK - R, TOK)
+    else:
+        kept, own, side = slice(0, TOK - R), slice(R, TOK), slice(0, R)
+    out_ref[own] = (stream_ref[kept].astype(F32) + part(own)).astype(BF16)
+    out_ref[side] = (side_ref[...].astype(F32) + part(side)).astype(BF16)
+
+
+def add_parts(layer, stream, side, parts):
+    return pl.pallas_call(
+        functools.partial(add_kernel, layer),
         out_shape=jax.ShapeDtypeStruct((TOK, FD), BF16),
-        in_specs=[VMEM, VMEM],
+        in_specs=[VMEM] * 3,
         out_specs=VMEM,
         name="add_parts",
         compiler_params=LIMIT,
-    )(stream, parts)
+    )(stream, side, parts)
 
 
 def copies_of(x, n):
@@ -248,12 +271,14 @@
     return came
 
 
-def neighbours(up, down):
+def from_next(x):
     n = NZ * NX * NC
-    ups = [(i, i + 1) for i in range(n - 1)]
-    before = lax.ppermute(up, SP, ups)
-    after = lax.ppermute(down, SP, [(j, i) for i, j in ups])
-    return before, after
+    return lax.ppermute(x, SP, [((i + 1) % n, i) for i in range(n)])
+
+
+def from_previous(x):
+    n = NZ * NX * NC
+    return lax.ppermute(x, SP, [(i, (i + 1) % n) for i in range(n)])
 
 
 def after_(x, *others):
@@ -267,28 +292,39 @@
     own = pack(w_value, w_gate, out_t)
     column = lax.all_gather(own, "z", axis=0, tiled=True)
     first_own, rest_own = split(column)
-    first = ring([first_own] * NX, "x")
+    first = exchange(copies_of(first_own, NX), "x")
     tokens_late, segments_late = lax.optimization_barrier((tokens, segments, column))[:2]
-    pieces = (exchange(copies_of(tokens_late, NT), "tp"),)
-    seg_before, seg_after = neighbours(segments_late, segments_late)
-    first = jnp.stack(first)
+    pieces = ring([tokens_late] * NT, "tp")
+    seg_after = from_next(segments_late)
     first_other = swap_core(first)
-    seg_wide = jnp.concatenate([seg_before[TOK - R :], segments, seg_after[:R]])
-    seg_lanes = jnp.broadcast_to(seg_wide[:, None], (TOK + 2 * R, LANES))
+
+    def seg_rows(*pieces):
+        return jnp.broadcast_to(jnp.concatenate(pieces)[:, None], (TOK + 2 * R, LANES))
+
+    seg_lanes = seg_rows(segments, seg_after[: 2 * R])
     taps = jnp.swapaxes(conv_taps, 0, 1)
 
     stream = tokens
     weights = (first, first_other)
     for layer in range(LAYERS):
         gated, out_weight = gate(layer, at, pieces, in_gain, *weights)
-        before, after = neighbours(gated[TOK - R :], gated[:R])
+        if layer == 0:
+            halo = from_next(gated[: 2 * R])
+        else:
+            halo = from_previous(gated[TOK - 2 * R :])
         inside = inner(layer, gated, seg_lanes, taps)
-        conv, stat = outer(layer, before, gated, after, seg_lanes, taps, inside)
+        conv, stat = outer(layer, gated, halo, seg_lanes, taps, inside)
         stats = exchange(stat, "tp").reshape(2 * NT, TOK)
+        if layer == 0:
+            tokens_after = from_next(after_(tokens, conv)[:R])
         parts = project(layer, conv, stats, norm_gain, out_weight)
         received = exchange(parts, "tp")
-        stream = add_parts(stream, received)
+        side = tokens_after if layer == 0 else stream_before
+        stream = add_parts(layer, stream, side, received)
         if layer == 0:
+            stream_before = from_previous(stream[TOK - R :])
+            seg_before = from_previous(after_(segments, stream))
+            seg_lanes = seg_rows(seg_before[TOK - R :], segments, seg_after[:R])
             rest = ring([after_(rest_own, parts)] * NX, "x")
             pieces = ring([stream] * NT, "tp")
             rest = jnp.stack(list(lax.optimization_barrier((*rest, stream))[:NX]))

time: 202 us -> 193 us (0.955)
  waiting for transfers between devices: 44 us -> 36.9 us
    ppermute x6, waiting for transfers between devices: 0.55 us -> 17.4 us  [the longest x3 9.58 us: from_next(): return lax.ppermute(x, SP, [((i + 1) % n, i) for i in range(n)])]
    ppermute x9, waiting for transfers between devices: 28.1 us -> 11.9 us  [ring(): lax.ppermute(piece, axis, [(i, (i + step) % n) for i in range(n)])]
    all_to_all x2, waiting for transfers between devices: 15.4 us -> 7.64 us  [exchange(): return lax.all_to_all(x, axis, 0, 0, tiled=True)]
    ppermute x9, starting transfers between devices: 27.6 us -> 33.1 us  [ring(): lax.ppermute(piece, axis, [(i, (i + step) % n) for i in range(n)])]
    ppermute x6, starting transfers between devices: 17 us -> 11.8 us  [the longest x3 5.95 us: from_previous(): return lax.ppermute(x, SP, [(i, (i + 1) % n) for i in range(n)])]
  transfers between devices with their start and end apart: 19 -> 19, of which waited for: 12 -> 12; matrix products, arithmetic and copies ran while one was open for 1% -> 1% of each run, Pallas kernels for 2% -> 3%
where the time goes in v4:
time: 193 us; the launch traced here: 191 us
  blocking collectives  74.3 us (38%)
  starting transfers between devices  56 us (29%)
  waiting for transfers between devices  36.9 us (19%)
  Pallas kernels  19.6 us (10%)
  local copies, waits for them, and re-layouts  2.54 us (1%)
    all_gather x1, blocking collectives, program(): column = lax.all_gather(own, 'z', axis=0, tiled=True)  40.4 us
    all_to_all x3, blocking collectives, exchange(): return lax.all_to_all(x, axis, 0, 0, tiled=True)  33.9 us
    ppermute x9, starting transfers between devices, ring(): lax.ppermute(piece, axis, [(i, (i + step) % n) for i in range(n)])  33.1 us
    ppermute x9, waiting for transfers between devices, ring(): lax.ppermute(piece, axis, [(i, (i + step) % n) for i in range(n)])  11.9 us
    ppermute x3, waiting for transfers between devices, from_next(): return lax.ppermute(x, SP, [((i + 1) % n, i) for i in range(n)])  9.58 us
    ppermute x3, waiting for transfers between devices, from_previous(): return lax.ppermute(x, SP, [(i, (i + 1) % n) for i in range(n)])  7.86 us
    all_to_all x2, waiting for transfers between devices, exchange(): return lax.all_to_all(x, axis, 0, 0, tiled=True)  7.64 us
    all_to_all x2, starting transfers between devices, exchange(): return lax.all_to_all(x, axis, 0, 0, tiled=True)  7.16 us
  transfers between devices with their start and end apart: 19, of which 12 were waited for; matrix products, arithmetic and copies ran while one was open for 1% of the time, Pallas kernels for 3%

profile of v4, /device:TPU:6, one launch (start us, length us, event | category | flops | bytes accessed | tf_op | source)
XLA Modules:
  0.0 191.0 jit_solution(18251143026286458997)
XLA Ops:
  1.5 40.4 %all_gather.3.column_ref = bf16[256,1536]{1,0:T(8,128)(2,1)S(1)} all-gather(bf16[16,1536]{1,0:T(8,128)(2,1)} %pack.1), channel_id=1, replica_groups=mesh['z'=16,'x'=4,'c'=2,'tp'=4] {'z'}, dimensions={0}, use_global_device_ids=true | all-gather | bytes 835584 | tf_op jit(solution)/shard_map/all_gather | solution.py:293
  42.1 16.3 %all_to_all.25.refs_5_ = bf16[4,256,768]{2,1,0:T(8,128)(2,1)S(1)} all-to-all(bf16[4,256,768]{2,1,0:T(8,128)(2,1)S(1)} %broadcast_in_dim.6), channel_id=1, replica_groups=mesh['z'=16,'x'=4,'c'=2,'tp'=4] {'x'}, dimensions={0} | all-to-all | bytes 3145728 | tf_op jit(solution)/shard_map/all_to_all | solution.py:263
  60.3 5.1 %collective-permute-start = (bf16[256,512]{1,0:T(8,128)(2,1)}, bf16[256,512]{1,0:T(8,128)(2,1)}, u32[]{:S(2)}, u32[]{:S(2)}) collective-permute-start(bf16[256,512]{1,0:T(8,128)(2,1)} %stream_ref.1), channel_id=1, source_target_pairs={{0,2},{1,3},{2,0},{3,1},{4,6},{5,7},{6,4},{7,5},{8,10},{9,11},{10,... | collective-permute-start | bytes 786440 | tf_op jit(solution)/shard_map/ppermute | solution.py:270
  65.4 2.6 %collective-permute-start.1 = (bf16[256,512]{1,0:T(8,128)(2,1)}, bf16[256,512]{1,0:T(8,128)(2,1)}, u32[]{:S(2)}, u32[]{:S(2)}) collective-permute-start(bf16[256,512]{1,0:T(8,128)(2,1)} %stream_ref.1), channel_id=1, source_target_pairs={{0,1},{1,2},{2,3},{3,0},{4,5},{5,6},{6,7},{7,4},{8,9},{9,10},{10,1... | collective-permute-start | bytes 786440 | tf_op jit(solution)/shard_map/ppermute | solution.py:270
  68.0 4.5 %collective-permute-start.2 = (bf16[256,512]{1,0:T(8,128)(2,1)}, bf16[256,512]{1,0:T(8,128)(2,1)}, u32[]{:S(2)}, u32[]{:S(2)}) collective-permute-start(bf16[256,512]{1,0:T(8,128)(2,1)} %stream_ref.1), channel_id=1, source_target_pairs={{0,3},{1,0},{2,1},{3,2},{4,7},{5,4},{6,5},{7,6},{8,11},{9,8},{10,9... | collective-permute-start | bytes 786440 | tf_op jit(solution)/shard_map/ppermute | solution.py:270
  75.7 2.6 %collective-permute-done.1.refs_2_ = bf16[256,512]{1,0:T(8,128)(2,1)} collective-permute-done((bf16[256,512]{1,0:T(8,128)(2,1)}, bf16[256,512]{1,0:T(8,128)(2,1)}, u32[]{:S(2)}, u32[]{:S(2)}) %collective-permute-start.1) | collective-permute-done | bytes 262176 | tf_op jit(solution)/shard_map/ppermute | solution.py:270
  78.7 2.3 %gate.2 = (bf16[256,256]{1,0:T(8,128)(2,1)S(1)}, bf16[16,4,2,16,256]{4,3,2,1,0:T(8,128)(2,1)S(1)}) custom-call(s32[3]{0:T(128)S(1)} %pad_add_fusion.2.at_ref, bf16[256,512]{1,0:T(8,128)(2,1)} %stream_ref.1, bf16[256,512]{1,0:T(8,128)(2,1)} %collective-permute-done.refs_1_, bf16[256,512]{1,0:T(8,128)(2,1)} %collective-permute-done.1.refs_2_, ...), custom_call_target="tpu_custom_call" | custom-call | tf_op jit(solution)/shard_map/gate/pallas_call | solution.py:102
  85.3 2.2 %outer.2 = (f32[256,256]{1,0:T(8,128)S(1)}, f32[4,2,256]{2,1,0:T(2,128)S(1)}) custom-call(bf16[256,256]{1,0:T(8,128)(2,1)S(1)} %get-tuple-element.26.own_ref, bf16[128,256]{1,0:T(8,128)(2,1)S(1)} %collective-permute-done.4.halo_ref, s32[384,128]{1,0:T(8,128)S(1)} %broadcast_in_dim.7.seg_ref, f32[129,2,256]{2,1,0:T(2,128)S(1)} %bitcast.10, ...), custom_call_target="tpu_custom_call" | custom-call | tf_op jit(solution)/shard_map/outer/pallas_call | solution.py:184
  87.6 9.8 %all_to_all.26 = f32[4,2,256]{2,1,0:T(2,128)S(1)} all-to-all(f32[4,2,256]{2,1,0:T(2,128)S(1)} %get-tuple-element.30), channel_id=1, replica_groups=mesh['z'=16,'x'=4,'c'=2,'tp'=4] {'tp'}, dimensions={0} | all-to-all | bytes 16384 | tf_op jit(solution)/shard_map/all_to_all | solution.py:263
  100.5 3.6 %all-to-all-start.2 = ((bf16[4,256,512]{2,1,0:T(8,128)(2,1)}), bf16[4,256,512]{2,1,0:T(8,128)(2,1)S(1)}, u32[]{:S(2)}, u32[]{:S(2)}) async-start(bf16[4,256,512]{2,1,0:T(8,128)(2,1)} %project.2), calls=%async_computation.2 | async-start | bytes 2097152 | tf_op jit(solution)/shard_map/all_to_all | solution.py:263
  104.1 4.5 %collective-permute-start.11 = (bf16[256,768]{1,0:T(8,128)(2,1)S(1)}, bf16[256,768]{1,0:T(8,128)(2,1)S(1)}, u32[]{:S(2)}, u32[]{:S(2)}) collective-permute-start(bf16[256,768]{1,0:T(8,128)(2,1)S(1)} %copy-done.4), channel_id=1, source_target_pairs={{0,16},{8,24},{16,0},{24,8},{1,17},{9,25},{17,1},{25,9},{2,18},{10... | collective-permute-start | bytes 1179656 | tf_op jit(solution)/shard_map/ppermute | solution.py:270
  108.6 3.1 %collective-permute-start.12 = (bf16[256,768]{1,0:T(8,128)(2,1)S(1)}, bf16[256,768]{1,0:T(8,128)(2,1)S(1)}, u32[]{:S(2)}, u32[]{:S(2)}) collective-permute-start(bf16[256,768]{1,0:T(8,128)(2,1)S(1)} %copy-done.4), channel_id=1, source_target_pairs={{0,8},{8,16},{16,24},{24,0},{1,9},{9,17},{17,25},{25,1},{2,10},{10... | collective-permute-start | bytes 1179656 | tf_op jit(solution)/shard_map/ppermute | solution.py:270
  111.7 2.8 %collective-permute-start.13 = (bf16[256,768]{1,0:T(8,128)(2,1)S(1)}, bf16[256,768]{1,0:T(8,128)(2,1)}, u32[]{:S(2)}, u32[]{:S(2)}) collective-permute-start(bf16[256,768]{1,0:T(8,128)(2,1)S(1)} %copy-done.4), channel_id=1, source_target_pairs={{0,24},{8,0},{16,8},{24,16},{1,25},{9,1},{17,9},{25,17},{2,26},{10... | collective-permute-start | bytes 1179656 | tf_op jit(solution)/shard_map/ppermute | solution.py:270
  117.3 8.4 %collective-permute-done.6.side_ref = bf16[64,512]{1,0:T(8,128)(2,1)S(1)} collective-permute-done((bf16[64,512]{1,0:T(8,128)(2,1)S(1)}, bf16[64,512]{1,0:T(8,128)(2,1)S(1)}, u32[]{:S(2)}, u32[]{:S(2)}) %collective-permute-start.6) | collective-permute-done | bytes 65568 | tf_op jit(solution)/shard_map/ppermute | solution.py:276
  131.9 5.1 %collective-permute-start.10 = (bf16[256,512]{1,0:T(8,128)(2,1)S(1)}, bf16[256,512]{1,0:T(8,128)(2,1)S(1)}, u32[]{:S(2)}, u32[]{:S(2)}) collective-permute-start(bf16[256,512]{1,0:T(8,128)(2,1)S(1)} %add_parts.2.refs_0_.stream_ref), channel_id=1, source_target_pairs={{0,3},{1,0},{2,1},{3,2},{4,7},{5,4},{6,5},{7,6},{8,11},{9,8},{10,9... | collective-permute-start | bytes 786440 | tf_op jit(solution)/shard_map/ppermute | solution.py:270
  137.0 2.8 %collective-permute-start.8 = (bf16[256,512]{1,0:T(8,128)(2,1)S(1)}, bf16[256,512]{1,0:T(8,128)(2,1)S(1)}, u32[]{:S(2)}, u32[]{:S(2)}) collective-permute-start(bf16[256,512]{1,0:T(8,128)(2,1)S(1)} %add_parts.2.refs_0_.stream_ref), channel_id=1, source_target_pairs={{0,2},{1,3},{2,0},{3,1},{4,6},{5,7},{6,4},{7,5},{8,10},{9,11},{10,... | collective-permute-start | bytes 786440 | tf_op jit(solution)/shard_map/ppermute | solution.py:270
  139.7 2.8 %collective-permute-start.9 = (bf16[256,512]{1,0:T(8,128)(2,1)S(1)}, bf16[256,512]{1,0:T(8,128)(2,1)S(1)}, u32[]{:S(2)}, u32[]{:S(2)}) collective-permute-start(bf16[256,512]{1,0:T(8,128)(2,1)S(1)} %add_parts.2.refs_0_.stream_ref), channel_id=1, source_target_pairs={{0,1},{1,2},{2,3},{3,0},{4,5},{5,6},{6,7},{7,4},{8,9},{9,10},{10,1... | collective-permute-start | bytes 786440 | tf_op jit(solution)/shard_map/ppermute | solution.py:270
  144.5 3.0 %collective-permute-done.16 = s32[256]{0:T(256)S(1)} collective-permute-done((s32[256]{0:T(256)S(1)}, s32[256]{0:T(256)S(1)}, u32[]{:S(2)}, u32[]{:S(2)}) %collective-permute-start.16) | collective-permute-done | bytes 1056 | tf_op jit(solution)/shard_map/ppermute | solution.py:281
  149.6 4.8 %collective-permute-done.9.refs_2_ = bf16[256,512]{1,0:T(8,128)(2,1)S(1)} collective-permute-done((bf16[256,512]{1,0:T(8,128)(2,1)S(1)}, bf16[256,512]{1,0:T(8,128)(2,1)S(1)}, u32[]{:S(2)}, u32[]{:S(2)}) %collective-permute-start.9) | collective-permute-done | bytes 262176 | tf_op jit(solution)/shard_map/ppermute | solution.py:270
  161.7 2.2 %outer.3 = (f32[256,256]{1,0:T(8,128)S(1)}, f32[4,2,256]{2,1,0:T(2,128)S(1)}) custom-call(bf16[256,256]{1,0:T(8,128)(2,1)S(1)} %get-tuple-element.38.own_ref, bf16[128,256]{1,0:T(8,128)(2,1)S(1)} %collective-permute-done.15.halo_ref, s32[384,128]{1,0:T(8,128)S(1)} %broadcast_in_dim.8.seg_ref, f32[129,2,256]{2,1,0:T(2,128)S(1)} %bitcast.12, ...), custom_call_target="tpu_custom_call" | custom-call | tf_op jit(solution)/shard_map/outer/pallas_call | solution.py:184
  163.9 7.7 %all_to_all.27 = f32[4,2,256]{2,1,0:T(2,128)S(1)} all-to-all(f32[4,2,256]{2,1,0:T(2,128)S(1)} %get-tuple-element.41), channel_id=1, replica_groups=mesh['z'=16,'x'=4,'c'=2,'tp'=4] {'tp'}, dimensions={0} | all-to-all | bytes 16384 | tf_op jit(solution)/shard_map/all_to_all | solution.py:263
  173.4 3.5 %all-to-all-start.4 = ((bf16[4,256,512]{2,1,0:T(8,128)(2,1)}), bf16[4,256,512]{2,1,0:T(8,128)(2,1)S(1)}, u32[]{:S(2)}, u32[]{:S(2)}) async-start(bf16[4,256,512]{2,1,0:T(8,128)(2,1)} %project.3), calls=%async_computation.4 | async-start | bytes 2097152 | tf_op jit(solution)/shard_map/all_to_all | solution.py:263
  178.9 3.7 %collective-permute-done.7.side_ref = bf16[64,512]{1,0:T(8,128)(2,1)S(1)} collective-permute-done((bf16[64,512]{1,0:T(8,128)(2,1)S(1)}, bf16[64,512]{1,0:T(8,128)(2,1)S(1)}, u32[]{:S(2)}, u32[]{:S(2)}) %collective-permute-start.7) | collective-permute-done | bytes 65568 | tf_op jit(solution)/shard_map/ppermute | solution.py:281
  182.5 7.6 %all-to-all-done.4.parts_ref = bf16[4,256,512]{2,1,0:T(8,128)(2,1)S(1)} async-done(((bf16[4,256,512]{2,1,0:T(8,128)(2,1)}), bf16[4,256,512]{2,1,0:T(8,128)(2,1)S(1)}, u32[]{:S(2)}, u32[]{:S(2)}) %all-to-all-start.4) | async-done | bytes 1048608 | tf_op jit(solution)/shard_map/all_to_all | solution.py:263
  (65 shorter events, 39.2 us)
Async XLA Ops:
  41.9 16.5 %copy-start.3 = (bf16[256,768]{1,0:T(8,128)(2,1)}, bf16[256,768]{1,0:T(8,128)(2,1)S(1)}, u32[]{:S(2)}) copy-start(bf16[256,768]{1,0:T(8,128)(2,1)S(1)} %get-tuple-element.34) | copy-start | bytes 1179652
  42.0 30.5 %copy-start.7 = (s32[256]{0:T(256)S(1)}, s32[256]{0:T(256)}, u32[]{:S(2)}) copy-start(s32[256]{0:T(256)} %param.9) | copy-start | bytes 3076
  42.1 36.7 %copy-start.5 = (f32[2,2048]{1,0:T(2,128)S(1)}, f32[2,2048]{1,0:T(2,128)}, u32[]{:S(2)}) copy-start(f32[2,2048]{1,0:T(2,128)} %refs_4_.3) | copy-start | bytes 49156
  58.4 20.3 %collective-permute-start.3 = (bf16[4,256,768]{2,1,0:T(8,128)(2,1)S(1)}, bf16[4,256,768]{2,1,0:T(8,128)(2,1)S(1)}, u32[]{:S(2)}, u32[]{:S(2)}) collective-permute-start(bf16[4,256,768]{2,1,0:T(8,128)(2,1)S(1)} %all_to_all.25.refs_5_), channel_id=1, source_target_pairs={{0,4},{4,0},{1,5},{5,1},{2,6},{6,2},{3,7},{7,3},{8,12},{12,8},{9,1... | collective-permute-start | bytes 4718600 | tf_op jit(solution)/shard_map/ppermute | solution.py:259
  60.3 15.4 %collective-permute-start = (bf16[256,512]{1,0:T(8,128)(2,1)}, bf16[256,512]{1,0:T(8,128)(2,1)}, u32[]{:S(2)}, u32[]{:S(2)}) collective-permute-start(bf16[256,512]{1,0:T(8,128)(2,1)} %stream_ref.1), channel_id=1, source_target_pairs={{0,2},{1,3},{2,0},{3,1},{4,6},{5,7},{6,4},{7,5},{8,10},{9,11},{10,... | collective-permute-start | bytes 786440 | tf_op jit(solution)/shard_map/ppermute | solution.py:270
  65.4 12.9 %collective-permute-start.1 = (bf16[256,512]{1,0:T(8,128)(2,1)}, bf16[256,512]{1,0:T(8,128)(2,1)}, u32[]{:S(2)}, u32[]{:S(2)}) collective-permute-start(bf16[256,512]{1,0:T(8,128)(2,1)} %stream_ref.1), channel_id=1, source_target_pairs={{0,1},{1,2},{2,3},{3,0},{4,5},{5,6},{6,7},{7,4},{8,9},{9,10},{10,1... | collective-permute-start | bytes 786440 | tf_op jit(solution)/shard_map/ppermute | solution.py:270
  68.0 10.7 %collective-permute-start.2 = (bf16[256,512]{1,0:T(8,128)(2,1)}, bf16[256,512]{1,0:T(8,128)(2,1)}, u32[]{:S(2)}, u32[]{:S(2)}) collective-permute-start(bf16[256,512]{1,0:T(8,128)(2,1)} %stream_ref.1), channel_id=1, source_target_pairs={{0,3},{1,0},{2,1},{3,2},{4,7},{5,4},{6,5},{7,6},{8,11},{9,8},{10,9... | collective-permute-start | bytes 786440 | tf_op jit(solution)/shard_map/ppermute | solution.py:270
  72.5 3.2 %collective-permute-start.5 = (s32[256]{0:T(256)S(1)}, s32[256]{0:T(256)S(1)}, u32[]{:S(2)}, u32[]{:S(2)}) collective-permute-start(s32[256]{0:T(256)S(1)} %copy-done.7), channel_id=1, source_target_pairs={{4,0},{8,4},{12,8},{16,12},{20,16},{24,20},{28,24},{32,28},{36,32}... | collective-permute-start | bytes 3080 | tf_op jit(solution)/shard_map/ppermute | solution.py:276
  75.7 68.7 %copy-start.8 = (s32[256]{0:T(256)}, s32[256]{0:T(256)S(1)}, u32[]{:S(2)}) copy-start(s32[256]{0:T(256)S(1)} %collective-permute-done.5) | copy-start | bytes 3076
  81.0 16.4 %copy-start.6 = (f32[2,256]{1,0:T(2,128)S(1)}, f32[2,256]{1,0:T(2,128)}, u32[]{:S(2)}) copy-start(f32[2,256]{1,0:T(2,128)} %gain_ref.3) | copy-start | bytes 6148
  81.1 4.2 %collective-permute-start.4 = (bf16[128,256]{1,0:T(8,128)(2,1)S(1)}, bf16[128,256]{1,0:T(8,128)(2,1)S(1)}, u32[]{:S(2)}, u32[]{:S(2)}) collective-permute-start(bf16[128,256]{1,0:T(8,128)(2,1)S(1)} %slice.21), channel_id=1, source_target_pairs={{4,0},{8,4},{12,8},{16,12},{20,16},{24,20},{28,24},{32,28},{36,32}... | collective-permute-start | bytes 196616 | tf_op jit(solution)/shard_map/ppermute | solution.py:276
  100.5 25.2 %all-to-all-start.2 = ((bf16[4,256,512]{2,1,0:T(8,128)(2,1)}), bf16[4,256,512]{2,1,0:T(8,128)(2,1)S(1)}, u32[]{:S(2)}, u32[]{:S(2)}) async-start(bf16[4,256,512]{2,1,0:T(8,128)(2,1)} %project.2), calls=%async_computation.2 | async-start | bytes 2097152 | tf_op jit(solution)/shard_map/all_to_all | solution.py:263
  104.1 22.6 %collective-permute-start.11 = (bf16[256,768]{1,0:T(8,128)(2,1)S(1)}, bf16[256,768]{1,0:T(8,128)(2,1)S(1)}, u32[]{:S(2)}, u32[]{:S(2)}) collective-permute-start(bf16[256,768]{1,0:T(8,128)(2,1)S(1)} %copy-done.4), channel_id=1, source_target_pairs={{0,16},{8,24},{16,0},{24,8},{1,17},{9,25},{17,1},{25,9},{2,18},{10... | collective-permute-start | bytes 1179656 | tf_op jit(solution)/shard_map/ppermute | solution.py:270
  108.6 18.1 %collective-permute-start.12 = (bf16[256,768]{1,0:T(8,128)(2,1)S(1)}, bf16[256,768]{1,0:T(8,128)(2,1)S(1)}, u32[]{:S(2)}, u32[]{:S(2)}) collective-permute-start(bf16[256,768]{1,0:T(8,128)(2,1)S(1)} %copy-done.4), channel_id=1, source_target_pairs={{0,8},{8,16},{16,24},{24,0},{1,9},{9,17},{17,25},{25,1},{2,10},{10... | collective-permute-start | bytes 1179656 | tf_op jit(solution)/shard_map/ppermute | solution.py:270
  111.7 17.0 %collective-permute-start.13 = (bf16[256,768]{1,0:T(8,128)(2,1)S(1)}, bf16[256,768]{1,0:T(8,128)(2,1)}, u32[]{:S(2)}, u32[]{:S(2)}) collective-permute-start(bf16[256,768]{1,0:T(8,128)(2,1)S(1)} %copy-done.4), channel_id=1, source_target_pairs={{0,24},{8,0},{16,8},{24,16},{1,25},{9,1},{17,9},{25,17},{2,26},{10... | collective-permute-start | bytes 1179656 | tf_op jit(solution)/shard_map/ppermute | solution.py:270
  115.3 10.3 %collective-permute-start.6 = (bf16[64,512]{1,0:T(8,128)(2,1)S(1)}, bf16[64,512]{1,0:T(8,128)(2,1)S(1)}, u32[]{:S(2)}, u32[]{:S(2)}) collective-permute-start(bf16[64,512]{1,0:T(8,128)(2,1)S(1)} %slice.23), channel_id=1, source_target_pairs={{4,0},{8,4},{12,8},{16,12},{20,16},{24,20},{28,24},{32,28},{36,32}... | collective-permute-start | bytes 196616 | tf_op jit(solution)/shard_map/ppermute | solution.py:276
  129.9 24.5 %collective-permute-start.14 = (bf16[4,256,768]{2,1,0:T(8,128)(2,1)S(1)}, bf16[4,256,768]{2,1,0:T(8,128)(2,1)S(1)}, u32[]{:S(2)}, u32[]{:S(2)}) collective-permute-start(bf16[4,256,768]{2,1,0:T(8,128)(2,1)S(1)} %pad_maximum_fusion.refs_5_), channel_id=1, source_target_pairs={{0,4},{4,0},{1,5},{5,1},{2,6},{6,2},{3,7},{7,3},{8,12},{12,8},{9,1... | collective-permute-start | bytes 4718600 | tf_op jit(solution)/shard_map/ppermute | solution.py:259
  131.9 16.9 %collective-permute-start.10 = (bf16[256,512]{1,0:T(8,128)(2,1)S(1)}, bf16[256,512]{1,0:T(8,128)(2,1)S(1)}, u32[]{:S(2)}, u32[]{:S(2)}) collective-permute-start(bf16[256,512]{1,0:T(8,128)(2,1)S(1)} %add_parts.2.refs_0_.stream_ref), channel_id=1, source_target_pairs={{0,3},{1,0},{2,1},{3,2},{4,7},{5,4},{6,5},{7,6},{8,11},{9,8},{10,9... | collective-permute-start | bytes 786440 | tf_op jit(solution)/shard_map/ppermute | solution.py:270
  137.0 12.6 %collective-permute-start.8 = (bf16[256,512]{1,0:T(8,128)(2,1)S(1)}, bf16[256,512]{1,0:T(8,128)(2,1)S(1)}, u32[]{:S(2)}, u32[]{:S(2)}) collective-permute-start(bf16[256,512]{1,0:T(8,128)(2,1)S(1)} %add_parts.2.refs_0_.stream_ref), channel_id=1, source_target_pairs={{0,2},{1,3},{2,0},{3,1},{4,6},{5,7},{6,4},{7,5},{8,10},{9,11},{10,... | collective-permute-start | bytes 786440 | tf_op jit(solution)/shard_map/ppermute | solution.py:270
  139.7 14.7 %collective-permute-start.9 = (bf16[256,512]{1,0:T(8,128)(2,1)S(1)}, bf16[256,512]{1,0:T(8,128)(2,1)S(1)}, u32[]{:S(2)}, u32[]{:S(2)}) collective-permute-start(bf16[256,512]{1,0:T(8,128)(2,1)S(1)} %add_parts.2.refs_0_.stream_ref), channel_id=1, source_target_pairs={{0,1},{1,2},{2,3},{3,0},{4,5},{5,6},{6,7},{7,4},{8,9},{9,10},{10,1... | collective-permute-start | bytes 786440 | tf_op jit(solution)/shard_map/ppermute | solution.py:270
  142.5 4.9 %collective-permute-start.16 = (s32[256]{0:T(256)S(1)}, s32[256]{0:T(256)S(1)}, u32[]{:S(2)}, u32[]{:S(2)}) collective-permute-start(s32[256]{0:T(256)S(1)} %copy-done.7), channel_id=1, source_target_pairs={{0,4},{4,8},{8,12},{12,16},{16,20},{20,24},{24,28},{28,32},{32,36}... | collective-permute-start | bytes 3080 | tf_op jit(solution)/shard_map/ppermute | solution.py:281
  156.1 5.6 %collective-permute-start.15 = (bf16[128,256]{1,0:T(8,128)(2,1)S(1)}, bf16[128,256]{1,0:T(8,128)(2,1)S(1)}, u32[]{:S(2)}, u32[]{:S(2)}) collective-permute-start(bf16[128,256]{1,0:T(8,128)(2,1)S(1)} %slice.25), channel_id=1, source_target_pairs={{0,4},{4,8},{8,12},{12,16},{16,20},{20,24},{24,28},{28,32},{32,36}... | collective-permute-start | bytes 196616 | tf_op jit(solution)/shard_map/ppermute | solution.py:281
  173.4 16.8 %all-to-all-start.4 = ((bf16[4,256,512]{2,1,0:T(8,128)(2,1)}), bf16[4,256,512]{2,1,0:T(8,128)(2,1)S(1)}, u32[]{:S(2)}, u32[]{:S(2)}) async-start(bf16[4,256,512]{2,1,0:T(8,128)(2,1)} %project.3), calls=%async_computation.4 | async-start | bytes 2097152 | tf_op jit(solution)/shard_map/all_to_all | solution.py:263
  177.0 5.6 %collective-permute-start.7 = (bf16[64,512]{1,0:T(8,128)(2,1)S(1)}, bf16[64,512]{1,0:T(8,128)(2,1)S(1)}, u32[]{:S(2)}, u32[]{:S(2)}) collective-permute-start(bf16[64,512]{1,0:T(8,128)(2,1)S(1)} %slice.28), channel_id=1, source_target_pairs={{0,4},{4,8},{8,12},{12,16},{16,20},{20,24},{24,28},{28,32},{32,36}... | collective-permute-start | bytes 196616 | tf_op jit(solution)/shard_map/ppermute | solution.py:281
  (5 other events, 29.6 us)

commit v5 on v4

--- a/solution.py
+++ b/solution.py
@@ -65,14 +65,18 @@
 
 
 def split_kernel(column_ref, first_ref, rest_ref):
-    first_ref[...] = column_ref[:, : 3 * CH]
+    for x in range(NX):
+        first_ref[x] = column_ref[:, : 3 * CH]
     rest_ref[...] = column_ref[:, 3 * CH :]
 
 
 def split(column):
     return pl.pallas_call(
         split_kernel,
-        out_shape=(jax.ShapeDtypeStruct((NZ * 16, 3 * CH), BF16),) * 2,
+        out_shape=(
+            jax.ShapeDtypeStruct((NX, NZ * 16, 3 * CH), BF16),
+            jax.ShapeDtypeStruct((NZ * 16, 3 * CH), BF16),
+        ),
         in_specs=[VMEM],
         out_specs=(VMEM, VMEM),
         name="split",
@@ -251,10 +255,6 @@
     )(stream, side, parts)
 
 
-def copies_of(x, n):
-    return jnp.broadcast_to(x[None], (n, *x.shape))
-
-
 def swap_core(x):
     return lax.ppermute(x, "c", [(0, 1), (1, 0)])
 
@@ -291,11 +291,13 @@
     out_t = jnp.swapaxes(w_out, 1, 2)
     own = pack(w_value, w_gate, out_t)
     column = lax.all_gather(own, "z", axis=0, tiled=True)
-    first_own, rest_own = split(column)
-    first = exchange(copies_of(first_own, NX), "x")
+    first_copies, rest_own = split(column)
+    first = exchange(first_copies, "x")
     tokens_late, segments_late = lax.optimization_barrier((tokens, segments, column))[:2]
     pieces = ring([tokens_late] * NT, "tp")
+    tokens_head = tokens_late[:R]
     seg_after = from_next(segments_late)
+    seg_before = from_previous(segments_late)
     first_other = swap_core(first)
 
     def seg_rows(*pieces):
@@ -316,15 +318,14 @@
         conv, stat = outer(layer, gated, halo, seg_lanes, taps, inside)
         stats = exchange(stat, "tp").reshape(2 * NT, TOK)
         if layer == 0:
-            tokens_after = from_next(after_(tokens, conv)[:R])
+            tokens_after = from_next(after_(tokens_head, conv))
         parts = project(layer, conv, stats, norm_gain, out_weight)
         received = exchange(parts, "tp")
         side = tokens_after if layer == 0 else stream_before
         stream = add_parts(layer, stream, side, received)
         if layer == 0:
             stream_before = from_previous(stream[TOK - R :])
-            seg_before = from_previous(after_(segments, stream))
-            seg_lanes = seg_rows(seg_before[TOK - R :], segments, seg_after[:R])
+            seg_lanes = seg_rows(after_(seg_before, stream)[TOK - R :], segments, seg_after[:R])
             rest = ring([after_(rest_own, parts)] * NX, "x")
             pieces = ring([stream] * NT, "tp")
             rest = jnp.stack(list(lax.optimization_barrier((*rest, stream))[:NX]))

time: 193 us -> 194 us (level)
  no operation moved by 1% of the time
where the time goes in v5:
time: 194 us; the launch traced here: 192 us
  blocking collectives  74.3 us (38%)
  starting transfers between devices  56 us (29%)
  waiting for transfers between devices  36.9 us (19%)
  Pallas kernels  20.5 us (11%)
  local copies, waits for them, and re-layouts  2.44 us (1%)
    all_gather x1, blocking collectives, program(): column = lax.all_gather(own, 'z', axis=0, tiled=True)  40.4 us
    all_to_all x3, blocking collectives, exchange(): return lax.all_to_all(x, axis, 0, 0, tiled=True)  33.9 us
    ppermute x9, starting transfers between devices, ring(): lax.ppermute(piece, axis, [(i, (i + step) % n) for i in range(n)])  33.1 us
    ppermute x9, waiting for transfers between devices, ring(): lax.ppermute(piece, axis, [(i, (i + step) % n) for i in range(n)])  12.1 us
    ppermute x3, waiting for transfers between devices, from_next(): return lax.ppermute(x, SP, [((i + 1) % n, i) for i in range(n)])  9.37 us
    all_to_all x2, waiting for transfers between devices, exchange(): return lax.all_to_all(x, axis, 0, 0, tiled=True)  7.85 us
    ppermute x3, waiting for transfers between devices, from_previous(): return lax.ppermute(x, SP, [(i, (i + 1) % n) for i in range(n)])  7.65 us
    all_to_all x2, starting transfers between devices, exchange(): return lax.all_to_all(x, axis, 0, 0, tiled=True)  7.16 us
  transfers between devices with their start and end apart: 19, of which 12 were waited for; matrix products, arithmetic and copies ran while one was open for 1% of the time, Pallas kernels for 3%

profile of v5, /device:TPU:6, one launch (start us, length us, event | category | flops | bytes accessed | tf_op | source)
XLA Modules:
  0.0 191.8 jit_solution(4440461957870400370)
XLA Ops:
  1.5 40.4 %all_gather.3.column_ref = bf16[256,1536]{1,0:T(8,128)(2,1)S(1)} all-gather(bf16[16,1536]{1,0:T(8,128)(2,1)} %pack.1), channel_id=1, replica_groups=mesh['z'=16,'x'=4,'c'=2,'tp'=4] {'z'}, dimensions={0}, use_global_device_ids=true | all-gather | bytes 835584 | tf_op jit(solution)/shard_map/all_gather | solution.py:293
  42.0 16.3 %all_to_all.25.refs_5_ = bf16[4,256,768]{2,1,0:T(8,128)(2,1)S(1)} all-to-all(bf16[4,256,768]{2,1,0:T(8,128)(2,1)S(1)} %get-tuple-element.25), channel_id=1, replica_groups=mesh['z'=16,'x'=4,'c'=2,'tp'=4] {'x'}, dimensions={0} | all-to-all | bytes 3145728 | tf_op jit(solution)/shard_map/all_to_all | solution.py:263
  60.3 5.1 %collective-permute-start = (bf16[256,512]{1,0:T(8,128)(2,1)}, bf16[256,512]{1,0:T(8,128)(2,1)}, u32[]{:S(2)}, u32[]{:S(2)}) collective-permute-start(bf16[256,512]{1,0:T(8,128)(2,1)} %stream_ref.1), channel_id=1, source_target_pairs={{0,2},{1,3},{2,0},{3,1},{4,6},{5,7},{6,4},{7,5},{8,10},{9,11},{10,... | collective-permute-start | bytes 786440 | tf_op jit(solution)/shard_map/ppermute | solution.py:270
  65.4 2.6 %collective-permute-start.1 = (bf16[256,512]{1,0:T(8,128)(2,1)}, bf16[256,512]{1,0:T(8,128)(2,1)}, u32[]{:S(2)}, u32[]{:S(2)}) collective-permute-start(bf16[256,512]{1,0:T(8,128)(2,1)} %stream_ref.1), channel_id=1, source_target_pairs={{0,1},{1,2},{2,3},{3,0},{4,5},{5,6},{6,7},{7,4},{8,9},{9,10},{10,1... | collective-permute-start | bytes 786440 | tf_op jit(solution)/shard_map/ppermute | solution.py:270
  68.0 4.5 %collective-permute-start.2 = (bf16[256,512]{1,0:T(8,128)(2,1)}, bf16[256,512]{1,0:T(8,128)(2,1)}, u32[]{:S(2)}, u32[]{:S(2)}) collective-permute-start(bf16[256,512]{1,0:T(8,128)(2,1)} %stream_ref.1), channel_id=1, source_target_pairs={{0,3},{1,0},{2,1},{3,2},{4,7},{5,4},{6,5},{7,6},{8,11},{9,8},{10,9... | collective-permute-start | bytes 786440 | tf_op jit(solution)/shard_map/ppermute | solution.py:270
  75.7 2.6 %collective-permute-done.1.refs_2_ = bf16[256,512]{1,0:T(8,128)(2,1)} collective-permute-done((bf16[256,512]{1,0:T(8,128)(2,1)}, bf16[256,512]{1,0:T(8,128)(2,1)}, u32[]{:S(2)}, u32[]{:S(2)}) %collective-permute-start.1) | collective-permute-done | bytes 262176 | tf_op jit(solution)/shard_map/ppermute | solution.py:270
  78.7 2.3 %gate.2 = (bf16[256,256]{1,0:T(8,128)(2,1)S(1)}, bf16[16,4,2,16,256]{4,3,2,1,0:T(8,128)(2,1)S(1)}) custom-call(s32[3]{0:T(128)S(1)} %pad_add_fusion.2.at_ref, bf16[256,512]{1,0:T(8,128)(2,1)} %stream_ref.1, bf16[256,512]{1,0:T(8,128)(2,1)} %collective-permute-done.refs_1_, bf16[256,512]{1,0:T(8,128)(2,1)} %collective-permute-done.1.refs_2_, ...), custom_call_target="tpu_custom_call" | custom-call | tf_op jit(solution)/shard_map/gate/pallas_call | solution.py:106
  85.5 2.5 %outer.2 = (f32[256,256]{1,0:T(8,128)S(1)}, f32[4,2,256]{2,1,0:T(2,128)S(1)}) custom-call(bf16[256,256]{1,0:T(8,128)(2,1)S(1)} %get-tuple-element.26.own_ref, bf16[128,256]{1,0:T(8,128)(2,1)S(1)} %collective-permute-done.4.halo_ref, s32[384,128]{1,0:T(8,128)S(1)} %broadcast_in_dim.4.seg_ref, f32[129,2,256]{2,1,0:T(2,128)S(1)} %bitcast.10, ...), custom_call_target="tpu_custom_call" | custom-call | tf_op jit(solution)/shard_map/outer/pallas_call | solution.py:188
  87.9 9.8 %all_to_all.26 = f32[4,2,256]{2,1,0:T(2,128)S(1)} all-to-all(f32[4,2,256]{2,1,0:T(2,128)S(1)} %get-tuple-element.30), channel_id=1, replica_groups=mesh['z'=16,'x'=4,'c'=2,'tp'=4] {'tp'}, dimensions={0} | all-to-all | bytes 16384 | tf_op jit(solution)/shard_map/all_to_all | solution.py:263
  100.8 3.6 %all-to-all-start.2 = ((bf16[4,256,512]{2,1,0:T(8,128)(2,1)}), bf16[4,256,512]{2,1,0:T(8,128)(2,1)S(1)}, u32[]{:S(2)}, u32[]{:S(2)}) async-start(bf16[4,256,512]{2,1,0:T(8,128)(2,1)} %project.2), calls=%async_computation.2 | async-start | bytes 2097152 | tf_op jit(solution)/shard_map/all_to_all | solution.py:263
  104.5 4.5 %collective-permute-start.11 = (bf16[256,768]{1,0:T(8,128)(2,1)S(1)}, bf16[256,768]{1,0:T(8,128)(2,1)S(1)}, u32[]{:S(2)}, u32[]{:S(2)}) collective-permute-start(bf16[256,768]{1,0:T(8,128)(2,1)S(1)} %copy-done.4), channel_id=1, source_target_pairs={{0,16},{8,24},{16,0},{24,8},{1,17},{9,25},{17,1},{25,9},{2,18},{10... | collective-permute-start | bytes 1179656 | tf_op jit(solution)/shard_map/ppermute | solution.py:270
  109.0 3.1 %collective-permute-start.12 = (bf16[256,768]{1,0:T(8,128)(2,1)S(1)}, bf16[256,768]{1,0:T(8,128)(2,1)S(1)}, u32[]{:S(2)}, u32[]{:S(2)}) collective-permute-start(bf16[256,768]{1,0:T(8,128)(2,1)S(1)} %copy-done.4), channel_id=1, source_target_pairs={{0,8},{8,16},{16,24},{24,0},{1,9},{9,17},{17,25},{25,1},{2,10},{10... | collective-permute-start | bytes 1179656 | tf_op jit(solution)/shard_map/ppermute | solution.py:270
  112.1 2.8 %collective-permute-start.13 = (bf16[256,768]{1,0:T(8,128)(2,1)S(1)}, bf16[256,768]{1,0:T(8,128)(2,1)}, u32[]{:S(2)}, u32[]{:S(2)}) collective-permute-start(bf16[256,768]{1,0:T(8,128)(2,1)S(1)} %copy-done.4), channel_id=1, source_target_pairs={{0,24},{8,0},{16,8},{24,16},{1,25},{9,1},{17,9},{25,17},{2,26},{10... | collective-permute-start | bytes 1179656 | tf_op jit(solution)/shard_map/ppermute | solution.py:270
  117.6 8.2 %collective-permute-done.6.side_ref = bf16[64,512]{1,0:T(8,128)(2,1)S(1)} collective-permute-done((bf16[64,512]{1,0:T(8,128)(2,1)S(1)}, bf16[64,512]{1,0:T(8,128)(2,1)S(1)}, u32[]{:S(2)}, u32[]{:S(2)}) %collective-permute-start.6) | collective-permute-done | bytes 65568 | tf_op jit(solution)/shard_map/ppermute | solution.py:276
  132.2 5.1 %collective-permute-start.10 = (bf16[256,512]{1,0:T(8,128)(2,1)S(1)}, bf16[256,512]{1,0:T(8,128)(2,1)S(1)}, u32[]{:S(2)}, u32[]{:S(2)}) collective-permute-start(bf16[256,512]{1,0:T(8,128)(2,1)S(1)} %add_parts.2.refs_0_.stream_ref), channel_id=1, source_target_pairs={{0,3},{1,0},{2,1},{3,2},{4,7},{5,4},{6,5},{7,6},{8,11},{9,8},{10,9... | collective-permute-start | bytes 786440 | tf_op jit(solution)/shard_map/ppermute | solution.py:270
  137.3 2.8 %collective-permute-start.8 = (bf16[256,512]{1,0:T(8,128)(2,1)S(1)}, bf16[256,512]{1,0:T(8,128)(2,1)S(1)}, u32[]{:S(2)}, u32[]{:S(2)}) collective-permute-start(bf16[256,512]{1,0:T(8,128)(2,1)S(1)} %add_parts.2.refs_0_.stream_ref), channel_id=1, source_target_pairs={{0,2},{1,3},{2,0},{3,1},{4,6},{5,7},{6,4},{7,5},{8,10},{9,11},{10,... | collective-permute-start | bytes 786440 | tf_op jit(solution)/shard_map/ppermute | solution.py:270
  140.1 2.8 %collective-permute-start.9 = (bf16[256,512]{1,0:T(8,128)(2,1)S(1)}, bf16[256,512]{1,0:T(8,128)(2,1)S(1)}, u32[]{:S(2)}, u32[]{:S(2)}) collective-permute-start(bf16[256,512]{1,0:T(8,128)(2,1)S(1)} %add_parts.2.refs_0_.stream_ref), channel_id=1, source_target_pairs={{0,1},{1,2},{2,3},{3,0},{4,5},{5,6},{6,7},{7,4},{8,9},{9,10},{10,1... | collective-permute-start | bytes 786440 | tf_op jit(solution)/shard_map/ppermute | solution.py:270
  144.8 3.0 %collective-permute-done.16 = s32[256]{0:T(256)S(1)} collective-permute-done((s32[256]{0:T(256)S(1)}, s32[256]{0:T(256)S(1)}, u32[]{:S(2)}, u32[]{:S(2)}) %collective-permute-start.16) | collective-permute-done | bytes 1056 | tf_op jit(solution)/shard_map/ppermute | solution.py:281
  150.0 4.8 %collective-permute-done.9.refs_2_ = bf16[256,512]{1,0:T(8,128)(2,1)S(1)} collective-permute-done((bf16[256,512]{1,0:T(8,128)(2,1)S(1)}, bf16[256,512]{1,0:T(8,128)(2,1)S(1)}, u32[]{:S(2)}, u32[]{:S(2)}) %collective-permute-start.9) | collective-permute-done | bytes 262176 | tf_op jit(solution)/shard_map/ppermute | solution.py:270
  162.1 2.4 %outer.3 = (f32[256,256]{1,0:T(8,128)S(1)}, f32[4,2,256]{2,1,0:T(2,128)S(1)}) custom-call(bf16[256,256]{1,0:T(8,128)(2,1)S(1)} %get-tuple-element.38.own_ref, bf16[128,256]{1,0:T(8,128)(2,1)S(1)} %collective-permute-done.15.halo_ref, s32[384,128]{1,0:T(8,128)S(1)} %broadcast_in_dim.5.seg_ref, f32[129,2,256]{2,1,0:T(2,128)S(1)} %bitcast.12, ...), custom_call_target="tpu_custom_call" | custom-call | tf_op jit(solution)/shard_map/outer/pallas_call | solution.py:188
  164.5 7.7 %all_to_all.27 = f32[4,2,256]{2,1,0:T(2,128)S(1)} all-to-all(f32[4,2,256]{2,1,0:T(2,128)S(1)} %get-tuple-element.41), channel_id=1, replica_groups=mesh['z'=16,'x'=4,'c'=2,'tp'=4] {'tp'}, dimensions={0} | all-to-all | bytes 16384 | tf_op jit(solution)/shard_map/all_to_all | solution.py:263
  174.0 3.5 %all-to-all-start.4 = ((bf16[4,256,512]{2,1,0:T(8,128)(2,1)}), bf16[4,256,512]{2,1,0:T(8,128)(2,1)S(1)}, u32[]{:S(2)}, u32[]{:S(2)}) async-start(bf16[4,256,512]{2,1,0:T(8,128)(2,1)} %project.3), calls=%async_computation.4 | async-start | bytes 2097152 | tf_op jit(solution)/shard_map/all_to_all | solution.py:263
  179.5 3.7 %collective-permute-done.7.side_ref = bf16[64,512]{1,0:T(8,128)(2,1)S(1)} collective-permute-done((bf16[64,512]{1,0:T(8,128)(2,1)S(1)}, bf16[64,512]{1,0:T(8,128)(2,1)S(1)}, u32[]{:S(2)}, u32[]{:S(2)}) %collective-permute-start.7) | collective-permute-done | bytes 65568 | tf_op jit(solution)/shard_map/ppermute | solution.py:281
  183.1 7.8 %all-to-all-done.4.parts_ref = bf16[4,256,512]{2,1,0:T(8,128)(2,1)S(1)} async-done(((bf16[4,256,512]{2,1,0:T(8,128)(2,1)}), bf16[4,256,512]{2,1,0:T(8,128)(2,1)S(1)}, u32[]{:S(2)}, u32[]{:S(2)}) %all-to-all-start.4) | async-done | bytes 1048608 | tf_op jit(solution)/shard_map/all_to_all | solution.py:263
  (64 shorter events, 39.6 us)
Async XLA Ops:
  42.0 16.4 %copy-start.3 = (bf16[256,768]{1,0:T(8,128)(2,1)}, bf16[256,768]{1,0:T(8,128)(2,1)S(1)}, u32[]{:S(2)}) copy-start(bf16[256,768]{1,0:T(8,128)(2,1)S(1)} %get-tuple-element.34) | copy-start | bytes 1179652
  42.0 30.5 %copy-start.7 = (s32[256]{0:T(256)S(1)}, s32[256]{0:T(256)}, u32[]{:S(2)}) copy-start(s32[256]{0:T(256)} %param.9) | copy-start | bytes 3076
  42.0 36.7 %copy-start.5 = (f32[2,2048]{1,0:T(2,128)S(1)}, f32[2,2048]{1,0:T(2,128)}, u32[]{:S(2)}) copy-start(f32[2,2048]{1,0:T(2,128)} %refs_4_.3) | copy-start | bytes 49156
  58.4 20.3 %collective-permute-start.3 = (bf16[4,256,768]{2,1,0:T(8,128)(2,1)S(1)}, bf16[4,256,768]{2,1,0:T(8,128)(2,1)S(1)}, u32[]{:S(2)}, u32[]{:S(2)}) collective-permute-start(bf16[4,256,768]{2,1,0:T(8,128)(2,1)S(1)} %all_to_all.25.refs_5_), channel_id=1, source_target_pairs={{0,4},{4,0},{1,5},{5,1},{2,6},{6,2},{3,7},{7,3},{8,12},{12,8},{9,1... | collective-permute-start | bytes 4718600 | tf_op jit(solution)/shard_map/ppermute | solution.py:259
  60.3 15.4 %collective-permute-start = (bf16[256,512]{1,0:T(8,128)(2,1)}, bf16[256,512]{1,0:T(8,128)(2,1)}, u32[]{:S(2)}, u32[]{:S(2)}) collective-permute-start(bf16[256,512]{1,0:T(8,128)(2,1)} %stream_ref.1), channel_id=1, source_target_pairs={{0,2},{1,3},{2,0},{3,1},{4,6},{5,7},{6,4},{7,5},{8,10},{9,11},{10,... | collective-permute-start | bytes 786440 | tf_op jit(solution)/shard_map/ppermute | solution.py:270
  65.4 12.9 %collective-permute-start.1 = (bf16[256,512]{1,0:T(8,128)(2,1)}, bf16[256,512]{1,0:T(8,128)(2,1)}, u32[]{:S(2)}, u32[]{:S(2)}) collective-permute-start(bf16[256,512]{1,0:T(8,128)(2,1)} %stream_ref.1), channel_id=1, source_target_pairs={{0,1},{1,2},{2,3},{3,0},{4,5},{5,6},{6,7},{7,4},{8,9},{9,10},{10,1... | collective-permute-start | bytes 786440 | tf_op jit(solution)/shard_map/ppermute | solution.py:270
  68.0 10.7 %collective-permute-start.2 = (bf16[256,512]{1,0:T(8,128)(2,1)}, bf16[256,512]{1,0:T(8,128)(2,1)}, u32[]{:S(2)}, u32[]{:S(2)}) collective-permute-start(bf16[256,512]{1,0:T(8,128)(2,1)} %stream_ref.1), channel_id=1, source_target_pairs={{0,3},{1,0},{2,1},{3,2},{4,7},{5,4},{6,5},{7,6},{8,11},{9,8},{10,9... | collective-permute-start | bytes 786440 | tf_op jit(solution)/shard_map/ppermute | solution.py:270
  72.5 3.2 %collective-permute-start.5 = (s32[256]{0:T(256)S(1)}, s32[256]{0:T(256)S(1)}, u32[]{:S(2)}, u32[]{:S(2)}) collective-permute-start(s32[256]{0:T(256)S(1)} %copy-done.7), channel_id=1, source_target_pairs={{4,0},{8,4},{12,8},{16,12},{20,16},{24,20},{28,24},{32,28},{36,32}... | collective-permute-start | bytes 3080 | tf_op jit(solution)/shard_map/ppermute | solution.py:276
  75.7 69.1 %copy-start.8 = (s32[256]{0:T(256)}, s32[256]{0:T(256)S(1)}, u32[]{:S(2)}) copy-start(s32[256]{0:T(256)S(1)} %collective-permute-done.5) | copy-start | bytes 3076
  81.0 16.8 %copy-start.6 = (f32[2,256]{1,0:T(2,128)S(1)}, f32[2,256]{1,0:T(2,128)}, u32[]{:S(2)}) copy-start(f32[2,256]{1,0:T(2,128)} %gain_ref.3) | copy-start | bytes 6148
  81.0 4.4 %collective-permute-start.4 = (bf16[128,256]{1,0:T(8,128)(2,1)S(1)}, bf16[128,256]{1,0:T(8,128)(2,1)S(1)}, u32[]{:S(2)}, u32[]{:S(2)}) collective-permute-start(bf16[128,256]{1,0:T(8,128)(2,1)S(1)} %slice.22), channel_id=1, source_target_pairs={{4,0},{8,4},{12,8},{16,12},{20,16},{24,20},{28,24},{32,28},{36,32}... | collective-permute-start | bytes 196616 | tf_op jit(solution)/shard_map/ppermute | solution.py:276
  100.8 25.0 %all-to-all-start.2 = ((bf16[4,256,512]{2,1,0:T(8,128)(2,1)}), bf16[4,256,512]{2,1,0:T(8,128)(2,1)S(1)}, u32[]{:S(2)}, u32[]{:S(2)}) async-start(bf16[4,256,512]{2,1,0:T(8,128)(2,1)} %project.2), calls=%async_computation.2 | async-start | bytes 2097152 | tf_op jit(solution)/shard_map/all_to_all | solution.py:263
  104.5 22.4 %collective-permute-start.11 = (bf16[256,768]{1,0:T(8,128)(2,1)S(1)}, bf16[256,768]{1,0:T(8,128)(2,1)S(1)}, u32[]{:S(2)}, u32[]{:S(2)}) collective-permute-start(bf16[256,768]{1,0:T(8,128)(2,1)S(1)} %copy-done.4), channel_id=1, source_target_pairs={{0,16},{8,24},{16,0},{24,8},{1,17},{9,25},{17,1},{25,9},{2,18},{10... | collective-permute-start | bytes 1179656 | tf_op jit(solution)/shard_map/ppermute | solution.py:270
  109.0 17.9 %collective-permute-start.12 = (bf16[256,768]{1,0:T(8,128)(2,1)S(1)}, bf16[256,768]{1,0:T(8,128)(2,1)S(1)}, u32[]{:S(2)}, u32[]{:S(2)}) collective-permute-start(bf16[256,768]{1,0:T(8,128)(2,1)S(1)} %copy-done.4), channel_id=1, source_target_pairs={{0,8},{8,16},{16,24},{24,0},{1,9},{9,17},{17,25},{25,1},{2,10},{10... | collective-permute-start | bytes 1179656 | tf_op jit(solution)/shard_map/ppermute | solution.py:270
  112.1 17.0 %collective-permute-start.13 = (bf16[256,768]{1,0:T(8,128)(2,1)S(1)}, bf16[256,768]{1,0:T(8,128)(2,1)}, u32[]{:S(2)}, u32[]{:S(2)}) collective-permute-start(bf16[256,768]{1,0:T(8,128)(2,1)S(1)} %copy-done.4), channel_id=1, source_target_pairs={{0,24},{8,0},{16,8},{24,16},{1,25},{9,1},{17,9},{25,17},{2,26},{10... | collective-permute-start | bytes 1179656 | tf_op jit(solution)/shard_map/ppermute | solution.py:270
  115.7 10.1 %collective-permute-start.6 = (bf16[64,512]{1,0:T(8,128)(2,1)S(1)}, bf16[64,512]{1,0:T(8,128)(2,1)S(1)}, u32[]{:S(2)}, u32[]{:S(2)}) collective-permute-start(bf16[64,512]{1,0:T(8,128)(2,1)S(1)} %slice.21), channel_id=1, source_target_pairs={{4,0},{8,4},{12,8},{16,12},{20,16},{24,20},{28,24},{32,28},{36,32}... | collective-permute-start | bytes 196616 | tf_op jit(solution)/shard_map/ppermute | solution.py:276
  130.3 24.5 %collective-permute-start.14 = (bf16[4,256,768]{2,1,0:T(8,128)(2,1)S(1)}, bf16[4,256,768]{2,1,0:T(8,128)(2,1)S(1)}, u32[]{:S(2)}, u32[]{:S(2)}) collective-permute-start(bf16[4,256,768]{2,1,0:T(8,128)(2,1)S(1)} %pad_maximum_fusion.refs_5_), channel_id=1, source_target_pairs={{0,4},{4,0},{1,5},{5,1},{2,6},{6,2},{3,7},{7,3},{8,12},{12,8},{9,1... | collective-permute-start | bytes 4718600 | tf_op jit(solution)/shard_map/ppermute | solution.py:259
  132.2 16.9 %collective-permute-start.10 = (bf16[256,512]{1,0:T(8,128)(2,1)S(1)}, bf16[256,512]{1,0:T(8,128)(2,1)S(1)}, u32[]{:S(2)}, u32[]{:S(2)}) collective-permute-start(bf16[256,512]{1,0:T(8,128)(2,1)S(1)} %add_parts.2.refs_0_.stream_ref), channel_id=1, source_target_pairs={{0,3},{1,0},{2,1},{3,2},{4,7},{5,4},{6,5},{7,6},{8,11},{9,8},{10,9... | collective-permute-start | bytes 786440 | tf_op jit(solution)/shard_map/ppermute | solution.py:270
  137.3 12.6 %collective-permute-start.8 = (bf16[256,512]{1,0:T(8,128)(2,1)S(1)}, bf16[256,512]{1,0:T(8,128)(2,1)S(1)}, u32[]{:S(2)}, u32[]{:S(2)}) collective-permute-start(bf16[256,512]{1,0:T(8,128)(2,1)S(1)} %add_parts.2.refs_0_.stream_ref), channel_id=1, source_target_pairs={{0,2},{1,3},{2,0},{3,1},{4,6},{5,7},{6,4},{7,5},{8,10},{9,11},{10,... | collective-permute-start | bytes 786440 | tf_op jit(solution)/shard_map/ppermute | solution.py:270
  140.1 14.7 %collective-permute-start.9 = (bf16[256,512]{1,0:T(8,128)(2,1)S(1)}, bf16[256,512]{1,0:T(8,128)(2,1)S(1)}, u32[]{:S(2)}, u32[]{:S(2)}) collective-permute-start(bf16[256,512]{1,0:T(8,128)(2,1)S(1)} %add_parts.2.refs_0_.stream_ref), channel_id=1, source_target_pairs={{0,1},{1,2},{2,3},{3,0},{4,5},{5,6},{6,7},{7,4},{8,9},{9,10},{10,1... | collective-permute-start | bytes 786440 | tf_op jit(solution)/shard_map/ppermute | solution.py:270
  142.9 4.9 %collective-permute-start.16 = (s32[256]{0:T(256)S(1)}, s32[256]{0:T(256)S(1)}, u32[]{:S(2)}, u32[]{:S(2)}) collective-permute-start(s32[256]{0:T(256)S(1)} %copy-done.7), channel_id=1, source_target_pairs={{0,4},{4,8},{8,12},{12,16},{16,20},{20,24},{24,28},{28,32},{32,36}... | collective-permute-start | bytes 3080 | tf_op jit(solution)/shard_map/ppermute | solution.py:281
  156.5 5.6 %collective-permute-start.15 = (bf16[128,256]{1,0:T(8,128)(2,1)S(1)}, bf16[128,256]{1,0:T(8,128)(2,1)S(1)}, u32[]{:S(2)}, u32[]{:S(2)}) collective-permute-start(bf16[128,256]{1,0:T(8,128)(2,1)S(1)} %slice.25), channel_id=1, source_target_pairs={{0,4},{4,8},{8,12},{12,16},{16,20},{20,24},{24,28},{28,32},{32,36}... | collective-permute-start | bytes 196616 | tf_op jit(solution)/shard_map/ppermute | solution.py:281
  174.0 17.0 %all-to-all-start.4 = ((bf16[4,256,512]{2,1,0:T(8,128)(2,1)}), bf16[4,256,512]{2,1,0:T(8,128)(2,1)S(1)}, u32[]{:S(2)}, u32[]{:S(2)}) async-start(bf16[4,256,512]{2,1,0:T(8,128)(2,1)} %project.3), calls=%async_computation.4 | async-start | bytes 2097152 | tf_op jit(solution)/shard_map/all_to_all | solution.py:263
  177.5 5.6 %collective-permute-start.7 = (bf16[64,512]{1,0:T(8,128)(2,1)S(1)}, bf16[64,512]{1,0:T(8,128)(2,1)S(1)}, u32[]{:S(2)}, u32[]{:S(2)}) collective-permute-start(bf16[64,512]{1,0:T(8,128)(2,1)S(1)} %slice.28), channel_id=1, source_target_pairs={{0,4},{4,8},{8,12},{12,16},{16,20},{20,24},{24,28},{28,32},{32,36}... | collective-permute-start | bytes 196616 | tf_op jit(solution)/shard_map/ppermute | solution.py:281
  (5 other events, 30.1 us)
